TPU v7x, 32 devices: a whole 2x2x4 slice. The times are simulated.
32 devices in a mesh: ep: 8 (over z, y), tp: 4 (over x, core).
Axes of the slice: x: 2, y: 2, z: 4, core: 2. Of those that a mesh axis runs over, the one named last changes fastest.
Arguments:
- tokens: bfloat16 [64, 1024], P('ep'), may hold values from -6 to 6
- mix_gain: float32 [1024], replicated, may hold values from 0.1 to 1.9
- w_query: bfloat16 [1024, 512], P(None, 'tp'), may hold values from -0.1875 to 0.1875
- w_key: bfloat16 [1024, 512], P(None, 'tp'), may hold values from -0.1875 to 0.1875
- w_value: bfloat16 [1024, 1024], P(None, 'tp'), may hold values from -0.1875 to 0.1875
- w_ogate: bfloat16 [1024, 1024], P(None, 'tp'), may hold values from -0.1875 to 0.1875
- w_igate: bfloat16 [1024, 4], replicated, may hold values from -0.1875 to 0.1875
- w_fgate: bfloat16 [1024, 4], replicated, may hold values from -0.1875 to 0.1875
- forget_bias: float32 [4], replicated, may hold values from -1 to 3
- head_gain: float32 [1024], P('tp'), may hold values from 0.1 to 1.9
- w_out: bfloat16 [1024, 1024], P('tp'), may hold values from -0.1875 to 0.1875
- memory: float32 [64, 4, 128, 256], P('ep', 'tp'), may hold values from -0.4 to 0.4
- normalizer: float32 [64, 4, 128], P('ep', 'tp'), may hold values from -0.4 to 0.4
- running_max: float32 [64, 4], P('ep', 'tp'), may hold values from -4 to 4
- ffn_gain: float32 [1024], replicated, may hold values from 0.1 to 1.9
- route: int32 [64, 2], replicated, may hold values from 0 to 7, all different within a row; in each aligned block of 64 rows (0 to 63, 64 to 127, ...) at most 32 rows name the same one
- route_weight: float32 [64, 2], replicated, may hold values from 0.05 to 1
- w_gate: bfloat16 [8, 1024, 512], P('ep', None, 'tp'), may hold values from -0.1875 to 0.1875
- w_up: bfloat16 [8, 1024, 512], P('ep', None, 'tp'), may hold values from -0.1875 to 0.1875
- w_down: bfloat16 [8, 512, 1024], P('ep', 'tp'), may hold values from -0.25 to 0.25
Outputs:
- mixed: bfloat16 [64, 1024], P(None, 'ep')
- new_memory: float32 [64, 4, 128, 256], P('ep', 'tp')
- new_normalizer: float32 [64, 4, 128], P('ep', 'tp')
- new_max: float32 [64, 4], P('ep', 'tp')
Inputs may be any that keep to these rules, and one draw needn't show every extreme that they name: `route`: each expert is named by at most 32 routes in all, a bound that some block reaches; the two choices of a token differ.
All inputs are finite; a program needn't handle non-finite values.
Results may differ from a plain program's by a relative error of at most 0.014.
Values may be sent and summed in bfloat16 or wider, within the bound.
No kernel may reach another device: no remote copies, remote signals or barrier semaphores. Data moves between devices by JAX's collectives and lax.ppermute only.
A program may use at most 64 MiB of HBM per device.

v0:
```python
import jax
import jax.numpy as jnp
from jax import lax
from jax.sharding import PartitionSpec as P

EXPERT_CAPACITY = 32


EPS = 1e-06


def round_trip(values):
    rounded = lax.optimization_barrier(values.astype(jnp.bfloat16))
    return rounded.astype(jnp.float32)


def norm_rows(values, gain):
    floats = values.astype(jnp.float32)
    scale = lax.rsqrt(jnp.mean(floats * floats, axis=-1, keepdims=True) + EPS)
    return (floats * scale * gain).astype(jnp.bfloat16)


def slot_targets(route, expert_count, capacity):
    flat = route.reshape(-1)
    onehot = (flat[:, None] == jnp.arange(expert_count, dtype=jnp.int32)[None, :]).astype(jnp.int32)
    before = jnp.cumsum(onehot, axis=0) - onehot
    slot = jnp.sum(before * onehot, axis=1)
    return flat * capacity + slot


def shards(
    tokens,
    mix_gain,
    w_query,
    w_key,
    w_value,
    w_ogate,
    w_igate,
    w_fgate,
    forget_bias,
    head_gain,
    w_out,
    memory,
    normalizer,
    running_max,
    ffn_gain,
    route,
    route_weight,
    w_gate,
    w_up,
    w_down,
):
    width = tokens.shape[1]
    col_count = width // lax.axis_size("ep")
    qk_dim = w_query.shape[1]
    normed = norm_rows(tokens, mix_gain)
    query = round_trip(jnp.dot(normed, w_query, preferred_element_type=jnp.float32))
    scaled_key = round_trip(
        jnp.dot(normed, w_key, preferred_element_type=jnp.float32)
    ) * qk_dim ** (-0.5)
    value = round_trip(jnp.dot(normed, w_value, preferred_element_type=jnp.float32))
    ogate = round_trip(jnp.dot(normed, w_ogate, preferred_element_type=jnp.float32))
    head_pick = (jnp.arange(w_igate.shape[1], dtype=jnp.int32) == lax.axis_index("tp")).astype(
        jnp.float32
    )
    log_in = jnp.sum(
        jnp.dot(normed, w_igate, preferred_element_type=jnp.float32) * head_pick, axis=1
    )
    forget_pre = jnp.sum(
        jnp.dot(normed, w_fgate, preferred_element_type=jnp.float32) * head_pick, axis=1
    )
    log_forget = jax.nn.log_sigmoid(forget_pre + jnp.sum(forget_bias * head_pick))
    old_max = running_max[:, 0]
    new_max = jnp.maximum(log_forget + old_max, log_in)
    keep = jnp.exp(log_forget + old_max - new_max)
    admit = jnp.exp(log_in - new_max)
    state = (
        keep[:, None, None] * memory[:, 0]
        + admit[:, None, None] * scaled_key[:, :, None] * value[:, None, :]
    )
    norm_state = keep[:, None] * normalizer[:, 0] + admit[:, None] * scaled_key
    numer = jnp.einsum("tk,tkv->tv", query, state, precision=lax.Precision.HIGHEST)
    denom = jnp.sum(query * norm_state, axis=1)
    read = numer / jnp.maximum(jnp.abs(denom), jnp.exp(-new_max))[:, None]
    scale = lax.rsqrt(jnp.mean(read * read, axis=-1, keepdims=True) + EPS)
    gated = (jax.nn.sigmoid(ogate) * read * scale * head_gain).astype(jnp.bfloat16)
    local_output = lax.psum(
        jnp.dot(gated, w_out, preferred_element_type=jnp.float32).astype(jnp.bfloat16), "tp"
    ).astype(jnp.float32)
    middle_rows = (tokens.astype(jnp.float32) + local_output).astype(jnp.bfloat16)
    middle = lax.all_to_all(middle_rows, "ep", split_axis=1, concat_axis=0, tiled=True)
    expert_count = w_gate.shape[0] * lax.axis_size("ep")
    topk_count = route.shape[1]
    targets = slot_targets(route, expert_count, EXPERT_CAPACITY)
    buffer = (
        jnp.zeros((expert_count * EXPERT_CAPACITY, col_count), jnp.bfloat16)
        .at[targets]
        .set(jnp.repeat(middle, topk_count, axis=0))
    )
    buffer = buffer.reshape(expert_count, EXPERT_CAPACITY, col_count)
    rows = lax.all_to_all(buffer, "ep", split_axis=0, concat_axis=2, tiled=True)
    rows = norm_rows(rows, ffn_gain)
    gate_v = jnp.einsum("ecd,edf->ecf", rows, w_gate, preferred_element_type=jnp.float32)
    up_v = jnp.einsum("ecd,edf->ecf", rows, w_up, preferred_element_type=jnp.float32)
    activation = (jax.nn.silu(gate_v) * up_v).astype(jnp.bfloat16)
    partial_value = jnp.einsum(
        "ecf,efd->ecd", activation, w_down, preferred_element_type=jnp.float32
    )
    results = lax.psum(partial_value.astype(jnp.bfloat16), "tp")
    returned = lax.all_to_all(results, "ep", split_axis=2, concat_axis=0, tiled=True)
    picked = returned.reshape(expert_count * EXPERT_CAPACITY, col_count)[targets]
    picked = picked.reshape(route.shape[0], topk_count, col_count).astype(jnp.float32)
    weights = route_weight / jnp.sum(route_weight, axis=1, keepdims=True)
    mixed = (middle.astype(jnp.float32) + jnp.sum(picked * weights[:, :, None], axis=1)).astype(
        jnp.bfloat16
    )
    return (mixed, state[:, None], norm_state[:, None], new_max[:, None])


def solution(mesh):
    return jax.shard_map(
        shards,
        mesh=mesh,
        in_specs=(
            P("ep", None),
            P(),
            P(None, "tp"),
            P(None, "tp"),
            P(None, "tp"),
            P(None, "tp"),
            P(),
            P(),
            P(),
            P("tp"),
            P("tp", None),
            P("ep", "tp", None, None),
            P("ep", "tp", None),
            P("ep", "tp"),
            P(),
            P(),
            P(),
            P("ep", None, "tp"),
            P("ep", None, "tp"),
            P("ep", "tp", None),
        ),
        out_specs=(P(None, "ep"), P("ep", "tp", None, None), P("ep", "tp", None), P("ep", "tp")),
        check_vma=False,
    )
```

profile of v0, /device:TPU:0, one launch (start us, length us, event | category | flops | bytes accessed | tf_op | source)
XLA Modules:
  0.0 114.8 jit_solution(4171381798939121330)
XLA Ops:
  7.2 1.4 %fusion.48 = f32[]{:T(128)} fusion(f32[4]{0:T(128)} %param.28, s32[]{:T(128)S(6)} %axis_index.12), kind=kLoop, calls=%fused_computation.81 | loop fusion | flops 11 | bytes 24 | tf_op jit(solution)/shard_map/reduce_sum | solution.py:72
  8.7 0.8 fusion.28
  9.5 0.9 fusion.3
  10.4 0.9 fusion.2
  11.3 1.3 %fusion.46 = (f32[8]{0:T(128)S(1)}, f32[8]{0:T(128)S(1)}) fusion(f32[8]{0:T(128)S(1)} %fusion.3, f32[8,1]{0,1:T(1,128)} %param.33, f32[8]{0:T(128)S(1)} %fusion.2, f32[]{:T(128)} %fusion.48), kind=kLoop, calls=%fused_computation.79 | loop fusion | flops 96 | bytes 164 | tf_op jit(solution)/shard_map/exp | solution.py:75
  12.7 1.3 %exponential_bitcast_fusion = (f32[8]{0:T(128)S(1)}, f32[8,1]{0,1:T(1,128)S(1)}) fusion(f32[8]{0:T(128)S(1)} %fusion.3, f32[8,1]{0,1:T(1,128)} %param.33, f32[8]{0:T(128)S(1)} %fusion.2, f32[]{:T(128)} %fusion.48), kind=kLoop, calls=%fused_computation.104 | loop fusion | flops 96 | bytes 164 | tf_op jit(solution)/shard_map/mul | solution.py:81
  14.1 0.9 convolution_convert_fusion.5
  14.9 1.2 %convolution_convert_fusion.4 = bf16[8,128]{1,0:T(8,128)(2,1)S(1)} fusion(bf16[1024,128]{1,0:T(8,128)(2,1)} %param.23, bf16[8,1024]{1,0:T(8,128)(2,1)S(1)} %copy-done.3, f32[1024]{0:T(1024)} %param.21, f32[8]{0:T(128)S(1)} %add_rsqrt_fusion.2), kind=kOutput, calls=%fused_computation.9 | convolution fusion | flops 2130944 | bytes 284704 | tf_op jit(solution)/shard_map/dot_general | solution.py:59
  16.1 0.9 convolution_convert_fusion.2
  17.0 1.3 %convolution_convert_fusion.3 = bf16[8,256]{1,0:T(8,128)(2,1)S(1)} fusion(bf16[1024,256]{1,0:T(8,128)(2,1)} %param.25, bf16[8,1024]{1,0:T(8,128)(2,1)S(1)} %copy-done.3, f32[1024]{0:T(1024)} %param.21, f32[8]{0:T(128)S(1)} %add_rsqrt_fusion.2), kind=kOutput, calls=%fused_computation.8 | convolution fusion | flops 4229120 | bytes 548896 | tf_op jit(solution)/shard_map/dot_general | solution.py:62
  18.3 0.7 copy-done.10
  19.0 0.8 multiply_reduce_fusion.1
  19.8 0.6 fusion.5
  20.4 0.2 multiply_reduce_fusion
  20.6 0.7 copy-done.13
  21.3 0.2 convolution_convert_fusion.1
  21.5 12.7 %psum.14 = bf16[8,1024]{1,0:T(8,128)(2,1)S(1)} all-reduce(bf16[8,1024]{1,0:T(8,128)(2,1)S(1)} %convolution_convert_fusion.1), channel_id=1, replica_groups=mesh['ep'=8,'tp'=4] {'tp'}, use_global_device_ids=true, to_apply=%region_6.7 | all-reduce | flops 8192 | bytes 32768 | tf_op jit(solution)/shard_map/psum | solution.py:87
  34.2 0.6 fusion.34
  34.8 6.0 %all-to-all-start = ((bf16[8,8,128]{2,0,1:T(8,128)(2,1)}), bf16[8,8,128]{2,0,1:T(8,128)(2,1)S(1)}, u32[]{:S(2)}, u32[]{:S(2)}) async-start(bf16[8,8,128]{2,0,1:T(8,128)(2,1)} %fusion.34), calls=%async_computation | async-start | bytes 32768 | tf_op jit(solution)/shard_map/all_to_all | solution.py:91
  40.8 0.1 copy.48
  40.9 0.1 copy.47
  41.0 0.1 mul.253
  41.2 0.1 eq.27
  41.4 0.2 reduce_window_sum.11
  41.6 0.2 select_reduce_fusion
  41.8 5.6 %all-to-all-done = bf16[8,8,128]{2,0,1:T(8,128)(2,1)S(1)} async-done(((bf16[8,8,128]{2,0,1:T(8,128)(2,1)}), bf16[8,8,128]{2,0,1:T(8,128)(2,1)S(1)}, u32[]{:S(2)}, u32[]{:S(2)}) %all-to-all-start) | async-done | bytes 16416 | tf_op jit(solution)/shard_map/all_to_all | solution.py:91
  47.4 0.9 scatter_custom_fusion
  48.3 9.3 %all_to_all.43 = bf16[8,32,128]{2,1,0:T(8,128)(2,1)S(1)} all-to-all(bf16[8,32,128]{2,1,0:T(8,128)(2,1)S(1)} %bitcast.126), channel_id=1, replica_groups=mesh['ep'=8,'tp'=4] {'ep'}, dimensions={0} | all-to-all | bytes 131072 | tf_op jit(solution)/shard_map/all_to_all | solution.py:101
  57.6 0.1 fusion.16
  57.7 0.6 copy-done.7
  58.4 0.2 fusion.14
  58.6 0.6 copy-done.6
  59.2 0.1 copy-done.5
  59.3 0.9 fusion
  60.3 1.2 %multiply_add_fusion = f32[8,1,128,256]{3,2,1,0:T(8,128)} fusion(f32[8,1,128,256]{3,2,1,0:T(8,128)S(1)} %copy-done.1, f32[8,256]{1,0:T(8,128)S(1)} %convert_element_type.117, f32[8,128]{1,0:T(8,128)S(1)} %get-tuple-element.30, f32[8]{0:T(128)S(1)} %get-tuple-element.24), kind=kLoop, calls=%fused_computation.18 | loop fusion | flops 786432 | bytes 2109472 | tf_op jit(solution)/shard_map/add | solution.py:78
  61.5 27.0 %all-reduce.2.cloned.1.call-done = bf16[1,32,1024]{2,1,0:T(8,128)(2,1)} async-done(((bf16[1,32,1024]{2,1,0:T(8,128)(2,1)}), bf16[1,32,1024]{2,1,0:T(8,128)(2,1)}) %all-reduce.2.cloned.1.call-update) | async-done | bytes 65552 | tf_op jit(solution)/shard_map/psum | solution.py:109
  88.5 1.1 copy.50
  89.6 0.5 broadcast.215
  90.1 2.3 %reduce.3 = bf16[1024,32]{1,0:T(8,128)(2,1)S(1)} reduce(bf16[1024,1,32]{2,1,0:T(2,128)(2,1)S(1)} %bitcast.121, bf16[]{:T(256)} %broadcast.215), dimensions={1}, to_apply=%bitcast.105.reduce_sub_computation | reduce | bytes 131074
  92.4 0.9 reshape.303
  93.3 5.5 %all-to-all-start.2 = ((bf16[8,2,2048]{2,1,0:T(2,128)(2,1)}), bf16[8,2,2048]{2,1,0:T(2,128)(2,1)S(1)}, u32[]{:S(2)}, u32[]{:S(2)}) async-start(bf16[8,2,2048]{2,1,0:T(2,128)(2,1)} %reshape.303), calls=%async_computation.2 | async-start | bytes 131072 | tf_op jit(solution)/shard_map/all_to_all | solution.py:110
  98.8 0.1 copy.53
  99.0 6.8 %all-to-all-done.2 = bf16[8,2,2048]{2,1,0:T(2,128)(2,1)S(1)} async-done(((bf16[8,2,2048]{2,1,0:T(2,128)(2,1)}), bf16[8,2,2048]{2,1,0:T(2,128)(2,1)S(1)}, u32[]{:S(2)}, u32[]{:S(2)}) %all-to-all-start.2) | async-done | bytes 65568 | tf_op jit(solution)/shard_map/all_to_all | solution.py:110
  105.7 0.3 reshape.304
  106.1 0.3 copy.51
  106.4 0.7 gather_fusion
  107.2 0.1 fusion.23
  107.3 0.6 add_convert_fusion
  (45 shorter events, 0.5 us)
Async XLA Ops:
  7.2 13.5 %copy-start = (bf16[256,1024]{1,0:T(8,128)(2,1)S(1)}, bf16[256,1024]{1,0:T(8,128)(2,1)}, u32[]{:S(2)}) copy-start(bf16[256,1024]{1,0:T(8,128)(2,1)} %param.30) | copy-start | bytes 1572868
  7.2 2.3 %copy-start.3 = (bf16[8,1024]{1,0:T(8,128)(2,1)S(1)}, bf16[8,1024]{1,0:T(8,128)(2,1)}, u32[]{:S(2)}) copy-start(bf16[8,1024]{1,0:T(8,128)(2,1)} %param.20) | copy-start | bytes 49156
  7.2 6.8 %copy-start.12 = (bf16[1024,128]{1,0:T(8,128)(2,1)S(1)}, bf16[1024,128]{1,0:T(8,128)(2,1)}, u32[]{:S(2)}) copy-start(bf16[1024,128]{1,0:T(8,128)(2,1)} %param.22) | copy-start | bytes 786436
  7.2 8.9 %copy-start.2 = (bf16[1024,256]{1,0:T(8,128)(2,1)S(1)}, bf16[1024,256]{1,0:T(8,128)(2,1)}, u32[]{:S(2)}) copy-start(bf16[1024,256]{1,0:T(8,128)(2,1)} %param.24) | copy-start | bytes 1572868
  7.2 12.6 %copy-start.1 = (f32[8,1,128,256]{3,2,1,0:T(8,128)S(1)}, f32[8,1,128,256]{3,2,1,0:T(8,128)}, u32[]{:S(2)}) copy-start(f32[8,1,128,256]{3,2,1,0:T(8,128)} %param.31) | copy-start | bytes 3145732
  14.0 5.8 %copy-start.11 = (f32[8,1]{0,1:T(1,128)}, f32[8,1]{0,1:T(1,128)S(1)}, u32[]{:S(2)}) copy-start(f32[8,1]{0,1:T(1,128)S(1)} %get-tuple-element.29) | copy-start | bytes 100
  18.3 0.7 copy-start.10
  20.6 0.7 copy-start.13
  34.8 6.0 %copy-start.8 = (s32[64,2]{0,1:T(2,128)S(1)}, s32[64,2]{0,1:T(2,128)}, u32[]{:S(2)}) copy-start(s32[64,2]{0,1:T(2,128)} %param.35) | copy-start | bytes 1540
  34.8 12.5 %all-to-all-start = ((bf16[8,8,128]{2,0,1:T(8,128)(2,1)}), bf16[8,8,128]{2,0,1:T(8,128)(2,1)S(1)}, u32[]{:S(2)}, u32[]{:S(2)}) async-start(bf16[8,8,128]{2,0,1:T(8,128)(2,1)} %fusion.34), calls=%async_computation | async-start | bytes 32768 | tf_op jit(solution)/shard_map/all_to_all | solution.py:91
  40.8 47.7 %all-reduce.2.cloned.1.call-start = ((), (), s32[]{:S(2)}) async-start(), calls=%async_computation.3 | async-start | bytes 131072 | tf_op jit(solution)/shard_map/psum | solution.py:109
  47.4 11.0 %copy-start.4 = (bf16[1,1024,128]{2,1,0:T(8,128)(2,1)S(1)}, bf16[1,1024,128]{2,1,0:T(8,128)(2,1)}, u32[]{:S(2)}) copy-start(bf16[1,1024,128]{2,1,0:T(8,128)(2,1)} %param.37) | copy-start | bytes 786436
  57.6 0.7 copy-start.7
  58.3 0.9 copy-start.6
  58.4 1.0 copy-start.5
  60.3 1.2 %copy-start.9 = (f32[64,2]{0,1:T(2,128)S(1)}, f32[64,2]{0,1:T(2,128)}, u32[]{:S(2)}) copy-start(f32[64,2]{0,1:T(2,128)} %param.36) | copy-start | bytes 1540
  93.3 12.4 %all-to-all-start.2 = ((bf16[8,2,2048]{2,1,0:T(2,128)(2,1)}), bf16[8,2,2048]{2,1,0:T(2,128)(2,1)S(1)}, u32[]{:S(2)}, u32[]{:S(2)}) async-start(bf16[8,2,2048]{2,1,0:T(2,128)(2,1)} %reshape.303), calls=%async_computation.2 | async-start | bytes 131072 | tf_op jit(solution)/shard_map/all_to_all | solution.py:110
Sparse Core Ops, SparseCore 0:
  60.4 28.0 all-reduce.1
where the time goes:
time: 116 us; the launch traced here: 115 us
  waiting for transfers between devices  39.4 us (34%)
  blocking collectives  22 us (19%)
  between operations  14.3 us (12%)
  starting transfers between devices  11.5 us (10%)
  other arithmetic  11.4 us (10%)
  local copies, waits for them, and re-layouts  8.14 us (7%)
  matrix products  7.98 us (7%)
    psum x1, waiting for transfers between devices, shards(): results = lax.psum(partial_value.astype(jnp.bfloat16), 'tp')  27 us
    psum x1, blocking collectives, shards(): lax.psum(jnp.dot(gated, w_out, preferred_element_type=jnp.float32).astype...  12.7 us
    all_to_all x1, blocking collectives, shards(): rows = lax.all_to_all(buffer, 'ep', split_axis=0, concat_axis=2, tiled=True)  9.29 us
    all_to_all x1, waiting for transfers between devices, shards(): lax.all_to_all(results, 'ep', split_axis=2, concat_axis=0, tiled=True)  6.79 us
    all_to_all x1, starting transfers between devices, shards(): lax.all_to_all(middle_rows, 'ep', split_axis=1, concat_axis=0, tiled=True)  5.97 us
    all_to_all x1, waiting for transfers between devices, shards(): lax.all_to_all(middle_rows, 'ep', split_axis=1, concat_axis=0, tiled=True)  5.58 us
    all_to_all x1, starting transfers between devices, shards(): lax.all_to_all(results, 'ep', split_axis=2, concat_axis=0, tiled=True)  5.52 us
    unnamed x33, local copies, waits for them, and re-layouts  4.59 us
  transfers between devices with their start and end apart: 3, of which 3 were waited for; matrix products, arithmetic and copies ran while one was open for 2% of the time, Pallas kernels for 0%

commit v1 on v0

v1 whole, which is shorter than its diff:
```python
import functools

import jax
import jax.numpy as jnp
from jax import lax
from jax.experimental import pallas as pl
from jax.experimental.pallas import tpu as pltpu
from jax.sharding import PartitionSpec as P

EXPERT_CAPACITY = 32
EPS = 1e-06
LANES = 128
CHUNK_ROWS = 512

F32 = jnp.float32
BF16 = jnp.bfloat16


def iota(shape, dim):
    return lax.broadcasted_iota(jnp.int32, shape, dim)


def dot(a, b):
    return jnp.dot(a, b, preferred_element_type=F32)


def rounded(a, b):
    return dot(a, b).astype(BF16).astype(F32)


def norm_rows(floats, gain):
    scale = lax.rsqrt(jnp.mean(floats * floats, axis=-1, keepdims=True) + EPS)
    return (floats * scale * gain).astype(BF16)


def column_of(row, eye):
    return jnp.sum(jnp.where(eye, row, 0.0), axis=1, keepdims=True)


def row_of(column, eye):
    return jnp.sum(jnp.where(eye, column, 0.0), axis=0, keepdims=True)


def cell_kernel(
    head_ref, bias_ref, tokens_ref, mix_ref, wi_ref, wf_ref, hgain_ref, norm_ref, max_ref,
    wq_hbm, wk_hbm, wv_hbm, wo_hbm, mem_hbm, wout_hbm,
    part_ref, nstate_ref, nmax_ref, keep_ref, adk_ref, value_ref,
    wq, wk, wv, wo, mem, wout, sems,
):
    pairs = ((wq_hbm, wq), (wk_hbm, wk), (wv_hbm, wv), (wo_hbm, wo), (mem_hbm, mem), (wout_hbm, wout))
    copies = [pltpu.make_async_copy(src, dst, sems.at[i]) for i, (src, dst) in enumerate(pairs)]
    for copy in copies:
        copy.start()
    head = head_ref[0]
    rows = tokens_ref.shape[0]
    qk_dim = wq.shape[1]
    normed = norm_rows(tokens_ref[...].astype(F32), mix_ref[...])
    contract_last = (((1,), (1,)), ((), ()))
    pick = iota((rows, wi_ref.shape[0]), 1) == head
    gate_in = lax.dot_general(normed, wi_ref[...], contract_last, preferred_element_type=F32)
    gate_forget = lax.dot_general(normed, wf_ref[...], contract_last, preferred_element_type=F32)
    log_in = jnp.sum(jnp.where(pick, gate_in, 0.0), axis=1, keepdims=True)
    forget_pre = jnp.sum(jnp.where(pick, gate_forget, 0.0), axis=1, keepdims=True) + bias_ref[head]
    log_forget = jnp.minimum(forget_pre, 0.0) - jnp.log1p(jnp.exp(-jnp.abs(forget_pre)))
    eye = iota((rows, rows), 0) == iota((rows, rows), 1)
    carried = log_forget + column_of(max_ref[...], eye)
    new_max = jnp.maximum(carried, log_in)
    keep = jnp.exp(carried - new_max)
    admit = jnp.exp(log_in - new_max)
    nmax_ref[...] = row_of(new_max, eye)
    copies[0].wait()
    query = rounded(normed, wq[...])
    copies[1].wait()
    scaled_key = rounded(normed, wk[...]) * qk_dim ** (-0.5)
    admitted = admit * scaled_key
    norm_state = keep * norm_ref[...] + admitted
    nstate_ref[...] = norm_state
    adk_ref[...] = admitted
    keep_ref[...] = jnp.broadcast_to(keep, keep_ref.shape)
    denom = jnp.sum(query * norm_state, axis=1, keepdims=True)
    overlap = jnp.sum(query * admitted, axis=1, keepdims=True)
    query_cols = jnp.transpose(query)
    copies[2].wait()
    value = rounded(normed, wv[...])
    value_ref[...] = value
    copies[3].wait()
    ogate = rounded(normed, wo[...])
    copies[4].wait()
    reads = [
        jnp.sum(query_cols[:, t : t + 1] * mem[t], axis=0, keepdims=True) for t in range(rows)
    ]
    numer = keep * jnp.concatenate(reads, axis=0) + overlap * value
    read = numer / jnp.maximum(jnp.abs(denom), jnp.exp(-new_max))
    scale = lax.rsqrt(jnp.mean(read * read, axis=-1, keepdims=True) + EPS)
    gated = (jax.nn.sigmoid(ogate) * read * scale * hgain_ref[...]).astype(BF16)
    copies[5].wait()
    part_ref[...] = dot(gated, wout[...]).astype(BF16)


def state_kernel(keep_ref, adk_ref, value_ref, mem_ref, out_ref):
    block = mem_ref.shape[0]
    first = pl.program_id(0) * block
    rows = adk_ref.shape[0]
    adk_cols = jnp.transpose(adk_ref[...])
    for t in range(block):
        lane = iota(adk_cols.shape, 1) == first + t
        column = jnp.sum(jnp.where(lane, adk_cols, 0.0), axis=1, keepdims=True)
        keep = keep_ref[pl.ds(first + t, 1), :][:, 0:1]
        out_ref[t] = keep * mem_ref[t] + column * value_ref[pl.ds(first + t, 1), :]


def middle_kernel(*refs):
    tokens_ref, *parts, out_ref = refs
    total = parts[0][...].astype(F32)
    for part in parts[1:]:
        total = total + part[...].astype(F32)
    middle = (tokens_ref[...].astype(F32) + total).astype(BF16)
    for copy in range(out_ref.shape[0]):
        out_ref[copy] = middle


def earlier_matrix(count):
    return (iota((count, count), 0) < iota((count, count), 1)).astype(BF16)


def expert_kernel(
    place_ref, middle_ref, gain_ref, route_ref, weight_ref, wg_ref, wu_ref, wd_ref, own_ref, send_ref
):
    expert, half = place_ref[0], place_ref[1]
    count = middle_ref.shape[0]
    normed = norm_rows(middle_ref[...].astype(F32), gain_ref[...])
    route = route_ref[...]
    weight = weight_ref[...]
    named = route == expert
    share = jnp.where(named, weight, 0.0) / jnp.sum(weight, axis=0, keepdims=True)
    share = jnp.sum(share, axis=0, keepdims=True)
    member = jnp.sum(named.astype(F32), axis=0, keepdims=True)
    slot = dot(jnp.broadcast_to(member, (8, count)).astype(BF16), earlier_matrix(count))[0:1]
    shape = (EXPERT_CAPACITY, count)
    chosen = (iota(shape, 0).astype(F32) == slot) & (member > 0.5)
    rows = dot(chosen.astype(BF16), normed).astype(BF16)
    slot_share = jnp.sum(jnp.where(chosen, share, 0.0), axis=1, keepdims=True)
    gate = dot(rows, wg_ref[...])
    up = dot(rows, wu_ref[...])
    act = (jax.nn.silu(gate) * up).astype(BF16)
    result = (dot(act, wd_ref[...]) * slot_share).astype(BF16)
    part = own_ref.shape[0]
    low, high = result[:part], result[EXPERT_CAPACITY - part :]
    own_ref[...] = jnp.where(half == 0, low, high)
    send_ref[...] = jnp.where(half == 0, high, low)


def spread_kernel(own_ref, got_ref, out_ref):
    total = (own_ref[...].astype(F32) + got_ref[...].astype(F32)).astype(BF16)
    owners, copies, _, cols = out_ref.shape
    for owner in range(owners):
        piece = total[:, owner * cols : (owner + 1) * cols]
        for copy in range(copies):
            out_ref[owner, copy] = piece


def mix_kernel(middle_ref, route_ref, got_ref, out_ref, *, experts, sources, part):
    route = route_ref[...]
    count = route.shape[1]
    shape = (experts, count)
    member = jnp.zeros(shape, jnp.bool_)
    for choice in range(route.shape[0]):
        member = member | (iota(shape, 0) == route[choice : choice + 1])
    slots = dot(member.astype(BF16), earlier_matrix(count))
    slots = jnp.where(member, slots, -1.0).astype(BF16)
    total_rows = got_ref.shape[0]
    chunk = min(CHUNK_ROWS, total_rows)
    per_expert = sources * part

    def picked(start):
        column = iota((experts, chunk), 1) + start
        expand = (column // per_expert == iota((experts, chunk), 0)).astype(BF16)
        expanded = lax.dot_general(
            slots, expand, (((0,), (0,)), ((), ())), preferred_element_type=F32
        )
        column = iota((1, chunk), 1) + start
        source = (column // part) % sources
        groups = EXPERT_CAPACITY // part
        slot = (source % groups) * part + column % part
        pick = (expanded == slot.astype(F32)).astype(BF16)
        return dot(pick, got_ref[pl.ds(start, chunk), :])

    total = middle_ref[...].astype(F32)
    if total_rows == chunk:
        total = total + picked(0)
    else:
        total = lax.fori_loop(
            0, total_rows // chunk, lambda i, acc: acc + picked(i * chunk), total
        )
    out_ref[...] = total.astype(BF16)


def exchanged(values, axis):
    count = lax.axis_size(axis)
    if count & (count - 1) == 0:
        pairings = [[(i, i ^ k) for i in range(count)] for k in range(1, count)]
    else:
        pairings = [[(i, (i + k) % count) for i in range(count)] for k in range(1, count)]
    return [lax.ppermute(values, axis, pairing) for pairing in pairings]


def call(kernel, out_shape, in_specs, name, out_specs=None, **kw):
    vmem = pl.BlockSpec(memory_space=pltpu.VMEM)
    if out_specs is None:
        out_specs = jax.tree.map(lambda _: vmem, out_shape)
    return pl.pallas_call(
        kernel, out_shape=out_shape, in_specs=in_specs, out_specs=out_specs, name=name, **kw
    )


def shards(
    tokens, mix_gain, w_query, w_key, w_value, w_ogate, w_igate, w_fgate, forget_bias, head_gain,
    w_out, memory, normalizer, running_max, ffn_gain, route, route_weight, w_gate, w_up, w_down,
):
    vmem = pl.BlockSpec(memory_space=pltpu.VMEM)
    smem = pl.BlockSpec(memory_space=pltpu.SMEM)
    hbm = pl.BlockSpec(memory_space=pl.ANY)
    owners, heads = lax.axis_size("ep"), lax.axis_size("tp")
    rows, width = tokens.shape
    cols = width // owners
    count = route.shape[0]
    qk_dim, dv = w_query.shape[1], w_value.shape[1]
    head = lax.axis_index("tp")
    spec = jax.ShapeDtypeStruct

    partial, norm_state, new_max, keep, admitted, value = call(
        cell_kernel,
        (
            spec((rows, width), BF16),
            spec((rows, qk_dim), F32),
            spec((1, rows), F32),
            spec((rows, LANES), F32),
            spec((rows, qk_dim), F32),
            spec((rows, dv), F32),
        ),
        [smem, smem] + [vmem] * 7 + [hbm] * 6,
        "cell",
        scratch_shapes=[
            pltpu.VMEM(w_query.shape, BF16),
            pltpu.VMEM(w_key.shape, BF16),
            pltpu.VMEM(w_value.shape, BF16),
            pltpu.VMEM(w_ogate.shape, BF16),
            pltpu.VMEM((rows, qk_dim, dv), F32),
            pltpu.VMEM(w_out.shape, BF16),
            pltpu.SemaphoreType.DMA((6,)),
        ],
    )(
        head.reshape(1),
        forget_bias,
        tokens,
        mix_gain.reshape(1, -1),
        w_igate.T,
        w_fgate.T,
        head_gain.reshape(1, -1),
        normalizer.reshape(rows, qk_dim),
        running_max.T,
        w_query,
        w_key,
        w_value,
        w_ogate,
        memory.reshape(rows, qk_dim, dv),
        w_out,
    )

    block = 2 if rows % 2 == 0 else 1
    mem_spec = pl.BlockSpec((block, qk_dim, dv), lambda i: (i, 0, 0))
    whole = lambda shape: pl.BlockSpec(shape, lambda i: (0, 0))
    state = call(
        state_kernel,
        spec((rows, qk_dim, dv), F32),
        [whole(keep.shape), whole(admitted.shape), whole(value.shape), mem_spec],
        "state",
        out_specs=mem_spec,
        grid=(rows // block,),
        cost_estimate=pl.CostEstimate(flops=1 << 23, bytes_accessed=1 << 21, transcendentals=0),
    )(keep, admitted, value, memory.reshape(rows, qk_dim, dv))

    parts = exchanged(partial, "tp")
    spread = call(
        middle_kernel, spec((owners, rows, width), BF16), [vmem] * (2 + len(parts)), "middle"
    )(tokens, partial, *parts)
    middle = lax.all_to_all(spread, "ep", split_axis=0, concat_axis=0, tiled=True)
    middle = middle.reshape(count, width)
    place = lax.axis_index("ep")
    own_middle = lax.dynamic_slice_in_dim(middle, place * cols, cols, axis=1)

    groups = 2 if heads % 2 == 0 else 1
    part = EXPERT_CAPACITY // groups
    half = head % groups
    own, send = call(
        expert_kernel,
        (spec((part, width), BF16), spec((part, width), BF16)),
        [smem] + [vmem] * 7,
        "expert",
    )(
        jnp.stack([place, half]).astype(jnp.int32),
        middle,
        ffn_gain.reshape(1, -1),
        route.T,
        route_weight.T,
        w_gate[0],
        w_up[0],
        w_down[0],
    )
    if groups == 2:
        got = lax.ppermute(send, "tp", [(i, i ^ 1) for i in range(heads)])
    else:
        got = jnp.zeros_like(send)
    if cols % LANES == 0:
        pieces = call(
            spread_kernel, spec((owners, heads, part, cols), BF16), [vmem, vmem], "spread"
        )(own, got)
    else:
        total = (own.astype(F32) + got.astype(F32)).astype(BF16)
        total = total.reshape(part, owners, cols).transpose(1, 0, 2)
        pieces = jnp.broadcast_to(total[:, None], (owners, heads, part, cols))
    pieces = pieces.reshape(owners * heads, part, cols)
    results = lax.all_to_all(pieces, ("ep", "tp"), split_axis=0, concat_axis=0, tiled=True)
    mixed = call(
        functools.partial(mix_kernel, experts=owners, sources=heads, part=part),
        spec((count, cols), BF16),
        [vmem] * 3,
        "mix",
    )(own_middle, route.T, results.reshape(owners * heads * part, cols))
    return (
        mixed,
        state.reshape(memory.shape),
        norm_state.reshape(normalizer.shape),
        new_max.T,
    )


def solution(mesh):
    return jax.shard_map(
        shards,
        mesh=mesh,
        in_specs=(
            P("ep", None),
            P(),
            P(None, "tp"),
            P(None, "tp"),
            P(None, "tp"),
            P(None, "tp"),
            P(),
            P(),
            P(),
            P("tp"),
            P("tp", None),
            P("ep", "tp", None, None),
            P("ep", "tp", None),
            P("ep", "tp"),
            P(),
            P(),
            P(),
            P("ep", None, "tp"),
            P("ep", None, "tp"),
            P("ep", "tp", None),
        ),
        out_specs=(P(None, "ep"), P("ep", "tp", None, None), P("ep", "tp", None), P("ep", "tp")),
        check_vma=False,
    )
```

time: 116 us -> 47.3 us (0.41)
  waiting for transfers between devices: 39.4 us -> 14.5 us
  blocking collectives: 22 us -> 0 us
  Pallas kernels: 0 us -> 14.9 us
  between operations: 14.3 us -> 0.67 us
  other arithmetic: 11.4 us -> 0.67 us
  matrix products: 7.98 us -> 0 us
  local copies, waits for them, and re-layouts: 8.14 us -> 4.42 us
    psum x1 -> x0, waiting for transfers between devices: 27 us -> none  [shards(): results = lax.psum(partial_value.astype(jnp.bfloat16), 'tp')]
    pallas_call x0 -> x6, Pallas kernels: none -> 14.9 us  [the longest x1 3.85 us: shards(): call(cell_kernel, (spec((rows, width), BF16), spec((rows, qk_dim), F32),...]
    psum x1 -> x0, blocking collectives: 12.7 us -> none  [shards(): lax.psum(jnp.dot(gated, w_out, preferred_element_type=jnp.float32).astype...]
    all_to_all x1 -> x0, blocking collectives: 9.29 us -> none  [shards(): rows = lax.all_to_all(buffer, 'ep', split_axis=0, concat_axis=2, tiled=True)]
    dot_general x10 -> x0, matrix products: 7.98 us -> none  [the longest x1 1.28 us: shards(): jnp.dot(normed, w_ogate, preferred_element_type=jnp.float32)]
    ppermute x0 -> x4, waiting for transfers between devices: none -> 4.69 us  [the longest x3 3.27 us: exchanged(): return [lax.ppermute(values, axis, pairing) for pairing in pairings]]
    reduce_sum x8 -> x0, other arithmetic: 3.67 us -> none  [the longest x1 1.41 us: shards(): jnp.sum(forget_bias * head_pick)]
    ppermute x0 -> x4, starting transfers between devices: none -> 3.15 us  [the longest x3 3.15 us: exchanged(): return [lax.ppermute(values, axis, pairing) for pairing in pairings]]
  transfers between devices with their start and end apart: 3 -> 6, of which waited for: 3 -> 5; matrix products, arithmetic and copies ran while one was open for 2% -> 4% of each run, Pallas kernels for 0% -> 8%
where the time goes in v1:
time: 47.3 us; the launch traced here: 46.7 us
  Pallas kernels  14.9 us (32%)
  waiting for transfers between devices  14.5 us (31%)
  starting transfers between devices  11.5 us (24%)
  local copies, waits for them, and re-layouts  4.42 us (9%)
  other arithmetic  0.67 us (1%)
  between operations  0.67 us (1%)
    all_to_all x1, waiting for transfers between devices, shards(): lax.all_to_all(spread, 'ep', split_axis=0, concat_axis=0, tiled=True)  6.68 us
    all_to_all x1, starting transfers between devices, shards(): lax.all_to_all(spread, 'ep', split_axis=0, concat_axis=0, tiled=True)  5.83 us
    pallas_call x1, Pallas kernels, shards(): call(cell_kernel, (spec((rows, width), BF16), spec((rows, qk_dim), F32),...  3.85 us
    pallas_call x1, Pallas kernels, shards(): call(state_kernel, spec((rows, qk_dim, dv), F32), [whole(keep.shape), who...  3.75 us
    ppermute x3, waiting for transfers between devices, exchanged(): return [lax.ppermute(values, axis, pairing) for pairing in pairings]  3.27 us
    ppermute x3, starting transfers between devices, exchanged(): return [lax.ppermute(values, axis, pairing) for pairing in pairings]  3.15 us
    all_to_all x1, waiting for transfers between devices, shards(): lax.all_to_all(pieces, ('ep', 'tp'), split_axis=0, concat_axis=0, tiled=T...  3.14 us
    unnamed x12, local copies, waits for them, and re-layouts  3.11 us
  transfers between devices with their start and end apart: 6, of which 5 were waited for; matrix products, arithmetic and copies ran while one was open for 4% of the time, Pallas kernels for 8%

profile of v1, /device:TPU:0, one launch (start us, length us, event | category | flops | bytes accessed | tf_op | source)
XLA Modules:
  0.0 46.7 jit_solution(17559231103885810937)
XLA Ops:
  0.6 3.8 %cell.1 = (bf16[8,1024]{1,0:T(8,128)(2,1)}, f32[8,128]{1,0:T(8,128)}, f32[1,8]{1,0:T(1,128)}, f32[8,128]{1,0:T(8,128)}, f32[8,128]{1,0:T(8,128)}, /*index=5*/f32[8,256]{1,0:T(8,128)}) custom-call(s32[1]{0:T(128)} %bitcast.head_ref, f32[4]{0:T(128)} %bias_ref.1, bf16[8,1024]{1,0:T(8,128)(2,1)} %refs_0_.1, f32[1,1024]{1,0:T(1,128)} %bitcast.38, ...), custom_call_target="tpu_custom_call" | custom-call | tf_op jit(solution)/shard_map/cell/pallas_call | solution.py:231
  4.5 2.5 %collective-permute-start.2 = (bf16[8,1024]{1,0:T(8,128)(2,1)}, bf16[8,1024]{1,0:T(8,128)(2,1)S(1)}, u32[]{:S(2)}, u32[]{:S(2)}) collective-permute-start(bf16[8,1024]{1,0:T(8,128)(2,1)} %get-tuple-element.12.refs_1_), channel_id=1, source_target_pairs={{0,3},{1,2},{2,1},{3,0},{4,7},{5,6},{6,5},{7,4},{8,11},{9,10},{10,... | collective-permute-start | bytes 49160 | tf_op jit(solution)/shard_map/ppermute | solution.py:204
  7.0 0.6 %collective-permute-start.1 = (bf16[8,1024]{1,0:T(8,128)(2,1)}, bf16[8,1024]{1,0:T(8,128)(2,1)S(1)}, u32[]{:S(2)}, u32[]{:S(2)}) collective-permute-start(bf16[8,1024]{1,0:T(8,128)(2,1)} %get-tuple-element.12.refs_1_), channel_id=1, source_target_pairs={{0,2},{1,3},{2,0},{3,1},{4,6},{5,7},{6,4},{7,5},{8,10},{9,11},{10,... | collective-permute-start | bytes 49160 | tf_op jit(solution)/shard_map/ppermute | solution.py:204
  7.6 0.0 collective-permute-start
  7.6 1.0 %collective-permute-done.2.refs_4_ = bf16[8,1024]{1,0:T(8,128)(2,1)S(1)} collective-permute-done((bf16[8,1024]{1,0:T(8,128)(2,1)}, bf16[8,1024]{1,0:T(8,128)(2,1)S(1)}, u32[]{:S(2)}, u32[]{:S(2)}) %collective-permute-start.2) | collective-permute-done | bytes 16416 | tf_op jit(solution)/shard_map/ppermute | solution.py:204
  8.6 0.0 copy-start.3
  8.6 2.3 %collective-permute-done.1.refs_3_ = bf16[8,1024]{1,0:T(8,128)(2,1)S(1)} collective-permute-done((bf16[8,1024]{1,0:T(8,128)(2,1)}, bf16[8,1024]{1,0:T(8,128)(2,1)S(1)}, u32[]{:S(2)}, u32[]{:S(2)}) %collective-permute-start.1) | collective-permute-done | bytes 16416 | tf_op jit(solution)/shard_map/ppermute | solution.py:204
  10.9 0.0 copy-start.4
  10.9 0.0 collective-permute-done.refs_2_
  10.9 0.0 copy-done.3
  10.9 0.6 %copy-done.4 = bf16[8,1024]{1,0:T(8,128)(2,1)} copy-done((bf16[8,1024]{1,0:T(8,128)(2,1)}, bf16[8,1024]{1,0:T(8,128)(2,1)S(1)}, u32[]{:S(2)}) %copy-start.4) | copy-done | bytes 16408
  11.5 0.0 copy-start.5
  11.5 0.6 %copy-done.5 = bf16[8,1024]{1,0:T(8,128)(2,1)} copy-done((bf16[8,1024]{1,0:T(8,128)(2,1)}, bf16[8,1024]{1,0:T(8,128)(2,1)S(1)}, u32[]{:S(2)}) %copy-start.5) | copy-done | bytes 16408
  12.1 1.5 %middle.1 = bf16[8,8,1024]{2,1,0:T(8,128)(2,1)} custom-call(bf16[8,1024]{1,0:T(8,128)(2,1)} %refs_0_.1, bf16[8,1024]{1,0:T(8,128)(2,1)} %get-tuple-element.12.refs_1_, bf16[8,1024]{1,0:T(8,128)(2,1)} %copy-done.5, bf16[8,1024]{1,0:T(8,128)(2,1)} %copy-done.4, bf16[8,1024]{1,0:T(8,128)(2,1)} %copy-done.3), custom_call_target="tpu_custom_call" | custom-call | tf_op jit(solution)/shard_map/middle/pallas_call | solution.py:284
  13.6 5.8 %all-to-all-start = ((bf16[8,8,1024]{2,1,0:T(8,128)(2,1)}), bf16[8,8,1024]{2,1,0:T(8,128)(2,1)S(1)}, u32[]{:S(2)}, u32[]{:S(2)}) async-start(bf16[8,8,1024]{2,1,0:T(8,128)(2,1)} %middle.1), calls=%async_computation | async-start | bytes 262144 | tf_op jit(solution)/shard_map/all_to_all | solution.py:287
  19.4 0.7 %pad_add_fusion.place_ref = s32[2]{0:T(128)} fusion(s32[1]{0:T(128)} %bitcast.11, s32[1]{0:T(128)} %bitcast.10), kind=kLoop, calls=%fused_computation | loop fusion | flops 2 | bytes 16 | tf_op jit(solution)/shard_map/stack | solution.py:301
  20.1 6.7 %all-to-all-done = bf16[8,8,1024]{2,1,0:T(8,128)(2,1)S(1)} async-done(((bf16[8,8,1024]{2,1,0:T(8,128)(2,1)}), bf16[8,8,1024]{2,1,0:T(8,128)(2,1)S(1)}, u32[]{:S(2)}, u32[]{:S(2)}) %all-to-all-start) | async-done | bytes 131104 | tf_op jit(solution)/shard_map/all_to_all | solution.py:287
  26.7 0.0 copy-start
  26.7 0.7 %copy-done = bf16[8,8,1024]{2,1,0:T(8,128)(2,1)} copy-done((bf16[8,8,1024]{2,1,0:T(8,128)(2,1)}, bf16[8,8,1024]{2,1,0:T(8,128)(2,1)S(1)}, u32[]{:S(2)}) %copy-start) | copy-done | bytes 131096
  27.4 2.4 %expert.1 = (bf16[16,1024]{1,0:T(8,128)(2,1)}, bf16[16,1024]{1,0:T(8,128)(2,1)}) custom-call(s32[2]{0:T(128)} %pad_add_fusion.place_ref, bf16[64,1024]{1,0:T(8,128)(2,1)} %bitcast.29, f32[1,1024]{1,0:T(1,128)} %bitcast.40, s32[2,64]{1,0:T(2,128)} %bitcast.41, f32[2,64]{1,0:T(2,128)} %bitcast.44, bf16[1024,128]{1,0:T(8,128)(2,1)} %bitcast.33, ...), custom_call_target="tpu_custom_call" | custom-call | tf_op jit(solution)/shard_map/expert/pallas_call | solution.py:295
  29.8 0.0 collective-permute-start.3
  29.8 1.4 %collective-permute-done.3.got_ref = bf16[16,1024]{1,0:T(8,128)(2,1)S(1)} collective-permute-done((bf16[16,1024]{1,0:T(8,128)(2,1)}, bf16[16,1024]{1,0:T(8,128)(2,1)S(1)}, u32[]{:S(2)}, u32[]{:S(2)}) %collective-permute-start.3) | collective-permute-done | bytes 32800 | tf_op jit(solution)/shard_map/ppermute | solution.py:311
  31.3 0.0 copy-start.2
  31.3 0.6 %copy-done.2 = bf16[16,1024]{1,0:T(8,128)(2,1)} copy-done((bf16[16,1024]{1,0:T(8,128)(2,1)}, bf16[16,1024]{1,0:T(8,128)(2,1)S(1)}, u32[]{:S(2)}) %copy-start.2) | copy-done | bytes 32792
  31.9 1.4 %spread.1 = bf16[8,4,16,128]{3,2,1,0:T(8,128)(2,1)} custom-call(bf16[16,1024]{1,0:T(8,128)(2,1)} %get-tuple-element.13.own_ref, bf16[16,1024]{1,0:T(8,128)(2,1)} %copy-done.2), custom_call_target="tpu_custom_call" | custom-call | tf_op jit(solution)/shard_map/spread/pallas_call | solution.py:315
  33.3 2.6 %all-to-all-start.1 = ((bf16[32,16,128]{2,1,0:T(8,128)(2,1)}), bf16[32,16,128]{2,1,0:T(8,128)(2,1)S(1)}, u32[]{:S(2)}, u32[]{:S(2)}) async-start(bf16[32,16,128]{2,1,0:T(8,128)(2,1)} %bitcast.32), calls=%async_computation.1 | async-start | bytes 262144 | tf_op jit(solution)/shard_map/all_to_all | solution.py:323
  35.9 3.7 %state.1 = f32[8,128,256]{2,1,0:T(8,128)} custom-call(f32[8,128]{1,0:T(8,128)} %get-tuple-element.15.keep_ref, f32[8,128]{1,0:T(8,128)} %get-tuple-element.16.adk_ref, f32[8,256]{1,0:T(8,128)} %get-tuple-element.17.value_ref, f32[8,128,256]{2,1,0:T(8,128)} %bitcast.27), custom_call_target="tpu_custom_call" | custom-call | flops 8388608 | bytes 2097152 | tf_op jit(solution)/shard_map/state/pallas_call | solution.py:273
  39.6 1.3 %constant_dynamic-slice_fusion.middle_ref = bf16[64,128]{1,0:T(8,128)(2,1)} fusion(bf16[64,1024]{1,0:T(8,128)(2,1)} %bitcast.30, s32[]{:T(128)S(6)} %select_n.10), kind=kLoop, calls=%fused_computation.1 | loop fusion | bytes 32772 | tf_op jit(solution)/shard_map/dynamic_slice | solution.py:290
  40.9 3.1 %all-to-all-done.1 = bf16[32,16,128]{2,1,0:T(8,128)(2,1)S(1)} async-done(((bf16[32,16,128]{2,1,0:T(8,128)(2,1)}), bf16[32,16,128]{2,1,0:T(8,128)(2,1)S(1)}, u32[]{:S(2)}, u32[]{:S(2)}) %all-to-all-start.1) | async-done | bytes 131104 | tf_op jit(solution)/shard_map/all_to_all | solution.py:323
  44.1 0.0 copy-start.1
  44.1 0.7 %copy-done.1 = bf16[32,16,128]{2,1,0:T(8,128)(2,1)} copy-done((bf16[32,16,128]{2,1,0:T(8,128)(2,1)}, bf16[32,16,128]{2,1,0:T(8,128)(2,1)S(1)}, u32[]{:S(2)}) %copy-start.1) | copy-done | bytes 131096
  44.7 2.0 %mix.1 = bf16[64,128]{1,0:T(8,128)(2,1)} custom-call(bf16[64,128]{1,0:T(8,128)(2,1)} %constant_dynamic-slice_fusion.middle_ref, s32[2,64]{1,0:T(2,128)} %bitcast.42, bf16[512,128]{1,0:T(8,128)(2,1)} %bitcast.31), custom_call_target="tpu_custom_call" | custom-call | tf_op jit(solution)/shard_map/mix/pallas_call | solution.py:324
Async XLA Ops:
  4.5 4.1 %collective-permute-start.2 = (bf16[8,1024]{1,0:T(8,128)(2,1)}, bf16[8,1024]{1,0:T(8,128)(2,1)S(1)}, u32[]{:S(2)}, u32[]{:S(2)}) collective-permute-start(bf16[8,1024]{1,0:T(8,128)(2,1)} %get-tuple-element.12.refs_1_), channel_id=1, source_target_pairs={{0,3},{1,2},{2,1},{3,0},{4,7},{5,6},{6,5},{7,4},{8,11},{9,10},{10,... | collective-permute-start | bytes 49160 | tf_op jit(solution)/shard_map/ppermute | solution.py:204
  7.0 3.9 %collective-permute-start.1 = (bf16[8,1024]{1,0:T(8,128)(2,1)}, bf16[8,1024]{1,0:T(8,128)(2,1)S(1)}, u32[]{:S(2)}, u32[]{:S(2)}) collective-permute-start(bf16[8,1024]{1,0:T(8,128)(2,1)} %get-tuple-element.12.refs_1_), channel_id=1, source_target_pairs={{0,2},{1,3},{2,0},{3,1},{4,6},{5,7},{6,4},{7,5},{8,10},{9,11},{10,... | collective-permute-start | bytes 49160 | tf_op jit(solution)/shard_map/ppermute | solution.py:204
  7.6 3.3 %collective-permute-start = (bf16[8,1024]{1,0:T(8,128)(2,1)}, bf16[8,1024]{1,0:T(8,128)(2,1)S(1)}, u32[]{:S(2)}, u32[]{:S(2)}) collective-permute-start(bf16[8,1024]{1,0:T(8,128)(2,1)} %get-tuple-element.12.refs_1_), channel_id=1, source_target_pairs={{0,1},{1,0},{2,3},{3,2},{4,5},{5,4},{6,7},{7,6},{8,9},{9,8},{10,11... | collective-permute-start | bytes 49160 | tf_op jit(solution)/shard_map/ppermute | solution.py:204
  8.6 2.3 %copy-start.3 = (bf16[8,1024]{1,0:T(8,128)(2,1)}, bf16[8,1024]{1,0:T(8,128)(2,1)S(1)}, u32[]{:S(2)}) copy-start(bf16[8,1024]{1,0:T(8,128)(2,1)S(1)} %collective-permute-done.2.refs_4_) | copy-start | bytes 49156
  10.9 0.6 %copy-start.4 = (bf16[8,1024]{1,0:T(8,128)(2,1)}, bf16[8,1024]{1,0:T(8,128)(2,1)S(1)}, u32[]{:S(2)}) copy-start(bf16[8,1024]{1,0:T(8,128)(2,1)S(1)} %collective-permute-done.1.refs_3_) | copy-start | bytes 49156
  11.5 0.6 %copy-start.5 = (bf16[8,1024]{1,0:T(8,128)(2,1)}, bf16[8,1024]{1,0:T(8,128)(2,1)S(1)}, u32[]{:S(2)}) copy-start(bf16[8,1024]{1,0:T(8,128)(2,1)S(1)} %collective-permute-done.refs_2_) | copy-start | bytes 49156
  13.6 13.2 %all-to-all-start = ((bf16[8,8,1024]{2,1,0:T(8,128)(2,1)}), bf16[8,8,1024]{2,1,0:T(8,128)(2,1)S(1)}, u32[]{:S(2)}, u32[]{:S(2)}) async-start(bf16[8,8,1024]{2,1,0:T(8,128)(2,1)} %middle.1), calls=%async_computation | async-start | bytes 262144 | tf_op jit(solution)/shard_map/all_to_all | solution.py:287
  26.7 0.7 %copy-start = (bf16[8,8,1024]{2,1,0:T(8,128)(2,1)}, bf16[8,8,1024]{2,1,0:T(8,128)(2,1)S(1)}, u32[]{:S(2)}) copy-start(bf16[8,8,1024]{2,1,0:T(8,128)(2,1)S(1)} %all-to-all-done) | copy-start | bytes 393220
  29.8 1.4 %collective-permute-start.3 = (bf16[16,1024]{1,0:T(8,128)(2,1)}, bf16[16,1024]{1,0:T(8,128)(2,1)S(1)}, u32[]{:S(2)}, u32[]{:S(2)}) collective-permute-start(bf16[16,1024]{1,0:T(8,128)(2,1)} %get-tuple-element.14), channel_id=1, source_target_pairs={{0,1},{1,0},{2,3},{3,2},{4,5},{5,4},{6,7},{7,6},{8,9},{9,8},{10,11... | collective-permute-start | bytes 98312 | tf_op jit(solution)/shard_map/ppermute | solution.py:311
  31.3 0.6 %copy-start.2 = (bf16[16,1024]{1,0:T(8,128)(2,1)}, bf16[16,1024]{1,0:T(8,128)(2,1)S(1)}, u32[]{:S(2)}) copy-start(bf16[16,1024]{1,0:T(8,128)(2,1)S(1)} %collective-permute-done.3.got_ref) | copy-start | bytes 98308
  33.3 10.8 %all-to-all-start.1 = ((bf16[32,16,128]{2,1,0:T(8,128)(2,1)}), bf16[32,16,128]{2,1,0:T(8,128)(2,1)S(1)}, u32[]{:S(2)}, u32[]{:S(2)}) async-start(bf16[32,16,128]{2,1,0:T(8,128)(2,1)} %bitcast.32), calls=%async_computation.1 | async-start | bytes 262144 | tf_op jit(solution)/shard_map/all_to_all | solution.py:323
  44.1 0.7 %copy-start.1 = (bf16[32,16,128]{2,1,0:T(8,128)(2,1)}, bf16[32,16,128]{2,1,0:T(8,128)(2,1)S(1)}, u32[]{:S(2)}) copy-start(bf16[32,16,128]{2,1,0:T(8,128)(2,1)S(1)} %all-to-all-done.1) | copy-start | bytes 393220

commit v2 on v1

--- a/solution.py
+++ b/solution.py
@@ -11,6 +11,7 @@
 EPS = 1e-06
 LANES = 128
 CHUNK_ROWS = 512
+VMEM_LIMIT = 32 << 20
 
 F32 = jnp.float32
 BF16 = jnp.bfloat16
@@ -123,27 +124,67 @@
     return (iota((count, count), 0) < iota((count, count), 1)).astype(BF16)
 
 
-def expert_kernel(
-    place_ref, middle_ref, gain_ref, route_ref, weight_ref, wg_ref, wu_ref, wd_ref, own_ref, send_ref
+def plan_kernel(
+    place_ref, gain_ref, route_ref, weight_ref, chosen_ref, share_ref, gain_out_ref, *pick_refs,
+    experts, sources, part,
 ):
-    expert, half = place_ref[0], place_ref[1]
-    count = middle_ref.shape[0]
-    normed = norm_rows(middle_ref[...].astype(F32), gain_ref[...])
     route = route_ref[...]
     weight = weight_ref[...]
-    named = route == expert
+    count = route.shape[1]
+    earlier = earlier_matrix(count)
+    named = route == place_ref[0]
     share = jnp.where(named, weight, 0.0) / jnp.sum(weight, axis=0, keepdims=True)
     share = jnp.sum(share, axis=0, keepdims=True)
     member = jnp.sum(named.astype(F32), axis=0, keepdims=True)
-    slot = dot(jnp.broadcast_to(member, (8, count)).astype(BF16), earlier_matrix(count))[0:1]
+    slot = dot(jnp.broadcast_to(member, (8, count)).astype(BF16), earlier)[0:1]
     shape = (EXPERT_CAPACITY, count)
     chosen = (iota(shape, 0).astype(F32) == slot) & (member > 0.5)
-    rows = dot(chosen.astype(BF16), normed).astype(BF16)
+    chosen_ref[...] = chosen.astype(BF16)
     slot_share = jnp.sum(jnp.where(chosen, share, 0.0), axis=1, keepdims=True)
+    share_ref[...] = jnp.broadcast_to(slot_share, share_ref.shape)
+    gain_out_ref[...] = gain_ref[...]
+    for pick_ref in pick_refs:
+        slots = slot_table(route, experts)
+        pick_ref[...] = pick_matrix(slots, 0, pick_ref.shape[1], sources, part)
+
+
+def slot_table(route, experts):
+    count = route.shape[1]
+    shape = (experts, count)
+    member = jnp.zeros(shape, jnp.bool_)
+    for choice in range(route.shape[0]):
+        member = member | (iota(shape, 0) == route[choice : choice + 1])
+    slots = dot(member.astype(BF16), earlier_matrix(count))
+    return jnp.where(member, slots, -1.0).astype(BF16)
+
+
+def pick_matrix(slots, start, size, sources, part):
+    experts = slots.shape[0]
+    column = iota((experts, size), 1) + start
+    expand = (column // (sources * part) == iota((experts, size), 0)).astype(BF16)
+    expanded = lax.dot_general(
+        slots, expand, (((0,), (0,)), ((), ())), preferred_element_type=F32
+    )
+    column = iota((1, size), 1) + start
+    source = (column // part) % sources
+    slot = (source % (EXPERT_CAPACITY // part)) * part + column % part
+    return (expanded == slot.astype(F32)).astype(BF16)
+
+
+def expert_kernel(
+    place_ref, middle_ref, gain_ref, chosen_ref, share_ref, wg_ref, wu_ref, wd_ref,
+    own_ref, send_ref, *block_refs,
+):
+    expert, half = place_ref[0], place_ref[1]
+    for block_ref in block_refs:
+        cols = block_ref.shape[1]
+        block_ref[...] = middle_ref[:, pl.ds(pl.multiple_of(expert * cols, cols), cols)]
+    normed = norm_rows(middle_ref[...].astype(F32), gain_ref[...])
+    rows = dot(chosen_ref[...], normed).astype(BF16)
     gate = dot(rows, wg_ref[...])
     up = dot(rows, wu_ref[...])
     act = (jax.nn.silu(gate) * up).astype(BF16)
-    result = (dot(act, wd_ref[...]) * slot_share).astype(BF16)
+    result = (dot(act, wd_ref[...]) * share_ref[:, 0:1]).astype(BF16)
     part = own_ref.shape[0]
     low, high = result[:part], result[EXPERT_CAPACITY - part :]
     own_ref[...] = jnp.where(half == 0, low, high)
@@ -159,39 +200,21 @@
             out_ref[owner, copy] = piece
 
 
-def mix_kernel(middle_ref, route_ref, got_ref, out_ref, *, experts, sources, part):
-    route = route_ref[...]
-    count = route.shape[1]
-    shape = (experts, count)
-    member = jnp.zeros(shape, jnp.bool_)
-    for choice in range(route.shape[0]):
-        member = member | (iota(shape, 0) == route[choice : choice + 1])
-    slots = dot(member.astype(BF16), earlier_matrix(count))
-    slots = jnp.where(member, slots, -1.0).astype(BF16)
-    total_rows = got_ref.shape[0]
-    chunk = min(CHUNK_ROWS, total_rows)
-    per_expert = sources * part
-
-    def picked(start):
-        column = iota((experts, chunk), 1) + start
-        expand = (column // per_expert == iota((experts, chunk), 0)).astype(BF16)
-        expanded = lax.dot_general(
-            slots, expand, (((0,), (0,)), ((), ())), preferred_element_type=F32
-        )
-        column = iota((1, chunk), 1) + start
-        source = (column // part) % sources
-        groups = EXPERT_CAPACITY // part
-        slot = (source % groups) * part + column % part
-        pick = (expanded == slot.astype(F32)).astype(BF16)
-        return dot(pick, got_ref[pl.ds(start, chunk), :])
-
-    total = middle_ref[...].astype(F32)
-    if total_rows == chunk:
-        total = total + picked(0)
-    else:
-        total = lax.fori_loop(
-            0, total_rows // chunk, lambda i, acc: acc + picked(i * chunk), total
-        )
+def mix_kernel(middle_ref, pick_ref, got_ref, out_ref):
+    total = middle_ref[...].astype(F32) + dot(pick_ref[...], got_ref[...])
+    out_ref[...] = total.astype(BF16)
+
+
+def long_mix_kernel(middle_ref, route_ref, got_ref, out_ref, *, experts, sources, part):
+    slots = slot_table(route_ref[...], experts)
+
+    def add(step, total):
+        start = step * CHUNK_ROWS
+        pick = pick_matrix(slots, start, CHUNK_ROWS, sources, part)
+        return total + dot(pick, got_ref[pl.ds(start, CHUNK_ROWS), :])
+
+    steps = got_ref.shape[0] // CHUNK_ROWS
+    total = lax.fori_loop(0, steps, add, middle_ref[...].astype(F32))
     out_ref[...] = total.astype(BF16)
 
 
@@ -204,12 +227,26 @@
     return [lax.ppermute(values, axis, pairing) for pairing in pairings]
 
 
+def near(values):
+    return pltpu.with_memory_space_constraint(values, pltpu.VMEM)
+
+
+def far(values):
+    return pltpu.with_memory_space_constraint(values, pltpu.HBM)
+
+
 def call(kernel, out_shape, in_specs, name, out_specs=None, **kw):
-    vmem = pl.BlockSpec(memory_space=pltpu.VMEM)
     if out_specs is None:
-        out_specs = jax.tree.map(lambda _: vmem, out_shape)
+        vmem = pl.BlockSpec(memory_space=pltpu.VMEM)
+        out_specs = [vmem] * len(out_shape) if isinstance(out_shape, tuple) else vmem
     return pl.pallas_call(
-        kernel, out_shape=out_shape, in_specs=in_specs, out_specs=out_specs, name=name, **kw
+        kernel,
+        out_shape=out_shape,
+        in_specs=in_specs,
+        out_specs=out_specs,
+        name=name,
+        compiler_params=pltpu.CompilerParams(vmem_limit_bytes=VMEM_LIMIT),
+        **kw,
     )
 
 
@@ -231,12 +268,12 @@
     partial, norm_state, new_max, keep, admitted, value = call(
         cell_kernel,
         (
-            spec((rows, width), BF16),
+            pltpu.VMEM((rows, width), BF16),
             spec((rows, qk_dim), F32),
             spec((1, rows), F32),
-            spec((rows, LANES), F32),
-            spec((rows, qk_dim), F32),
-            spec((rows, dv), F32),
+            pltpu.VMEM((rows, LANES), F32),
+            pltpu.VMEM((rows, qk_dim), F32),
+            pltpu.VMEM((rows, dv), F32),
         ),
         [smem, smem] + [vmem] * 7 + [hbm] * 6,
         "cell",
@@ -252,19 +289,19 @@
     )(
         head.reshape(1),
         forget_bias,
-        tokens,
-        mix_gain.reshape(1, -1),
-        w_igate.T,
-        w_fgate.T,
-        head_gain.reshape(1, -1),
-        normalizer.reshape(rows, qk_dim),
-        running_max.T,
-        w_query,
-        w_key,
-        w_value,
-        w_ogate,
-        memory.reshape(rows, qk_dim, dv),
-        w_out,
+        far(tokens),
+        far(mix_gain.reshape(1, -1)),
+        far(w_igate.T),
+        far(w_fgate.T),
+        far(head_gain.reshape(1, -1)),
+        far(normalizer.reshape(rows, qk_dim)),
+        far(running_max.T),
+        far(w_query),
+        far(w_key),
+        far(w_value),
+        far(w_ogate),
+        far(memory.reshape(rows, qk_dim, dv)),
+        far(w_out),
     )
 
     block = 2 if rows % 2 == 0 else 1
@@ -278,55 +315,79 @@
         out_specs=mem_spec,
         grid=(rows // block,),
         cost_estimate=pl.CostEstimate(flops=1 << 23, bytes_accessed=1 << 21, transcendentals=0),
-    )(keep, admitted, value, memory.reshape(rows, qk_dim, dv))
+    )(near(keep), near(admitted), near(value), far(memory.reshape(rows, qk_dim, dv)))
 
     parts = exchanged(partial, "tp")
     spread = call(
-        middle_kernel, spec((owners, rows, width), BF16), [vmem] * (2 + len(parts)), "middle"
-    )(tokens, partial, *parts)
+        middle_kernel, pltpu.VMEM((owners, rows, width), BF16), [vmem] * (2 + len(parts)), "middle"
+    )(near(tokens), near(partial), *map(near, parts))
     middle = lax.all_to_all(spread, "ep", split_axis=0, concat_axis=0, tiled=True)
     middle = middle.reshape(count, width)
     place = lax.axis_index("ep")
-    own_middle = lax.dynamic_slice_in_dim(middle, place * cols, cols, axis=1)
-
     groups = 2 if heads % 2 == 0 else 1
     part = EXPERT_CAPACITY // groups
-    half = head % groups
-    own, send = call(
+    half = lax.bitwise_and(head, groups - 1)
+    places = jnp.stack([place, half]).astype(jnp.int32)
+    got_rows = owners * heads * part
+    short = got_rows <= CHUNK_ROWS
+    aligned = cols % LANES == 0
+    sizes = dict(experts=owners, sources=heads, part=part)
+    chosen, share, gain, *pick = call(
+        functools.partial(plan_kernel, **sizes),
+        (
+            pltpu.VMEM((EXPERT_CAPACITY, count), BF16),
+            pltpu.VMEM((EXPERT_CAPACITY, LANES), F32),
+            pltpu.VMEM((1, width), F32),
+        )
+        + ((pltpu.VMEM((count, got_rows), BF16),) if short else ()),
+        [smem] + [vmem] * 3,
+        "plan",
+        cost_estimate=pl.CostEstimate(flops=1 << 22, bytes_accessed=1 << 16, transcendentals=0),
+    )(places, far(ffn_gain.reshape(1, -1)), far(route.T), far(route_weight.T))
+    own, send, *own_middle = call(
         expert_kernel,
-        (spec((part, width), BF16), spec((part, width), BF16)),
+        (pltpu.VMEM((part, width), BF16), pltpu.VMEM((part, width), BF16))
+        + ((pltpu.VMEM((count, cols), BF16),) if aligned else ()),
         [smem] + [vmem] * 7,
         "expert",
     )(
-        jnp.stack([place, half]).astype(jnp.int32),
-        middle,
-        ffn_gain.reshape(1, -1),
-        route.T,
-        route_weight.T,
-        w_gate[0],
-        w_up[0],
-        w_down[0],
-    )
+        places,
+        near(middle),
+        near(gain),
+        near(chosen),
+        near(share),
+        near(w_gate[0]),
+        near(w_up[0]),
+        near(w_down[0]),
+    )
+    if not aligned:
+        own_middle = [lax.dynamic_slice_in_dim(middle, place * cols, cols, axis=1)]
     if groups == 2:
         got = lax.ppermute(send, "tp", [(i, i ^ 1) for i in range(heads)])
     else:
         got = jnp.zeros_like(send)
-    if cols % LANES == 0:
+    if aligned:
         pieces = call(
-            spread_kernel, spec((owners, heads, part, cols), BF16), [vmem, vmem], "spread"
-        )(own, got)
+            spread_kernel, pltpu.VMEM((owners, heads, part, cols), BF16), [vmem, vmem], "spread"
+        )(near(own), near(got))
     else:
         total = (own.astype(F32) + got.astype(F32)).astype(BF16)
         total = total.reshape(part, owners, cols).transpose(1, 0, 2)
         pieces = jnp.broadcast_to(total[:, None], (owners, heads, part, cols))
     pieces = pieces.reshape(owners * heads, part, cols)
     results = lax.all_to_all(pieces, ("ep", "tp"), split_axis=0, concat_axis=0, tiled=True)
-    mixed = call(
-        functools.partial(mix_kernel, experts=owners, sources=heads, part=part),
-        spec((count, cols), BF16),
-        [vmem] * 3,
-        "mix",
-    )(own_middle, route.T, results.reshape(owners * heads * part, cols))
+    results = near(results.reshape(got_rows, cols))
+    if short:
+        mixed = call(mix_kernel, spec((count, cols), BF16), [vmem] * 3, "mix")(
+            near(own_middle[0]), near(pick[0]), results
+        )
+    else:
+        mixed = call(
+            functools.partial(long_mix_kernel, **sizes),
+            spec((count, cols), BF16),
+            [vmem] * 3,
+            "mix",
+        )(own_middle[0], route.T, results)
     return (
         mixed,
         state.reshape(memory.shape),

time: 47.3 us -> 40.1 us (0.85)
  local copies, waits for them, and re-layouts: 4.42 us -> 0.67 us
  Pallas kernels: 14.9 us -> 11.7 us
  other arithmetic: 0.67 us -> 0.07 us
    pallas_call x5 -> x6, Pallas kernels: 11.2 us -> 7.97 us  [the longest x1 3.68 us: shards(): call(cell_kernel, (pltpu.VMEM((rows, width), BF16), spec((rows, qk_dim),...]
    unnamed x12 -> x10, local copies, waits for them, and re-layouts: 3.11 us -> 0.67 us
    all_to_all x1, waiting for transfers between devices: 3.14 us -> 4.46 us  [shards(): lax.all_to_all(pieces, ('ep', 'tp'), split_axis=0, concat_axis=0, tiled=T...]
    dynamic_slice x1 -> x0, local copies, waits for them, and re-layouts: 1.31 us -> none  [shards(): own_middle = lax.dynamic_slice_in_dim(middle, place * cols, cols, axis=1)]
    another operation x1, other arithmetic: 0.67 us -> 0.07 us  [shards(): places = jnp.stack([place, half]).astype(jnp.int32)]
  transfers between devices with their start and end apart: 6 -> 6, of which waited for: 5 -> 5; matrix products, arithmetic and copies ran while one was open for 4% -> 0% of each run, Pallas kernels for 8% -> 12%
where the time goes in v2:
time: 40.1 us; the launch traced here: 39.7 us
  waiting for transfers between devices  14.9 us (37%)
  Pallas kernels  11.7 us (29%)
  starting transfers between devices  11.6 us (29%)
  between operations  0.71 us (2%)
  local copies, waits for them, and re-layouts  0.67 us (2%)
    all_to_all x1, waiting for transfers between devices, shards(): lax.all_to_all(spread, 'ep', split_axis=0, concat_axis=0, tiled=True)  6.23 us
    all_to_all x1, starting transfers between devices, shards(): lax.all_to_all(spread, 'ep', split_axis=0, concat_axis=0, tiled=True)  5.83 us
    all_to_all x1, waiting for transfers between devices, shards(): lax.all_to_all(pieces, ('ep', 'tp'), split_axis=0, concat_axis=0, tiled=T...  4.46 us
    pallas_call x1, Pallas kernels, shards(): call(state_kernel, spec((rows, qk_dim, dv), F32), [whole(keep.shape), who...  3.74 us
    pallas_call x1, Pallas kernels, shards(): call(cell_kernel, (pltpu.VMEM((rows, width), BF16), spec((rows, qk_dim),...  3.68 us
    ppermute x3, starting transfers between devices, exchanged(): return [lax.ppermute(values, axis, pairing) for pairing in pairings]  3.15 us
    ppermute x3, waiting for transfers between devices, exchanged(): return [lax.ppermute(values, axis, pairing) for pairing in pairings]  3.06 us
    all_to_all x1, starting transfers between devices, shards(): lax.all_to_all(pieces, ('ep', 'tp'), split_axis=0, concat_axis=0, tiled=T...  2.56 us
  transfers between devices with their start and end apart: 6, of which 5 were waited for; matrix products, arithmetic and copies ran while one was open for 0% of the time, Pallas kernels for 12%

profile of v2, /device:TPU:0, one launch (start us, length us, event | category | flops | bytes accessed | tf_op | source)
XLA Modules:
  0.0 39.7 jit_solution(9877289195795487062)
XLA Ops:
  0.6 0.0 copy-start.4
  0.6 0.6 %copy-done.4 = f32[4]{0:T(128)S(1)} copy-done((f32[4]{0:T(128)S(1)}, f32[4]{0:T(128)}, u32[]{:S(2)}) %copy-start.4) | copy-done | bytes 40
  1.3 0.0 copy-start.3
  1.3 0.0 copy-start.2
  1.3 3.7 %cell.1 = (bf16[8,1024]{1,0:T(8,128)(2,1)S(1)}, f32[8,128]{1,0:T(8,128)}, f32[1,8]{1,0:T(1,128)}, f32[8,128]{1,0:T(8,128)S(1)}, f32[8,128]{1,0:T(8,128)S(1)}, /*index=5*/f32[8,256]{1,0:T(8,128)S(1)}) custom-call(s32[1]{0:T(128)} %bitcast.2.head_ref, f32[4]{0:T(128)S(1)} %copy-done.4, bf16[8,1024]{1,0:T(8,128)(2,1)} %refs_0_.1, f32[1,1024]{1,0:T(1,128)} %bitcast.36, ...), custom_call_target="tpu_custom_call" | custom-call | tf_op jit(solution)/shard_map/cell/pallas_call | solution.py:268
  5.0 0.0 copy-start.1
  5.0 0.0 copy-start
  5.0 2.5 %collective-permute-start.2 = (bf16[8,1024]{1,0:T(8,128)(2,1)S(1)}, bf16[8,1024]{1,0:T(8,128)(2,1)S(1)}, u32[]{:S(2)}, u32[]{:S(2)}) collective-permute-start(bf16[8,1024]{1,0:T(8,128)(2,1)S(1)} %get-tuple-element.17.refs_1_), channel_id=1, source_target_pairs={{0,3},{1,2},{2,1},{3,0},{4,7},{5,6},{6,5},{7,4},{8,11},{9,10},{10,... | collective-permute-start | bytes 49160 | tf_op jit(solution)/shard_map/ppermute | solution.py:227
  7.5 0.6 %collective-permute-start.1 = (bf16[8,1024]{1,0:T(8,128)(2,1)S(1)}, bf16[8,1024]{1,0:T(8,128)(2,1)S(1)}, u32[]{:S(2)}, u32[]{:S(2)}) collective-permute-start(bf16[8,1024]{1,0:T(8,128)(2,1)S(1)} %get-tuple-element.17.refs_1_), channel_id=1, source_target_pairs={{0,2},{1,3},{2,0},{3,1},{4,6},{5,7},{6,4},{7,5},{8,10},{9,11},{10,... | collective-permute-start | bytes 49160 | tf_op jit(solution)/shard_map/ppermute | solution.py:227
  8.1 0.0 collective-permute-start
  8.2 0.8 %collective-permute-done.2.refs_4_ = bf16[8,1024]{1,0:T(8,128)(2,1)S(1)} collective-permute-done((bf16[8,1024]{1,0:T(8,128)(2,1)S(1)}, bf16[8,1024]{1,0:T(8,128)(2,1)S(1)}, u32[]{:S(2)}, u32[]{:S(2)}) %collective-permute-start.2) | collective-permute-done | bytes 16416 | tf_op jit(solution)/shard_map/ppermute | solution.py:227
  8.9 2.3 %collective-permute-done.1.refs_3_ = bf16[8,1024]{1,0:T(8,128)(2,1)S(1)} collective-permute-done((bf16[8,1024]{1,0:T(8,128)(2,1)S(1)}, bf16[8,1024]{1,0:T(8,128)(2,1)S(1)}, u32[]{:S(2)}, u32[]{:S(2)}) %collective-permute-start.1) | collective-permute-done | bytes 16416 | tf_op jit(solution)/shard_map/ppermute | solution.py:227
  11.2 0.0 collective-permute-done.refs_2_
  11.2 0.0 copy-done.3
  11.2 0.7 %middle.1 = bf16[8,8,1024]{2,1,0:T(8,128)(2,1)} custom-call(bf16[8,1024]{1,0:T(8,128)(2,1)S(1)} %copy-done.3, bf16[8,1024]{1,0:T(8,128)(2,1)S(1)} %get-tuple-element.17.refs_1_, bf16[8,1024]{1,0:T(8,128)(2,1)S(1)} %collective-permute-done.refs_2_, bf16[8,1024]{1,0:T(8,128)(2,1)S(1)} %collective-permute-done.1.refs_3_, ...), custom_call_target="tpu_custom_call" | custom-call | tf_op jit(solution)/shard_map/middle/pallas_call | solution.py:321
  11.9 5.8 %all-to-all-start = ((bf16[8,8,1024]{2,1,0:T(8,128)(2,1)}), bf16[8,8,1024]{2,1,0:T(8,128)(2,1)S(1)}, u32[]{:S(2)}, u32[]{:S(2)}) async-start(bf16[8,8,1024]{2,1,0:T(8,128)(2,1)} %middle.1), calls=%async_computation | async-start | bytes 262144 | tf_op jit(solution)/shard_map/all_to_all | solution.py:324
  17.7 0.1 pad_add_fusion.place_ref
  17.8 1.0 %plan.1 = (bf16[32,64]{1,0:T(8,128)(2,1)S(1)}, f32[32,128]{1,0:T(8,128)S(1)}, f32[1,1024]{1,0:T(1,128)S(1)}, bf16[64,512]{1,0:T(8,128)(2,1)S(1)}) custom-call(s32[2]{0:T(128)S(1)} %pad_add_fusion.place_ref, f32[1,1024]{1,0:T(1,128)} %bitcast.40, s32[2,64]{1,0:T(2,128)} %bitcast.42, f32[2,64]{1,0:T(2,128)} %bitcast.43), custom_call_target="tpu_custom_call" | custom-call | flops 4194304 | bytes 65536 | tf_op jit(solution)/shard_map/plan/pallas_call | solution.py:335
  18.8 6.2 %all-to-all-done = bf16[8,8,1024]{2,1,0:T(8,128)(2,1)S(1)} async-done(((bf16[8,8,1024]{2,1,0:T(8,128)(2,1)}), bf16[8,8,1024]{2,1,0:T(8,128)(2,1)S(1)}, u32[]{:S(2)}, u32[]{:S(2)}) %all-to-all-start) | async-done | bytes 131104 | tf_op jit(solution)/shard_map/all_to_all | solution.py:324
  25.1 0.0 copy-done.2
  25.1 0.0 copy-done.1
  25.1 0.0 copy-done
  25.1 1.1 %expert.1 = (bf16[16,1024]{1,0:T(8,128)(2,1)S(1)}, bf16[16,1024]{1,0:T(8,128)(2,1)S(1)}, bf16[64,128]{1,0:T(8,128)(2,1)S(1)}) custom-call(s32[2]{0:T(128)S(1)} %pad_add_fusion.place_ref, bf16[64,1024]{1,0:T(8,128)(2,1)S(1)} %bitcast.26, f32[1,1024]{1,0:T(1,128)S(1)} %get-tuple-element.18.gain_ref, bf16[32,64]{1,0:T(8,128)(2,1)S(1)} %get-tuple-element.19.chosen_ref, ...), custom_call_target="tpu_custom_call" | custom-call | tf_op jit(solution)/shard_map/expert/pallas_call | solution.py:347
  26.2 0.1 collective-permute-start.3
  26.3 1.2 %collective-permute-done.3.got_ref = bf16[16,1024]{1,0:T(8,128)(2,1)S(1)} collective-permute-done((bf16[16,1024]{1,0:T(8,128)(2,1)S(1)}, bf16[16,1024]{1,0:T(8,128)(2,1)S(1)}, u32[]{:S(2)}, u32[]{:S(2)}) %collective-permute-start.3) | collective-permute-done | bytes 32800 | tf_op jit(solution)/shard_map/ppermute | solution.py:366
  27.5 0.7 %spread.1 = bf16[8,4,16,128]{3,2,1,0:T(8,128)(2,1)} custom-call(bf16[16,1024]{1,0:T(8,128)(2,1)S(1)} %get-tuple-element.23.own_ref, bf16[16,1024]{1,0:T(8,128)(2,1)S(1)} %collective-permute-done.3.got_ref), custom_call_target="tpu_custom_call" | custom-call | tf_op jit(solution)/shard_map/spread/pallas_call | solution.py:370
  28.2 2.6 %all-to-all-start.1 = ((bf16[32,16,128]{2,1,0:T(8,128)(2,1)}), bf16[32,16,128]{2,1,0:T(8,128)(2,1)S(1)}, u32[]{:S(2)}, u32[]{:S(2)}) async-start(bf16[32,16,128]{2,1,0:T(8,128)(2,1)} %bitcast.17), calls=%async_computation.1 | async-start | bytes 262144 | tf_op jit(solution)/shard_map/all_to_all | solution.py:378
  30.8 3.7 %state.1 = f32[8,128,256]{2,1,0:T(8,128)} custom-call(f32[8,128]{1,0:T(8,128)S(1)} %get-tuple-element.25.keep_ref, f32[8,128]{1,0:T(8,128)S(1)} %get-tuple-element.26.adk_ref, f32[8,256]{1,0:T(8,128)S(1)} %get-tuple-element.27.value_ref, f32[8,128,256]{2,1,0:T(8,128)} %bitcast.32), custom_call_target="tpu_custom_call" | custom-call | flops 8388608 | bytes 2097152 | tf_op jit(solution)/shard_map/state/pallas_call | solution.py:310
  34.5 4.5 %all-to-all-done.1 = bf16[32,16,128]{2,1,0:T(8,128)(2,1)S(1)} async-done(((bf16[32,16,128]{2,1,0:T(8,128)(2,1)}), bf16[32,16,128]{2,1,0:T(8,128)(2,1)S(1)}, u32[]{:S(2)}, u32[]{:S(2)}) %all-to-all-start.1) | async-done | bytes 131104 | tf_op jit(solution)/shard_map/all_to_all | solution.py:378
  39.0 0.8 %mix.1 = bf16[64,128]{1,0:T(8,128)(2,1)} custom-call(bf16[64,128]{1,0:T(8,128)(2,1)S(1)} %get-tuple-element.21.middle_ref, bf16[64,512]{1,0:T(8,128)(2,1)S(1)} %get-tuple-element.22.pick_ref, bf16[512,128]{1,0:T(8,128)(2,1)S(1)} %bitcast.27), custom_call_target="tpu_custom_call" | custom-call | tf_op jit(solution)/shard_map/mix/pallas_call | solution.py:381
Async XLA Ops:
  0.6 0.7 %copy-start.4 = (f32[4]{0:T(128)S(1)}, f32[4]{0:T(128)}, u32[]{:S(2)}) copy-start(f32[4]{0:T(128)} %bias_ref.1) | copy-start | bytes 52
  1.3 9.9 %copy-start.3 = (bf16[8,1024]{1,0:T(8,128)(2,1)S(1)}, bf16[8,1024]{1,0:T(8,128)(2,1)}, u32[]{:S(2)}) copy-start(bf16[8,1024]{1,0:T(8,128)(2,1)} %refs_0_.1) | copy-start | bytes 49156
  1.3 23.8 %copy-start.2 = (bf16[1,128,1024]{2,1,0:T(8,128)(2,1)S(1)}, bf16[1,128,1024]{2,1,0:T(8,128)(2,1)}, u32[]{:S(2)}) copy-start(bf16[1,128,1024]{2,1,0:T(8,128)(2,1)} %param.39) | copy-start | bytes 786436
  5.0 20.1 %copy-start.1 = (bf16[1,1024,128]{2,1,0:T(8,128)(2,1)S(1)}, bf16[1,1024,128]{2,1,0:T(8,128)(2,1)}, u32[]{:S(2)}) copy-start(bf16[1,1024,128]{2,1,0:T(8,128)(2,1)} %param.38) | copy-start | bytes 786436
  5.0 20.1 %copy-start = (bf16[1,1024,128]{2,1,0:T(8,128)(2,1)S(1)}, bf16[1,1024,128]{2,1,0:T(8,128)(2,1)}, u32[]{:S(2)}) copy-start(bf16[1,1024,128]{2,1,0:T(8,128)(2,1)} %param.37) | copy-start | bytes 786436
  5.0 3.9 %collective-permute-start.2 = (bf16[8,1024]{1,0:T(8,128)(2,1)S(1)}, bf16[8,1024]{1,0:T(8,128)(2,1)S(1)}, u32[]{:S(2)}, u32[]{:S(2)}) collective-permute-start(bf16[8,1024]{1,0:T(8,128)(2,1)S(1)} %get-tuple-element.17.refs_1_), channel_id=1, source_target_pairs={{0,3},{1,2},{2,1},{3,0},{4,7},{5,6},{6,5},{7,4},{8,11},{9,10},{10,... | collective-permute-start | bytes 49160 | tf_op jit(solution)/shard_map/ppermute | solution.py:227
  7.5 3.7 %collective-permute-start.1 = (bf16[8,1024]{1,0:T(8,128)(2,1)S(1)}, bf16[8,1024]{1,0:T(8,128)(2,1)S(1)}, u32[]{:S(2)}, u32[]{:S(2)}) collective-permute-start(bf16[8,1024]{1,0:T(8,128)(2,1)S(1)} %get-tuple-element.17.refs_1_), channel_id=1, source_target_pairs={{0,2},{1,3},{2,0},{3,1},{4,6},{5,7},{6,4},{7,5},{8,10},{9,11},{10,... | collective-permute-start | bytes 49160 | tf_op jit(solution)/shard_map/ppermute | solution.py:227
  8.1 3.1 %collective-permute-start = (bf16[8,1024]{1,0:T(8,128)(2,1)S(1)}, bf16[8,1024]{1,0:T(8,128)(2,1)S(1)}, u32[]{:S(2)}, u32[]{:S(2)}) collective-permute-start(bf16[8,1024]{1,0:T(8,128)(2,1)S(1)} %get-tuple-element.17.refs_1_), channel_id=1, source_target_pairs={{0,1},{1,0},{2,3},{3,2},{4,5},{5,4},{6,7},{7,6},{8,9},{9,8},{10,11... | collective-permute-start | bytes 49160 | tf_op jit(solution)/shard_map/ppermute | solution.py:227
  11.9 13.2 %all-to-all-start = ((bf16[8,8,1024]{2,1,0:T(8,128)(2,1)}), bf16[8,8,1024]{2,1,0:T(8,128)(2,1)S(1)}, u32[]{:S(2)}, u32[]{:S(2)}) async-start(bf16[8,8,1024]{2,1,0:T(8,128)(2,1)} %middle.1), calls=%async_computation | async-start | bytes 262144 | tf_op jit(solution)/shard_map/all_to_all | solution.py:324
  26.2 1.3 %collective-permute-start.3 = (bf16[16,1024]{1,0:T(8,128)(2,1)S(1)}, bf16[16,1024]{1,0:T(8,128)(2,1)S(1)}, u32[]{:S(2)}, u32[]{:S(2)}) collective-permute-start(bf16[16,1024]{1,0:T(8,128)(2,1)S(1)} %get-tuple-element.24), channel_id=1, source_target_pairs={{0,1},{1,0},{2,3},{3,2},{4,5},{5,4},{6,7},{7,6},{8,9},{9,8},{10,11... | collective-permute-start | bytes 98312 | tf_op jit(solution)/shard_map/ppermute | solution.py:366
  28.2 10.8 %all-to-all-start.1 = ((bf16[32,16,128]{2,1,0:T(8,128)(2,1)}), bf16[32,16,128]{2,1,0:T(8,128)(2,1)S(1)}, u32[]{:S(2)}, u32[]{:S(2)}) async-start(bf16[32,16,128]{2,1,0:T(8,128)(2,1)} %bitcast.17), calls=%async_computation.1 | async-start | bytes 262144 | tf_op jit(solution)/shard_map/all_to_all | solution.py:378

commit v3 on v2

--- a/solution.py
+++ b/solution.py
@@ -12,6 +12,9 @@
 LANES = 128
 CHUNK_ROWS = 512
 VMEM_LIMIT = 32 << 20
+CELL_INPUTS = (
+    "tokens", "mix", "wi", "wf", "bias", "max", "wq", "wk", "norm", "mem", "wv", "wo", "hgain", "wout"
+)
 
 F32 = jnp.float32
 BF16 = jnp.bfloat16
@@ -42,72 +45,62 @@
     return jnp.sum(jnp.where(eye, column, 0.0), axis=0, keepdims=True)
 
 
-def cell_kernel(
-    head_ref, bias_ref, tokens_ref, mix_ref, wi_ref, wf_ref, hgain_ref, norm_ref, max_ref,
-    wq_hbm, wk_hbm, wv_hbm, wo_hbm, mem_hbm, wout_hbm,
-    part_ref, nstate_ref, nmax_ref, keep_ref, adk_ref, value_ref,
-    wq, wk, wv, wo, mem, wout, sems,
-):
-    pairs = ((wq_hbm, wq), (wk_hbm, wk), (wv_hbm, wv), (wo_hbm, wo), (mem_hbm, mem), (wout_hbm, wout))
-    copies = [pltpu.make_async_copy(src, dst, sems.at[i]) for i, (src, dst) in enumerate(pairs)]
-    for copy in copies:
-        copy.start()
-    head = head_ref[0]
-    rows = tokens_ref.shape[0]
-    qk_dim = wq.shape[1]
-    normed = norm_rows(tokens_ref[...].astype(F32), mix_ref[...])
+def cell_kernel(*refs):
+    count = len(CELL_INPUTS)
+    far_refs, outs, near_refs, sems = refs[:count], refs[count:-count - 1], refs[-count - 1 : -1], refs[-1]
+    part_ref, nstate_ref, nmax_ref, keep_ref, adk_ref, value_ref, mem_ref = outs
+    copies, local = {}, {}
+    for i, name in enumerate(CELL_INPUTS):
+        local[name] = mem_ref if name == "mem" else near_refs[i]
+        copies[name] = pltpu.make_async_copy(far_refs[i], local[name], sems.at[i])
+        copies[name].start()
+
+    def ready(name):
+        copies[name].wait()
+        return local[name]
+
+    head = lax.axis_index("tp")
+    tokens = ready("tokens")[...].astype(F32)
+    rows = tokens.shape[0]
+    normed = norm_rows(tokens, ready("mix")[...])
     contract_last = (((1,), (1,)), ((), ()))
-    pick = iota((rows, wi_ref.shape[0]), 1) == head
+    wi_ref, wf_ref = ready("wi"), ready("wf")
+    bias, old_max = ready("bias")[...], ready("max")[...]
+    heads = bias.shape[1]
+    pick = iota((rows, heads), 1) == head
     gate_in = lax.dot_general(normed, wi_ref[...], contract_last, preferred_element_type=F32)
     gate_forget = lax.dot_general(normed, wf_ref[...], contract_last, preferred_element_type=F32)
     log_in = jnp.sum(jnp.where(pick, gate_in, 0.0), axis=1, keepdims=True)
-    forget_pre = jnp.sum(jnp.where(pick, gate_forget, 0.0), axis=1, keepdims=True) + bias_ref[head]
+    forget_pre = jnp.sum(jnp.where(pick, gate_forget + bias, 0.0), axis=1, keepdims=True)
     log_forget = jnp.minimum(forget_pre, 0.0) - jnp.log1p(jnp.exp(-jnp.abs(forget_pre)))
     eye = iota((rows, rows), 0) == iota((rows, rows), 1)
-    carried = log_forget + column_of(max_ref[...], eye)
+    carried = log_forget + column_of(old_max, eye)
     new_max = jnp.maximum(carried, log_in)
     keep = jnp.exp(carried - new_max)
     admit = jnp.exp(log_in - new_max)
     nmax_ref[...] = row_of(new_max, eye)
-    copies[0].wait()
-    query = rounded(normed, wq[...])
-    copies[1].wait()
-    scaled_key = rounded(normed, wk[...]) * qk_dim ** (-0.5)
+    query = rounded(normed, ready("wq")[...])
+    scaled_key = rounded(normed, ready("wk")[...]) * query.shape[1] ** (-0.5)
     admitted = admit * scaled_key
-    norm_state = keep * norm_ref[...] + admitted
+    norm_state = keep * ready("norm")[...] + admitted
     nstate_ref[...] = norm_state
     adk_ref[...] = admitted
     keep_ref[...] = jnp.broadcast_to(keep, keep_ref.shape)
     denom = jnp.sum(query * norm_state, axis=1, keepdims=True)
     overlap = jnp.sum(query * admitted, axis=1, keepdims=True)
     query_cols = jnp.transpose(query)
-    copies[2].wait()
-    value = rounded(normed, wv[...])
-    value_ref[...] = value
-    copies[3].wait()
-    ogate = rounded(normed, wo[...])
-    copies[4].wait()
+    mem = ready("mem")
     reads = [
         jnp.sum(query_cols[:, t : t + 1] * mem[t], axis=0, keepdims=True) for t in range(rows)
     ]
+    value = rounded(normed, ready("wv")[...])
+    value_ref[...] = value
     numer = keep * jnp.concatenate(reads, axis=0) + overlap * value
     read = numer / jnp.maximum(jnp.abs(denom), jnp.exp(-new_max))
     scale = lax.rsqrt(jnp.mean(read * read, axis=-1, keepdims=True) + EPS)
-    gated = (jax.nn.sigmoid(ogate) * read * scale * hgain_ref[...]).astype(BF16)
-    copies[5].wait()
-    part_ref[...] = dot(gated, wout[...]).astype(BF16)
-
-
-def state_kernel(keep_ref, adk_ref, value_ref, mem_ref, out_ref):
-    block = mem_ref.shape[0]
-    first = pl.program_id(0) * block
-    rows = adk_ref.shape[0]
-    adk_cols = jnp.transpose(adk_ref[...])
-    for t in range(block):
-        lane = iota(adk_cols.shape, 1) == first + t
-        column = jnp.sum(jnp.where(lane, adk_cols, 0.0), axis=1, keepdims=True)
-        keep = keep_ref[pl.ds(first + t, 1), :][:, 0:1]
-        out_ref[t] = keep * mem_ref[t] + column * value_ref[pl.ds(first + t, 1), :]
+    ogate = rounded(normed, ready("wo")[...])
+    gated = (jax.nn.sigmoid(ogate) * read * scale * ready("hgain")[...]).astype(BF16)
+    part_ref[...] = dot(gated, ready("wout")[...]).astype(BF16)
 
 
 def middle_kernel(*refs):
@@ -125,9 +118,12 @@
 
 
 def plan_kernel(
-    place_ref, gain_ref, route_ref, weight_ref, chosen_ref, share_ref, gain_out_ref, *pick_refs,
+    place_ref, nstate_ref, nmax_ref, gain_ref, route_ref, weight_ref,
+    nstate_out_ref, nmax_out_ref, chosen_ref, share_ref, gain_out_ref, *pick_refs,
     experts, sources, part,
 ):
+    nstate_out_ref[...] = nstate_ref[...]
+    nmax_out_ref[...] = nmax_ref[...]
     route = route_ref[...]
     weight = weight_ref[...]
     count = route.shape[1]
@@ -264,65 +260,47 @@
     qk_dim, dv = w_query.shape[1], w_value.shape[1]
     head = lax.axis_index("tp")
     spec = jax.ShapeDtypeStruct
-
-    partial, norm_state, new_max, keep, admitted, value = call(
+    memory_rows = memory.reshape(rows, qk_dim, dv)
+    cell_inputs = dict(
+        tokens=tokens,
+        mix=mix_gain.reshape(1, -1),
+        wi=w_igate.T,
+        wf=w_fgate.T,
+        bias=forget_bias.reshape(1, -1),
+        max=running_max.T,
+        wq=w_query,
+        wk=w_key,
+        norm=normalizer.reshape(rows, qk_dim),
+        mem=memory_rows,
+        wv=w_value,
+        wo=w_ogate,
+        hgain=head_gain.reshape(1, -1),
+        wout=w_out,
+    )
+    cell_inputs = [cell_inputs[name] for name in CELL_INPUTS]
+    partial, norm_state, new_max, keep, admitted, value, near_memory = call(
         cell_kernel,
         (
             pltpu.VMEM((rows, width), BF16),
-            spec((rows, qk_dim), F32),
-            spec((1, rows), F32),
+            pltpu.VMEM((rows, qk_dim), F32),
+            pltpu.VMEM((1, rows), F32),
             pltpu.VMEM((rows, LANES), F32),
             pltpu.VMEM((rows, qk_dim), F32),
             pltpu.VMEM((rows, dv), F32),
+            pltpu.VMEM((rows, qk_dim, dv), F32),
         ),
-        [smem, smem] + [vmem] * 7 + [hbm] * 6,
+        [hbm] * len(cell_inputs),
         "cell",
         scratch_shapes=[
-            pltpu.VMEM(w_query.shape, BF16),
-            pltpu.VMEM(w_key.shape, BF16),
-            pltpu.VMEM(w_value.shape, BF16),
-            pltpu.VMEM(w_ogate.shape, BF16),
-            pltpu.VMEM((rows, qk_dim, dv), F32),
-            pltpu.VMEM(w_out.shape, BF16),
-            pltpu.SemaphoreType.DMA((6,)),
-        ],
-    )(
-        head.reshape(1),
-        forget_bias,
-        far(tokens),
-        far(mix_gain.reshape(1, -1)),
-        far(w_igate.T),
-        far(w_fgate.T),
-        far(head_gain.reshape(1, -1)),
-        far(normalizer.reshape(rows, qk_dim)),
-        far(running_max.T),
-        far(w_query),
-        far(w_key),
-        far(w_value),
-        far(w_ogate),
-        far(memory.reshape(rows, qk_dim, dv)),
-        far(w_out),
-    )
-
-    block = 2 if rows % 2 == 0 else 1
-    mem_spec = pl.BlockSpec((block, qk_dim, dv), lambda i: (i, 0, 0))
-    whole = lambda shape: pl.BlockSpec(shape, lambda i: (0, 0))
-    state = call(
-        state_kernel,
-        spec((rows, qk_dim, dv), F32),
-        [whole(keep.shape), whole(admitted.shape), whole(value.shape), mem_spec],
-        "state",
-        out_specs=mem_spec,
-        grid=(rows // block,),
-        cost_estimate=pl.CostEstimate(flops=1 << 23, bytes_accessed=1 << 21, transcendentals=0),
-    )(near(keep), near(admitted), near(value), far(memory.reshape(rows, qk_dim, dv)))
+            pltpu.VMEM((8, LANES) if name == "mem" else x.shape, x.dtype)
+            for name, x in zip(CELL_INPUTS, cell_inputs)
+        ]
+        + [pltpu.SemaphoreType.DMA((len(cell_inputs),))],
+    )(*map(far, cell_inputs))
+
+    state = keep[:, 0:1, None] * near_memory + admitted[:, :, None] * value[:, None, :]
 
     parts = exchanged(partial, "tp")
-    spread = call(
-        middle_kernel, pltpu.VMEM((owners, rows, width), BF16), [vmem] * (2 + len(parts)), "middle"
-    )(near(tokens), near(partial), *map(near, parts))
-    middle = lax.all_to_all(spread, "ep", split_axis=0, concat_axis=0, tiled=True)
-    middle = middle.reshape(count, width)
     place = lax.axis_index("ep")
     groups = 2 if heads % 2 == 0 else 1
     part = EXPERT_CAPACITY // groups
@@ -332,18 +310,28 @@
     short = got_rows <= CHUNK_ROWS
     aligned = cols % LANES == 0
     sizes = dict(experts=owners, sources=heads, part=part)
-    chosen, share, gain, *pick = call(
+    norm_state, new_max, chosen, share, gain, *pick = call(
         functools.partial(plan_kernel, **sizes),
         (
+            spec(norm_state.shape, F32),
+            spec(new_max.shape, F32),
             pltpu.VMEM((EXPERT_CAPACITY, count), BF16),
             pltpu.VMEM((EXPERT_CAPACITY, LANES), F32),
             pltpu.VMEM((1, width), F32),
         )
         + ((pltpu.VMEM((count, got_rows), BF16),) if short else ()),
-        [smem] + [vmem] * 3,
+        [smem] + [vmem] * 5,
         "plan",
         cost_estimate=pl.CostEstimate(flops=1 << 22, bytes_accessed=1 << 16, transcendentals=0),
-    )(places, far(ffn_gain.reshape(1, -1)), far(route.T), far(route_weight.T))
+    )(places, near(norm_state), near(new_max), far(ffn_gain.reshape(1, -1)), far(route.T), far(route_weight.T))
+    parts, state, norm_state, new_max, chosen, share, gain, pick = lax.optimization_barrier(
+        (parts, state, norm_state, new_max, chosen, share, gain, pick)
+    )
+    spread = call(
+        middle_kernel, pltpu.VMEM((owners, rows, width), BF16), [vmem] * (2 + len(parts)), "middle"
+    )(near(tokens), near(partial), *map(near, parts))
+    middle = lax.all_to_all(spread, "ep", split_axis=0, concat_axis=0, tiled=True)
+    middle = middle.reshape(count, width)
     own, send, *own_middle = call(
         expert_kernel,
         (pltpu.VMEM((part, width), BF16), pltpu.VMEM((part, width), BF16))

time: 40.1 us -> 37.1 us (0.925)
  blocking collectives: 0 us -> 24 us
  waiting for transfers between devices: 14.9 us -> 1.36 us
  starting transfers between devices: 11.6 us -> 3.22 us
  Pallas kernels: 11.7 us -> 6.11 us
  other arithmetic: 0.07 us -> 1.26 us
  local copies, waits for them, and re-layouts: 0.67 us -> 0.13 us
    all_to_all x0 -> x2, blocking collectives: none -> 24 us  [the longest x1 13.2 us: shards(): lax.all_to_all(spread, 'ep', split_axis=0, concat_axis=0, tiled=True)]
    all_to_all x2 -> x0, waiting for transfers between devices: 10.7 us -> none  [the longest x1 6.23 us: shards(): lax.all_to_all(spread, 'ep', split_axis=0, concat_axis=0, tiled=True)]
    all_to_all x2 -> x0, starting transfers between devices: 8.39 us -> none  [the longest x1 5.83 us: shards(): lax.all_to_all(spread, 'ep', split_axis=0, concat_axis=0, tiled=True)]
    pallas_call x3 -> x2, Pallas kernels: 8.46 us -> 4.17 us  [the longest x1 2.62 us: shards(): call(cell_kernel, (pltpu.VMEM((rows, width), BF16), pltpu.VMEM((rows, qk_...]
    ppermute x3, waiting for transfers between devices: 3.06 us -> 0.17 us  [exchanged(): return [lax.ppermute(values, axis, pairing) for pairing in pairings]]
    add x0 -> x1, other arithmetic: none -> 1.19 us  [shards(): keep[:, 0:1, None] * near_memory + admitted[:, :, None] * value[:, None, :]]
    pallas_call x1, Pallas kernels: 0.67 us -> 0.01 us  [shards(): call(spread_kernel, pltpu.VMEM((owners, heads, part, cols), BF16), [vmem,...]
    pallas_call x1, Pallas kernels: 0.67 us -> 0.02 us  [shards(): call(middle_kernel, pltpu.VMEM((owners, rows, width), BF16), [vmem] * (2...]
  transfers between devices with their start and end apart: 6 -> 4, of which waited for: 5 -> 2; matrix products, arithmetic and copies ran while one was open for 0% -> 4% of each run, Pallas kernels for 12% -> 4%
where the time goes in v3:
time: 37.1 us; the launch traced here: 36.8 us
  blocking collectives  24 us (65%)
  Pallas kernels  6.11 us (16%)
  starting transfers between devices  3.22 us (9%)
  waiting for transfers between devices  1.36 us (4%)
  other arithmetic  1.26 us (3%)
  between operations  0.7 us (2%)
    all_to_all x1, blocking collectives, shards(): lax.all_to_all(spread, 'ep', split_axis=0, concat_axis=0, tiled=True)  13.2 us
    all_to_all x1, blocking collectives, shards(): lax.all_to_all(pieces, ('ep', 'tp'), split_axis=0, concat_axis=0, tiled=T...  10.7 us
    ppermute x3, starting transfers between devices, exchanged(): return [lax.ppermute(values, axis, pairing) for pairing in pairings]  3.15 us
    pallas_call x1, Pallas kernels, shards(): call(cell_kernel, (pltpu.VMEM((rows, width), BF16), pltpu.VMEM((rows, qk_...  2.62 us
    pallas_call x1, Pallas kernels, shards(): call(functools.partial(plan_kernel, **sizes), (spec(norm_state.shape, F32...  1.55 us
    ppermute x1, waiting for transfers between devices, shards(): got = lax.ppermute(send, 'tp', [(i, i ^ 1) for i in range(heads)])  1.19 us
    add x1, other arithmetic, shards(): keep[:, 0:1, None] * near_memory + admitted[:, :, None] * value[:, None, :]  1.19 us
    pallas_call x1, Pallas kernels, shards(): call(expert_kernel, (pltpu.VMEM((part, width), BF16), pltpu.VMEM((part, w...  1.15 us
  transfers between devices with their start and end apart: 4, of which 2 were waited for; matrix products, arithmetic and copies ran while one was open for 4% of the time, Pallas kernels for 4%

profile of v3, /device:TPU:0, one launch (start us, length us, event | category | flops | bytes accessed | tf_op | source)
XLA Modules:
  0.0 36.8 jit_solution(16296262362261001886)
XLA Ops:
  0.6 2.6 %cell.1 = (bf16[8,1024]{1,0:T(8,128)(2,1)S(1)}, f32[8,128]{1,0:T(8,128)S(1)}, f32[1,8]{1,0:T(1,128)S(1)}, f32[8,128]{1,0:T(8,128)S(1)}, f32[8,128]{1,0:T(8,128)S...) custom-call(bf16[8,1024]{1,0:T(8,128)(2,1)} %refs_0_.3, f32[1,1024]{1,0:T(1,128)} %bitcast.36, ...), custom_call_target="tpu_custom_call" | custom-call | tf_op jit(solution)/shard_map/cell/pallas_call | solution.py:281
  3.3 0.6 %collective-permute-start = (bf16[8,1024]{1,0:T(8,128)(2,1)S(1)}, bf16[8,1024]{1,0:T(8,128)(2,1)S(1)}, u32[]{:S(2)}, u32[]{:S(2)}) collective-permute-start(bf16[8,1024]{1,0:T(8,128)(2,1)S(1)} %get-tuple-element.30.refs_1_), channel_id=1, source_target_pairs={{0,1},{1,0},{2,3},{3,2},{4,5},{5,4},{6,7},{7,6},{8,9},{9,8},{10,11... | collective-permute-start | bytes 49160 | tf_op jit(solution)/shard_map/ppermute | solution.py:223
  3.8 2.6 %collective-permute-start.1 = (bf16[8,1024]{1,0:T(8,128)(2,1)S(1)}, bf16[8,1024]{1,0:T(8,128)(2,1)S(1)}, u32[]{:S(2)}, u32[]{:S(2)}) collective-permute-start(bf16[8,1024]{1,0:T(8,128)(2,1)S(1)} %get-tuple-element.30.refs_1_), channel_id=1, source_target_pairs={{0,2},{1,3},{2,0},{3,1},{4,6},{5,7},{6,4},{7,5},{8,10},{9,11},{10,... | collective-permute-start | bytes 49160 | tf_op jit(solution)/shard_map/ppermute | solution.py:223
  6.4 0.0 collective-permute-start.2
  6.4 0.1 slice_reduce_fusion
  6.5 0.0 copy-start.3
  6.5 0.0 copy-start.2
  6.6 1.2 %multiply_add_fusion = f32[8,128,256]{2,1,0:T(8,128)} fusion(f32[8,128,256]{2,1,0:T(8,128)S(1)} %get-tuple-element.32, f32[8,256]{1,0:T(8,128)S(1)} %get-tuple-element.34, f32[8,128]{1,0:T(8,128)S(1)} %get-tuple-element.33, f32[8]{0:T(128)S(1)} %slice_reduce_fusion), kind=kLoop, calls=%fused_computation | loop fusion | flops 786432 | bytes 2109472 | tf_op jit(solution)/shard_map/add | solution.py:301
  7.7 0.0 copy-start.1
  7.7 0.0 copy-start
  7.7 0.1 pad_add_fusion.place_ref
  7.8 1.5 %plan.1 = (f32[8,128]{1,0:T(8,128)}, f32[1,8]{1,0:T(1,128)}, bf16[32,64]{1,0:T(8,128)(2,1)S(1)}, f32[32,128]{1,0:T(8,128)S(1)}, f32[1,1024]{1,0:T(1,128)S(1)}, /*index=5*/bf16[64,512]{1,0:T(8,128)(2,1)S(1)}) custom-call(s32[2]{0:T(128)S(1)} %pad_add_fusion.place_ref, f32[8,128]{1,0:T(8,128)S(1)} %get-tuple-element.35.nstate_ref, ...), custom_call_target="tpu_custom_call" | custom-call | flops 4194304 | bytes 65536 | tf_op jit(solution)/shard_map/plan/pallas_call | solution.py:313
  9.4 0.0 collective-permute-done.refs_2_
  9.4 0.0 collective-permute-done.1.refs_3_
  9.4 0.2 collective-permute-done.2.refs_4_
  9.5 0.0 copy-done.3
  9.6 13.2 %all_to_all.10 = bf16[8,8,1024]{2,1,0:T(8,128)(2,1)S(1)} all-to-all(bf16[8,8,1024]{2,1,0:T(8,128)(2,1)S(1)} %middle.1), channel_id=1, replica_groups=mesh['ep'=8,'tp'=4] {'ep'}, dimensions={0} | all-to-all | bytes 262144 | tf_op jit(solution)/shard_map/all_to_all | solution.py:333
  22.8 0.0 copy-done.2
  22.8 0.0 copy-done.1
  22.8 0.0 copy-done
  22.8 1.1 %expert.1 = (bf16[16,1024]{1,0:T(8,128)(2,1)S(1)}, bf16[16,1024]{1,0:T(8,128)(2,1)S(1)}, bf16[64,128]{1,0:T(8,128)(2,1)S(1)}) custom-call(s32[2]{0:T(128)S(1)} %pad_add_fusion.place_ref, bf16[64,1024]{1,0:T(8,128)(2,1)S(1)} %bitcast.26, f32[1,1024]{1,0:T(1,128)S(1)} %get-tuple-element.46.gain_ref, bf16[32,64]{1,0:T(8,128)(2,1)S(1)} %get-tuple-element.47.chosen_ref, ...), custom_call_target="tpu_custom_call" | custom-call | tf_op jit(solution)/shard_map/expert/pallas_call | solution.py:335
  24.0 0.1 collective-permute-start.3
  24.1 1.2 %collective-permute-done.3.got_ref = bf16[16,1024]{1,0:T(8,128)(2,1)S(1)} collective-permute-done((bf16[16,1024]{1,0:T(8,128)(2,1)S(1)}, bf16[16,1024]{1,0:T(8,128)(2,1)S(1)}, u32[]{:S(2)}, u32[]{:S(2)}) %collective-permute-start.3) | collective-permute-done | bytes 32800 | tf_op jit(solution)/shard_map/ppermute | solution.py:354
  25.3 10.7 %all_to_all.11 = bf16[32,16,128]{2,1,0:T(8,128)(2,1)S(1)} all-to-all(bf16[32,16,128]{2,1,0:T(8,128)(2,1)S(1)} %bitcast.28), channel_id=1, replica_groups=mesh['ep'=8,'tp'=4] {'ep','tp'}, dimensions={0} | all-to-all | bytes 262144 | tf_op jit(solution)/shard_map/all_to_all | solution.py:366
  36.0 0.8 %mix.1 = bf16[64,128]{1,0:T(8,128)(2,1)} custom-call(bf16[64,128]{1,0:T(8,128)(2,1)S(1)} %get-tuple-element.49.middle_ref, bf16[64,512]{1,0:T(8,128)(2,1)S(1)} %get-tuple-element.50.pick_ref, bf16[512,128]{1,0:T(8,128)(2,1)S(1)} %bitcast.27), custom_call_target="tpu_custom_call" | custom-call | tf_op jit(solution)/shard_map/mix/pallas_call | solution.py:369
  (2 shorter events, 0.0 us)
Async XLA Ops:
  3.3 6.1 %collective-permute-start = (bf16[8,1024]{1,0:T(8,128)(2,1)S(1)}, bf16[8,1024]{1,0:T(8,128)(2,1)S(1)}, u32[]{:S(2)}, u32[]{:S(2)}) collective-permute-start(bf16[8,1024]{1,0:T(8,128)(2,1)S(1)} %get-tuple-element.30.refs_1_), channel_id=1, source_target_pairs={{0,1},{1,0},{2,3},{3,2},{4,5},{5,4},{6,7},{7,6},{8,9},{9,8},{10,11... | collective-permute-start | bytes 49160 | tf_op jit(solution)/shard_map/ppermute | solution.py:223
  3.8 5.5 %collective-permute-start.1 = (bf16[8,1024]{1,0:T(8,128)(2,1)S(1)}, bf16[8,1024]{1,0:T(8,128)(2,1)S(1)}, u32[]{:S(2)}, u32[]{:S(2)}) collective-permute-start(bf16[8,1024]{1,0:T(8,128)(2,1)S(1)} %get-tuple-element.30.refs_1_), channel_id=1, source_target_pairs={{0,2},{1,3},{2,0},{3,1},{4,6},{5,7},{6,4},{7,5},{8,10},{9,11},{10,... | collective-permute-start | bytes 49160 | tf_op jit(solution)/shard_map/ppermute | solution.py:223
  6.4 3.2 %collective-permute-start.2 = (bf16[8,1024]{1,0:T(8,128)(2,1)S(1)}, bf16[8,1024]{1,0:T(8,128)(2,1)S(1)}, u32[]{:S(2)}, u32[]{:S(2)}) collective-permute-start(bf16[8,1024]{1,0:T(8,128)(2,1)S(1)} %get-tuple-element.30.refs_1_), channel_id=1, source_target_pairs={{0,3},{1,2},{2,1},{3,0},{4,7},{5,6},{6,5},{7,4},{8,11},{9,10},{10,... | collective-permute-start | bytes 49160 | tf_op jit(solution)/shard_map/ppermute | solution.py:223
  6.5 3.0 %copy-start.3 = (bf16[8,1024]{1,0:T(8,128)(2,1)S(1)}, bf16[8,1024]{1,0:T(8,128)(2,1)}, u32[]{:S(2)}) copy-start(bf16[8,1024]{1,0:T(8,128)(2,1)} %refs_0_.3) | copy-start | bytes 49156
  6.5 16.3 %copy-start.2 = (bf16[1,128,1024]{2,1,0:T(8,128)(2,1)S(1)}, bf16[1,128,1024]{2,1,0:T(8,128)(2,1)}, u32[]{:S(2)}) copy-start(bf16[1,128,1024]{2,1,0:T(8,128)(2,1)} %param.39) | copy-start | bytes 786436
  7.7 15.1 %copy-start.1 = (bf16[1,1024,128]{2,1,0:T(8,128)(2,1)S(1)}, bf16[1,1024,128]{2,1,0:T(8,128)(2,1)}, u32[]{:S(2)}) copy-start(bf16[1,1024,128]{2,1,0:T(8,128)(2,1)} %param.38) | copy-start | bytes 786436
  7.7 15.1 %copy-start = (bf16[1,1024,128]{2,1,0:T(8,128)(2,1)S(1)}, bf16[1,1024,128]{2,1,0:T(8,128)(2,1)}, u32[]{:S(2)}) copy-start(bf16[1,1024,128]{2,1,0:T(8,128)(2,1)} %param.37) | copy-start | bytes 786436
  24.0 1.3 %collective-permute-start.3 = (bf16[16,1024]{1,0:T(8,128)(2,1)S(1)}, bf16[16,1024]{1,0:T(8,128)(2,1)S(1)}, u32[]{:S(2)}, u32[]{:S(2)}) collective-permute-start(bf16[16,1024]{1,0:T(8,128)(2,1)S(1)} %get-tuple-element.52), channel_id=1, source_target_pairs={{0,1},{1,0},{2,3},{3,2},{4,5},{5,4},{6,7},{7,6},{8,9},{9,8},{10,11... | collective-permute-start | bytes 98312 | tf_op jit(solution)/shard_map/ppermute | solution.py:354

commit v4 on v3

--- a/solution.py
+++ b/solution.py
@@ -13,7 +13,8 @@
 CHUNK_ROWS = 512
 VMEM_LIMIT = 32 << 20
 CELL_INPUTS = (
-    "tokens", "mix", "wi", "wf", "bias", "max", "wq", "wk", "norm", "mem", "wv", "wo", "hgain", "wout"
+    "tokens", "mix", "wi", "wf", "bias", "max", "route", "share", "wq", "wk", "norm", "mem", "wv",
+    "wo", "hgain", "wout", "fgain",
 )
 
 F32 = jnp.float32
@@ -45,13 +46,18 @@
     return jnp.sum(jnp.where(eye, column, 0.0), axis=0, keepdims=True)
 
 
-def cell_kernel(*refs):
+def cell_kernel(*refs, experts, sources, part):
     count = len(CELL_INPUTS)
-    far_refs, outs, near_refs, sems = refs[:count], refs[count:-count - 1], refs[-count - 1 : -1], refs[-1]
-    part_ref, nstate_ref, nmax_ref, keep_ref, adk_ref, value_ref, mem_ref = outs
+    far_refs, outs, scratch = refs[:count], refs[count : -count - 4], refs[-count - 4 :]
+    near_refs, (nstate_near, nmax_near), (sems, out_sems) = scratch[:count], scratch[count:-2], scratch[-2:]
+    (
+        own_ref, send_ref, nstate_ref, nmax_ref, keep_ref, adk_ref, value_ref, mem_ref, gain_ref,
+        chosen_ref, share_ref, *pick_refs,
+    ) = outs
+    direct = {"mem": mem_ref, "fgain": gain_ref}
     copies, local = {}, {}
     for i, name in enumerate(CELL_INPUTS):
-        local[name] = mem_ref if name == "mem" else near_refs[i]
+        local[name] = direct.get(name, near_refs[i])
         copies[name] = pltpu.make_async_copy(far_refs[i], local[name], sems.at[i])
         copies[name].start()
 
@@ -78,12 +84,21 @@
     new_max = jnp.maximum(carried, log_in)
     keep = jnp.exp(carried - new_max)
     admit = jnp.exp(log_in - new_max)
-    nmax_ref[...] = row_of(new_max, eye)
+    nmax_near[...] = row_of(new_max, eye)
+    nmax_copy = pltpu.make_async_copy(nmax_near, nmax_ref, out_sems.at[0])
+    nmax_copy.start()
+    route, weight = ready("route")[...], ready("share")[...]
+    plan(route, weight, chosen_ref, share_ref)
+    for pick_ref in pick_refs:
+        slots = slot_table(route, experts)
+        pick_ref[...] = pick_matrix(slots, 0, pick_ref.shape[1], sources, part)
     query = rounded(normed, ready("wq")[...])
     scaled_key = rounded(normed, ready("wk")[...]) * query.shape[1] ** (-0.5)
     admitted = admit * scaled_key
     norm_state = keep * ready("norm")[...] + admitted
-    nstate_ref[...] = norm_state
+    nstate_near[...] = norm_state
+    nstate_copy = pltpu.make_async_copy(nstate_near, nstate_ref, out_sems.at[1])
+    nstate_copy.start()
     adk_ref[...] = admitted
     keep_ref[...] = jnp.broadcast_to(keep, keep_ref.shape)
     denom = jnp.sum(query * norm_state, axis=1, keepdims=True)
@@ -100,48 +115,48 @@
     scale = lax.rsqrt(jnp.mean(read * read, axis=-1, keepdims=True) + EPS)
     ogate = rounded(normed, ready("wo")[...])
     gated = (jax.nn.sigmoid(ogate) * read * scale * ready("hgain")[...]).astype(BF16)
-    part_ref[...] = dot(gated, ready("wout")[...]).astype(BF16)
-
-
-def middle_kernel(*refs):
-    tokens_ref, *parts, out_ref = refs
-    total = parts[0][...].astype(F32)
-    for part in parts[1:]:
-        total = total + part[...].astype(F32)
-    middle = (tokens_ref[...].astype(F32) + total).astype(BF16)
+    partial = dot(gated, ready("wout")[...])
+    span = own_ref.shape[1]
+    low, high = partial[:, :span], partial[:, span:]
+    first = head % 2 == 0
+    residual = jnp.where(first, tokens[:, :span], tokens[:, span:]) * 0.5
+    own_ref[...] = jnp.where(first, low, high) + residual
+    send_ref[...] = jnp.where(first, high, low).astype(BF16)
+    ready("fgain")
+    nmax_copy.wait()
+    nstate_copy.wait()
+
+
+def pair_kernel(own_ref, got_ref, out_ref):
+    total = (own_ref[...] + got_ref[...].astype(F32)).astype(BF16)
     for copy in range(out_ref.shape[0]):
-        out_ref[copy] = middle
+        out_ref[copy] = total
+
+
+def join_kernel(got_ref, out_ref):
+    owners, chips, rows, span = got_ref.shape
+    total = got_ref[:, 0].astype(F32)
+    for chip in range(1, chips):
+        total = total + got_ref[:, chip].astype(F32)
+    out_ref[...] = total.astype(BF16).reshape(owners * rows, span)
 
 
 def earlier_matrix(count):
     return (iota((count, count), 0) < iota((count, count), 1)).astype(BF16)
 
 
-def plan_kernel(
-    place_ref, nstate_ref, nmax_ref, gain_ref, route_ref, weight_ref,
-    nstate_out_ref, nmax_out_ref, chosen_ref, share_ref, gain_out_ref, *pick_refs,
-    experts, sources, part,
-):
-    nstate_out_ref[...] = nstate_ref[...]
-    nmax_out_ref[...] = nmax_ref[...]
-    route = route_ref[...]
-    weight = weight_ref[...]
+def plan(route, weight, chosen_ref, share_ref):
     count = route.shape[1]
-    earlier = earlier_matrix(count)
-    named = route == place_ref[0]
+    named = route == lax.axis_index("ep")
     share = jnp.where(named, weight, 0.0) / jnp.sum(weight, axis=0, keepdims=True)
     share = jnp.sum(share, axis=0, keepdims=True)
     member = jnp.sum(named.astype(F32), axis=0, keepdims=True)
-    slot = dot(jnp.broadcast_to(member, (8, count)).astype(BF16), earlier)[0:1]
+    slot = dot(jnp.broadcast_to(member, (8, count)).astype(BF16), earlier_matrix(count))[0:1]
     shape = (EXPERT_CAPACITY, count)
     chosen = (iota(shape, 0).astype(F32) == slot) & (member > 0.5)
     chosen_ref[...] = chosen.astype(BF16)
     slot_share = jnp.sum(jnp.where(chosen, share, 0.0), axis=1, keepdims=True)
     share_ref[...] = jnp.broadcast_to(slot_share, share_ref.shape)
-    gain_out_ref[...] = gain_ref[...]
-    for pick_ref in pick_refs:
-        slots = slot_table(route, experts)
-        pick_ref[...] = pick_matrix(slots, 0, pick_ref.shape[1], sources, part)
 
 
 def slot_table(route, experts):
@@ -168,22 +183,35 @@
 
 
 def expert_kernel(
-    place_ref, middle_ref, gain_ref, chosen_ref, share_ref, wg_ref, wu_ref, wd_ref,
-    own_ref, send_ref, *block_refs,
+    own_ref, got_ref, gain_ref, chosen_ref, share_ref, wg_ref, wu_ref, wd_ref,
+    keep_ref, send_ref, *block_refs,
 ):
-    expert, half = place_ref[0], place_ref[1]
+    expert, half = lax.axis_index("ep"), lax.axis_index("tp") % 2
+    span = own_ref.shape[1]
+    width = 2 * span
     for block_ref in block_refs:
         cols = block_ref.shape[1]
-        block_ref[...] = middle_ref[:, pl.ds(pl.multiple_of(expert * cols, cols), cols)]
-    normed = norm_rows(middle_ref[...].astype(F32), gain_ref[...])
-    rows = dot(chosen_ref[...], normed).astype(BF16)
-    gate = dot(rows, wg_ref[...])
-    up = dot(rows, wu_ref[...])
+        start = expert * cols
+        inner = pl.ds(pl.multiple_of(start % span, cols), cols)
+        mine = start // span == half
+        block_ref[...] = jnp.where(mine, own_ref[:, inner], got_ref[:, inner])
+    gate = up = 0.0
+    chosen = chosen_ref[...]
+    sides = []
+    for side, ref in ((half, own_ref), (1 - half, got_ref)):
+        rows = dot(chosen, ref[...])
+        sides.append((rows, pl.multiple_of(side * span, span)))
+    square = sum(jnp.sum(rows * rows, axis=-1, keepdims=True) for rows, _ in sides)
+    scale = lax.rsqrt(square / width + EPS)
+    for rows, start in sides:
+        normed = (rows * scale * gain_ref[:, pl.ds(start, span)]).astype(BF16)
+        gate = gate + dot(normed, wg_ref[pl.ds(start, span), :])
+        up = up + dot(normed, wu_ref[pl.ds(start, span), :])
     act = (jax.nn.silu(gate) * up).astype(BF16)
     result = (dot(act, wd_ref[...]) * share_ref[:, 0:1]).astype(BF16)
-    part = own_ref.shape[0]
-    low, high = result[:part], result[EXPERT_CAPACITY - part :]
-    own_ref[...] = jnp.where(half == 0, low, high)
+    part = keep_ref.shape[0]
+    low, high = result[:part], result[part:]
+    keep_ref[...] = jnp.where(half == 0, low, high)
     send_ref[...] = jnp.where(half == 0, high, low)
 
 
@@ -214,13 +242,9 @@
     out_ref[...] = total.astype(BF16)
 
 
-def exchanged(values, axis):
-    count = lax.axis_size(axis)
-    if count & (count - 1) == 0:
-        pairings = [[(i, i ^ k) for i in range(count)] for k in range(1, count)]
-    else:
-        pairings = [[(i, (i + k) % count) for i in range(count)] for k in range(1, count)]
-    return [lax.ppermute(values, axis, pairing) for pairing in pairings]
+def paired(values):
+    heads = lax.axis_size("tp")
+    return lax.ppermute(values, "tp", [(i, i ^ 1) for i in range(heads)])
 
 
 def near(values):
@@ -251,14 +275,19 @@
     w_out, memory, normalizer, running_max, ffn_gain, route, route_weight, w_gate, w_up, w_down,
 ):
     vmem = pl.BlockSpec(memory_space=pltpu.VMEM)
-    smem = pl.BlockSpec(memory_space=pltpu.SMEM)
     hbm = pl.BlockSpec(memory_space=pl.ANY)
     owners, heads = lax.axis_size("ep"), lax.axis_size("tp")
+    chips = heads // 2
     rows, width = tokens.shape
+    span = width // 2
     cols = width // owners
     count = route.shape[0]
     qk_dim, dv = w_query.shape[1], w_value.shape[1]
-    head = lax.axis_index("tp")
+    part = EXPERT_CAPACITY // 2
+    got_rows = owners * heads * part
+    short = got_rows <= CHUNK_ROWS
+    aligned = cols % LANES == 0
+    sizes = dict(experts=owners, sources=heads, part=part)
     spec = jax.ShapeDtypeStruct
     memory_rows = memory.reshape(rows, qk_dim, dv)
     cell_inputs = dict(
@@ -268,6 +297,9 @@
         wf=w_fgate.T,
         bias=forget_bias.reshape(1, -1),
         max=running_max.T,
+        route=route.T,
+        share=route_weight.T,
+        fgain=ffn_gain.reshape(1, -1),
         wq=w_query,
         wk=w_key,
         norm=normalizer.reshape(rows, qk_dim),
@@ -278,69 +310,60 @@
         wout=w_out,
     )
     cell_inputs = [cell_inputs[name] for name in CELL_INPUTS]
-    partial, norm_state, new_max, keep, admitted, value, near_memory = call(
-        cell_kernel,
+    scratch = [(8, LANES) if name in ("mem", "fgain") else x.shape for name, x in zip(CELL_INPUTS, cell_inputs)]
+    own, send, norm_state, new_max, keep, admitted, value, near_memory, gain, chosen, share, *pick = call(
+        functools.partial(cell_kernel, **sizes),
         (
-            pltpu.VMEM((rows, width), BF16),
-            pltpu.VMEM((rows, qk_dim), F32),
-            pltpu.VMEM((1, rows), F32),
+            pltpu.VMEM((rows, span), F32),
+            pltpu.VMEM((rows, span), BF16),
+            pltpu.HBM((rows, qk_dim), F32),
+            pltpu.HBM((1, rows), F32),
             pltpu.VMEM((rows, LANES), F32),
             pltpu.VMEM((rows, qk_dim), F32),
             pltpu.VMEM((rows, dv), F32),
             pltpu.VMEM((rows, qk_dim, dv), F32),
-        ),
+            pltpu.VMEM((1, width), F32),
+            pltpu.VMEM((EXPERT_CAPACITY, count), BF16),
+            pltpu.VMEM((EXPERT_CAPACITY, LANES), F32),
+        )
+        + ((pltpu.VMEM((count, got_rows), BF16),) if short else ()),
         [hbm] * len(cell_inputs),
         "cell",
-        scratch_shapes=[
-            pltpu.VMEM((8, LANES) if name == "mem" else x.shape, x.dtype)
-            for name, x in zip(CELL_INPUTS, cell_inputs)
-        ]
-        + [pltpu.SemaphoreType.DMA((len(cell_inputs),))],
+        out_specs=[vmem, vmem, hbm, hbm] + [vmem] * (8 if short else 7),
+        scratch_shapes=[pltpu.VMEM(shape, x.dtype) for shape, x in zip(scratch, cell_inputs)]
+        + [
+            pltpu.VMEM((rows, qk_dim), F32),
+            pltpu.VMEM((1, rows), F32),
+            pltpu.SemaphoreType.DMA((len(cell_inputs),)),
+            pltpu.SemaphoreType.DMA((2,)),
+        ],
     )(*map(far, cell_inputs))
 
+    chunks = call(pair_kernel, pltpu.VMEM((owners * chips, rows, span), BF16), [vmem] * 2, "pair")(
+        near(own), near(paired(send))
+    )
+    same = [[e * heads + t for e in range(owners) for t in range(c, heads, 2)] for c in range(2)]
+    chunks = lax.all_to_all(
+        chunks, ("ep", "tp"), split_axis=0, concat_axis=0, tiled=True, axis_index_groups=same
+    )
+    own = call(join_kernel, pltpu.VMEM((count, span), BF16), [vmem], "join")(
+        near(chunks.reshape(owners, chips, rows, span))
+    )
+    own, near_memory, keep, admitted, value = lax.optimization_barrier(
+        (own, near_memory, keep, admitted, value)
+    )
+    got = paired(own)
     state = keep[:, 0:1, None] * near_memory + admitted[:, :, None] * value[:, None, :]
-
-    parts = exchanged(partial, "tp")
-    place = lax.axis_index("ep")
-    groups = 2 if heads % 2 == 0 else 1
-    part = EXPERT_CAPACITY // groups
-    half = lax.bitwise_and(head, groups - 1)
-    places = jnp.stack([place, half]).astype(jnp.int32)
-    got_rows = owners * heads * part
-    short = got_rows <= CHUNK_ROWS
-    aligned = cols % LANES == 0
-    sizes = dict(experts=owners, sources=heads, part=part)
-    norm_state, new_max, chosen, share, gain, *pick = call(
-        functools.partial(plan_kernel, **sizes),
-        (
-            spec(norm_state.shape, F32),
-            spec(new_max.shape, F32),
-            pltpu.VMEM((EXPERT_CAPACITY, count), BF16),
-            pltpu.VMEM((EXPERT_CAPACITY, LANES), F32),
-            pltpu.VMEM((1, width), F32),
-        )
-        + ((pltpu.VMEM((count, got_rows), BF16),) if short else ()),
-        [smem] + [vmem] * 5,
-        "plan",
-        cost_estimate=pl.CostEstimate(flops=1 << 22, bytes_accessed=1 << 16, transcendentals=0),
-    )(places, near(norm_state), near(new_max), far(ffn_gain.reshape(1, -1)), far(route.T), far(route_weight.T))
-    parts, state, norm_state, new_max, chosen, share, gain, pick = lax.optimization_barrier(
-        (parts, state, norm_state, new_max, chosen, share, gain, pick)
-    )
-    spread = call(
-        middle_kernel, pltpu.VMEM((owners, rows, width), BF16), [vmem] * (2 + len(parts)), "middle"
-    )(near(tokens), near(partial), *map(near, parts))
-    middle = lax.all_to_all(spread, "ep", split_axis=0, concat_axis=0, tiled=True)
-    middle = middle.reshape(count, width)
-    own, send, *own_middle = call(
+    got, state = lax.optimization_barrier((got, state))
+    kept, send, *own_middle = call(
         expert_kernel,
         (pltpu.VMEM((part, width), BF16), pltpu.VMEM((part, width), BF16))
         + ((pltpu.VMEM((count, cols), BF16),) if aligned else ()),
-        [smem] + [vmem] * 7,
+        [vmem] * 8,
         "expert",
     )(
-        places,
-        near(middle),
+        near(own),
+        near(got),
         near(gain),
         near(chosen),
         near(share),
@@ -348,18 +371,17 @@
         near(w_up[0]),
         near(w_down[0]),
     )
-    if not aligned:
-        own_middle = [lax.dynamic_slice_in_dim(middle, place * cols, cols, axis=1)]
-    if groups == 2:
-        got = lax.ppermute(send, "tp", [(i, i ^ 1) for i in range(heads)])
-    else:
-        got = jnp.zeros_like(send)
+    handed = paired(send)
     if aligned:
         pieces = call(
             spread_kernel, pltpu.VMEM((owners, heads, part, cols), BF16), [vmem, vmem], "spread"
-        )(near(own), near(got))
+        )(near(kept), near(handed))
     else:
-        total = (own.astype(F32) + got.astype(F32)).astype(BF16)
+        first = lax.axis_index("tp") % 2 == 0
+        middle = jnp.concatenate([jnp.where(first, own, got), jnp.where(first, got, own)], axis=1)
+        start = lax.axis_index("ep") * cols
+        own_middle = [lax.dynamic_slice_in_dim(middle, start, cols, axis=1)]
+        total = (kept.astype(F32) + handed.astype(F32)).astype(BF16)
         total = total.reshape(part, owners, cols).transpose(1, 0, 2)
         pieces = jnp.broadcast_to(total[:, None], (owners, heads, part, cols))
     pieces = pieces.reshape(owners * heads, part, cols)

time: 37.1 us -> 35.5 us (0.957)
  starting transfers between devices: 3.22 us -> 1.15 us
  blocking collectives: 24 us -> 25.9 us
  Pallas kernels: 6.11 us -> 4.38 us
  waiting for transfers between devices: 1.36 us -> 1.74 us
    all_to_all x1, blocking collectives: 13.2 us -> 15.8 us  [shards(): lax.all_to_all(chunks, ('ep', 'tp'), split_axis=0, concat_axis=0, tiled=T...]
    ppermute x4 -> x3, starting transfers between devices: 3.22 us -> 1.15 us  [paired(): return lax.ppermute(values, 'tp', [(i, i ^ 1) for i in range(heads)])]
    pallas_call x3, Pallas kernels: 4.19 us -> 3.02 us  [the longest x1 2.99 us: shards(): call(functools.partial(cell_kernel, **sizes), (pltpu.VMEM((rows, span), F...]
    all_to_all x1, blocking collectives: 10.7 us -> 10.1 us  [shards(): lax.all_to_all(pieces, ('ep', 'tp'), split_axis=0, concat_axis=0, tiled=T...]
    pallas_call x1, Pallas kernels: 1.15 us -> 0.58 us  [shards(): call(expert_kernel, (pltpu.VMEM((part, width), BF16), pltpu.VMEM((part, w...]
    ppermute x4 -> x3, waiting for transfers between devices: 1.36 us -> 1.74 us  [paired(): return lax.ppermute(values, 'tp', [(i, i ^ 1) for i in range(heads)])]
  transfers between devices with their start and end apart: 4 -> 3, of which waited for: 2 -> 3; matrix products, arithmetic and copies ran while one was open for 4% -> 3% of each run, Pallas kernels for 4% -> 0%
where the time goes in v4:
time: 35.5 us; the launch traced here: 35.2 us
  blocking collectives  25.9 us (73%)
  Pallas kernels  4.38 us (12%)
  waiting for transfers between devices  1.74 us (5%)
  other arithmetic  1.19 us (3%)
  starting transfers between devices  1.15 us (3%)
  between operations  0.7 us (2%)
    all_to_all x1, blocking collectives, shards(): lax.all_to_all(chunks, ('ep', 'tp'), split_axis=0, concat_axis=0, tiled=T...  15.8 us
    all_to_all x1, blocking collectives, shards(): lax.all_to_all(pieces, ('ep', 'tp'), split_axis=0, concat_axis=0, tiled=T...  10.1 us
    pallas_call x1, Pallas kernels, shards(): call(functools.partial(cell_kernel, **sizes), (pltpu.VMEM((rows, span), F...  2.99 us
    ppermute x3, waiting for transfers between devices, paired(): return lax.ppermute(values, 'tp', [(i, i ^ 1) for i in range(heads)])  1.74 us
    add x1, other arithmetic, shards(): keep[:, 0:1, None] * near_memory + admitted[:, :, None] * value[:, None, :]  1.19 us
    ppermute x3, starting transfers between devices, paired(): return lax.ppermute(values, 'tp', [(i, i ^ 1) for i in range(heads)])  1.15 us
    pallas_call x1, Pallas kernels, shards(): call(mix_kernel, spec((count, cols), BF16), [vmem] * 3, 'mix')  0.76 us
  transfers between devices with their start and end apart: 3, of which 3 were waited for; matrix products, arithmetic and copies ran while one was open for 3% of the time, Pallas kernels for 0%

profile of v4, /device:TPU:0, one launch (start us, length us, event | category | flops | bytes accessed | tf_op | source)
XLA Modules:
  0.0 35.2 jit_solution(11360936376147868233)
XLA Ops:
  0.6 3.0 %cell.1 = (f32[8,512]{1,0:T(8,128)S(1)}, bf16[8,512]{1,0:T(8,128)(2,1)S(1)}, f32[8,128]{1,0:T(8,128)}, f32[1,8]{1,0:T(1,128)}, f32[8,128]{1,0:T(8,128)S(1)}, /*i...) custom-call(bf16[8,1024]{1,0:T(8,128)(2,1)} %refs_0_.1, ...), custom_call_target="tpu_custom_call" | custom-call | tf_op jit(solution)/shard_map/cell/pallas_call | solution.py:314
  3.6 0.6 %collective-permute-start = (bf16[8,512]{1,0:T(8,128)(2,1)S(1)}, bf16[8,512]{1,0:T(8,128)(2,1)S(1)}, u32[]{:S(2)}, u32[]{:S(2)}) collective-permute-start(bf16[8,512]{1,0:T(8,128)(2,1)S(1)} %get-tuple-element.27), channel_id=1, source_target_pairs={{0,1},{1,0},{2,3},{3,2},{4,5},{5,4},{6,7},{7,6},{8,9},{9,8},{10,11... | collective-permute-start | bytes 24584 | tf_op jit(solution)/shard_map/ppermute | solution.py:247
  4.2 0.8 %collective-permute-done.got_ref = bf16[8,512]{1,0:T(8,128)(2,1)S(1)} collective-permute-done((bf16[8,512]{1,0:T(8,128)(2,1)S(1)}, bf16[8,512]{1,0:T(8,128)(2,1)S(1)}, u32[]{:S(2)}, u32[]{:S(2)}) %collective-permute-start) | collective-permute-done | bytes 8224 | tf_op jit(solution)/shard_map/ppermute | solution.py:247
  5.0 15.8 %all_to_all.10 = bf16[16,8,512]{2,1,0:T(8,128)(2,1)S(1)} all-to-all(bf16[16,8,512]{2,1,0:T(8,128)(2,1)S(1)} %pair.1), channel_id=1, replica_groups={{0,2,4,6,8,10,12,14,16,18,20,22,24,26,28,30},{1,3,5,7,9,11,13,15,17,19,..., dimensions={0} | all-to-all | bytes 262144 | tf_op jit(solution)/shard_map/all_to_all | solution.py:346
  20.8 0.1 slice_reduce_fusion
  21.0 0.0 copy-start
  21.0 0.0 copy-start.1
  21.0 0.0 copy-start.2
  21.0 0.1 collective-permute-start.1
  21.1 1.2 %multiply_add_fusion = f32[8,128,256]{2,1,0:T(8,128)} fusion(f32[8,128,256]{2,1,0:T(8,128)S(1)} %get-tuple-element.34, f32[8,256]{1,0:T(8,128)S(1)} %get-tuple-element.36, f32[8,128]{1,0:T(8,128)S(1)} %get-tuple-element.35, f32[8]{0:T(128)S(1)} %slice_reduce_fusion), kind=kLoop, calls=%fused_computation | loop fusion | flops 786432 | bytes 2109472 | tf_op jit(solution)/shard_map/add | solution.py:356
  22.3 0.1 collective-permute-done.1.got_ref
  22.3 0.0 copy-done
  22.3 0.0 copy-done.1
  22.3 0.0 copy-done.2
  22.3 0.6 %expert.1 = (bf16[16,1024]{1,0:T(8,128)(2,1)S(1)}, bf16[16,1024]{1,0:T(8,128)(2,1)S(1)}, bf16[64,128]{1,0:T(8,128)(2,1)S(1)}) custom-call(bf16[64,512]{1,0:T(8,128)(2,1)S(1)} %join.1.own_ref, bf16[64,512]{1,0:T(8,128)(2,1)S(1)} %collective-permute-done.1.got_ref, f32[1,1024]{1,0:T(1,128)S(1)} %get-tuple-element.38.gain_ref, ...), custom_call_target="tpu_custom_call" | custom-call | tf_op jit(solution)/shard_map/expert/pallas_call | solution.py:358
  22.9 0.5 %collective-permute-start.2 = (bf16[16,1024]{1,0:T(8,128)(2,1)S(1)}, bf16[16,1024]{1,0:T(8,128)(2,1)S(1)}, u32[]{:S(2)}, u32[]{:S(2)}) collective-permute-start(bf16[16,1024]{1,0:T(8,128)(2,1)S(1)} %get-tuple-element.44), channel_id=1, source_target_pairs={{0,1},{1,0},{2,3},{3,2},{4,5},{5,4},{6,7},{7,6},{8,9},{9,8},{10,11... | collective-permute-start | bytes 98312 | tf_op jit(solution)/shard_map/ppermute | solution.py:247
  23.4 0.9 %collective-permute-done.2.got_ref = bf16[16,1024]{1,0:T(8,128)(2,1)S(1)} collective-permute-done((bf16[16,1024]{1,0:T(8,128)(2,1)S(1)}, bf16[16,1024]{1,0:T(8,128)(2,1)S(1)}, u32[]{:S(2)}, u32[]{:S(2)}) %collective-permute-start.2) | collective-permute-done | bytes 32800 | tf_op jit(solution)/shard_map/ppermute | solution.py:247
  24.3 10.1 %all_to_all.11 = bf16[32,16,128]{2,1,0:T(8,128)(2,1)S(1)} all-to-all(bf16[32,16,128]{2,1,0:T(8,128)(2,1)S(1)} %bitcast.25), channel_id=1, replica_groups=mesh['ep'=8,'tp'=4] {'ep','tp'}, dimensions={0} | all-to-all | bytes 262144 | tf_op jit(solution)/shard_map/all_to_all | solution.py:388
  34.4 0.8 %mix.1 = bf16[64,128]{1,0:T(8,128)(2,1)} custom-call(bf16[64,128]{1,0:T(8,128)(2,1)S(1)} %get-tuple-element.41.middle_ref, bf16[64,512]{1,0:T(8,128)(2,1)S(1)} %get-tuple-element.42.pick_ref, bf16[512,128]{1,0:T(8,128)(2,1)S(1)} %bitcast.24), custom_call_target="tpu_custom_call" | custom-call | tf_op jit(solution)/shard_map/mix/pallas_call | solution.py:391
  (3 shorter events, 0.0 us)
Async XLA Ops:
  3.6 1.4 %collective-permute-start = (bf16[8,512]{1,0:T(8,128)(2,1)S(1)}, bf16[8,512]{1,0:T(8,128)(2,1)S(1)}, u32[]{:S(2)}, u32[]{:S(2)}) collective-permute-start(bf16[8,512]{1,0:T(8,128)(2,1)S(1)} %get-tuple-element.27), channel_id=1, source_target_pairs={{0,1},{1,0},{2,3},{3,2},{4,5},{5,4},{6,7},{7,6},{8,9},{9,8},{10,11... | collective-permute-start | bytes 24584 | tf_op jit(solution)/shard_map/ppermute | solution.py:247
  21.0 1.4 %copy-start = (bf16[1,1024,128]{2,1,0:T(8,128)(2,1)S(1)}, bf16[1,1024,128]{2,1,0:T(8,128)(2,1)}, u32[]{:S(2)}) copy-start(bf16[1,1024,128]{2,1,0:T(8,128)(2,1)} %param.37) | copy-start | bytes 786436
  21.0 1.3 %copy-start.1 = (bf16[1,1024,128]{2,1,0:T(8,128)(2,1)S(1)}, bf16[1,1024,128]{2,1,0:T(8,128)(2,1)}, u32[]{:S(2)}) copy-start(bf16[1,1024,128]{2,1,0:T(8,128)(2,1)} %param.38) | copy-start | bytes 786436
  21.0 1.3 %copy-start.2 = (bf16[1,128,1024]{2,1,0:T(8,128)(2,1)S(1)}, bf16[1,128,1024]{2,1,0:T(8,128)(2,1)}, u32[]{:S(2)}) copy-start(bf16[1,128,1024]{2,1,0:T(8,128)(2,1)} %param.39) | copy-start | bytes 786436
  21.0 1.3 %collective-permute-start.1 = (bf16[64,512]{1,0:T(8,128)(2,1)S(1)}, bf16[64,512]{1,0:T(8,128)(2,1)S(1)}, u32[]{:S(2)}, u32[]{:S(2)}) collective-permute-start(bf16[64,512]{1,0:T(8,128)(2,1)S(1)} %join.1.own_ref), channel_id=1, source_target_pairs={{0,1},{1,0},{2,3},{3,2},{4,5},{5,4},{6,7},{7,6},{8,9},{9,8},{10,11... | collective-permute-start | bytes 196616 | tf_op jit(solution)/shard_map/ppermute | solution.py:247
  22.9 1.4 %collective-permute-start.2 = (bf16[16,1024]{1,0:T(8,128)(2,1)S(1)}, bf16[16,1024]{1,0:T(8,128)(2,1)S(1)}, u32[]{:S(2)}, u32[]{:S(2)}) collective-permute-start(bf16[16,1024]{1,0:T(8,128)(2,1)S(1)} %get-tuple-element.44), channel_id=1, source_target_pairs={{0,1},{1,0},{2,3},{3,2},{4,5},{5,4},{6,7},{7,6},{8,9},{9,8},{10,11... | collective-permute-start | bytes 98312 | tf_op jit(solution)/shard_map/ppermute | solution.py:247

commit v5 on v4

--- a/solution.py
+++ b/solution.py
@@ -13,9 +13,10 @@
 CHUNK_ROWS = 512
 VMEM_LIMIT = 32 << 20
 CELL_INPUTS = (
-    "tokens", "mix", "wi", "wf", "bias", "max", "route", "share", "wq", "wk", "norm", "mem", "wv",
-    "wo", "hgain", "wout", "fgain",
+    "tokens", "mix", "wi", "wf", "bias", "max", "wq", "wk", "norm", "mem", "wv", "wo", "hgain",
+    "wout", "fgain", "route", "share",
 )
+CELL_PASSED = ("mem", "fgain", "route", "share")
 
 F32 = jnp.float32
 BF16 = jnp.bfloat16
@@ -46,15 +47,15 @@
     return jnp.sum(jnp.where(eye, column, 0.0), axis=0, keepdims=True)
 
 
-def cell_kernel(*refs, experts, sources, part):
+def cell_kernel(*refs):
     count = len(CELL_INPUTS)
     far_refs, outs, scratch = refs[:count], refs[count : -count - 4], refs[-count - 4 :]
     near_refs, (nstate_near, nmax_near), (sems, out_sems) = scratch[:count], scratch[count:-2], scratch[-2:]
     (
         own_ref, send_ref, nstate_ref, nmax_ref, keep_ref, adk_ref, value_ref, mem_ref, gain_ref,
-        chosen_ref, share_ref, *pick_refs,
+        route_ref, share_ref,
     ) = outs
-    direct = {"mem": mem_ref, "fgain": gain_ref}
+    direct = dict(zip(CELL_PASSED, (mem_ref, gain_ref, route_ref, share_ref)))
     copies, local = {}, {}
     for i, name in enumerate(CELL_INPUTS):
         local[name] = direct.get(name, near_refs[i])
@@ -87,11 +88,6 @@
     nmax_near[...] = row_of(new_max, eye)
     nmax_copy = pltpu.make_async_copy(nmax_near, nmax_ref, out_sems.at[0])
     nmax_copy.start()
-    route, weight = ready("route")[...], ready("share")[...]
-    plan(route, weight, chosen_ref, share_ref)
-    for pick_ref in pick_refs:
-        slots = slot_table(route, experts)
-        pick_ref[...] = pick_matrix(slots, 0, pick_ref.shape[1], sources, part)
     query = rounded(normed, ready("wq")[...])
     scaled_key = rounded(normed, ready("wk")[...]) * query.shape[1] ** (-0.5)
     admitted = admit * scaled_key
@@ -122,7 +118,8 @@
     residual = jnp.where(first, tokens[:, :span], tokens[:, span:]) * 0.5
     own_ref[...] = jnp.where(first, low, high) + residual
     send_ref[...] = jnp.where(first, high, low).astype(BF16)
-    ready("fgain")
+    for name in ("fgain", "route", "share"):
+        ready(name)
     nmax_copy.wait()
     nstate_copy.wait()
 
@@ -145,7 +142,10 @@
     return (iota((count, count), 0) < iota((count, count), 1)).astype(BF16)
 
 
-def plan(route, weight, chosen_ref, share_ref):
+def plan_kernel(
+    route_ref, weight_ref, chosen_ref, share_ref, *pick_refs, experts, sources, part
+):
+    route, weight = route_ref[...], weight_ref[...]
     count = route.shape[1]
     named = route == lax.axis_index("ep")
     share = jnp.where(named, weight, 0.0) / jnp.sum(weight, axis=0, keepdims=True)
@@ -157,6 +157,9 @@
     chosen_ref[...] = chosen.astype(BF16)
     slot_share = jnp.sum(jnp.where(chosen, share, 0.0), axis=1, keepdims=True)
     share_ref[...] = jnp.broadcast_to(slot_share, share_ref.shape)
+    for pick_ref in pick_refs:
+        slots = slot_table(route, experts)
+        pick_ref[...] = pick_matrix(slots, 0, pick_ref.shape[1], sources, part)
 
 
 def slot_table(route, experts):
@@ -310,26 +313,27 @@
         wout=w_out,
     )
     cell_inputs = [cell_inputs[name] for name in CELL_INPUTS]
-    scratch = [(8, LANES) if name in ("mem", "fgain") else x.shape for name, x in zip(CELL_INPUTS, cell_inputs)]
-    own, send, norm_state, new_max, keep, admitted, value, near_memory, gain, chosen, share, *pick = call(
-        functools.partial(cell_kernel, **sizes),
+    scratch = [
+        (8, LANES) if name in CELL_PASSED else x.shape for name, x in zip(CELL_INPUTS, cell_inputs)
+    ]
+    own, send, norm_state, new_max, *state_parts, gain, near_route, near_weight = call(
+        cell_kernel,
         (
             pltpu.VMEM((rows, span), F32),
             pltpu.VMEM((rows, span), BF16),
             pltpu.HBM((rows, qk_dim), F32),
             pltpu.HBM((1, rows), F32),
-            pltpu.VMEM((rows, LANES), F32),
+            pltpu.VMEM((rows, dv), F32),
             pltpu.VMEM((rows, qk_dim), F32),
             pltpu.VMEM((rows, dv), F32),
             pltpu.VMEM((rows, qk_dim, dv), F32),
             pltpu.VMEM((1, width), F32),
-            pltpu.VMEM((EXPERT_CAPACITY, count), BF16),
-            pltpu.VMEM((EXPERT_CAPACITY, LANES), F32),
-        )
-        + ((pltpu.VMEM((count, got_rows), BF16),) if short else ()),
+            pltpu.VMEM((route.shape[1], count), jnp.int32),
+            pltpu.VMEM((route.shape[1], count), F32),
+        ),
         [hbm] * len(cell_inputs),
         "cell",
-        out_specs=[vmem, vmem, hbm, hbm] + [vmem] * (8 if short else 7),
+        out_specs=[vmem, vmem, hbm, hbm] + [vmem] * 7,
         scratch_shapes=[pltpu.VMEM(shape, x.dtype) for shape, x in zip(scratch, cell_inputs)]
         + [
             pltpu.VMEM((rows, qk_dim), F32),
@@ -339,8 +343,20 @@
         ],
     )(*map(far, cell_inputs))
 
+    chosen, share, *pick = call(
+        functools.partial(plan_kernel, **sizes),
+        (
+            pltpu.VMEM((EXPERT_CAPACITY, count), BF16),
+            pltpu.VMEM((EXPERT_CAPACITY, LANES), F32),
+        )
+        + ((pltpu.VMEM((count, got_rows), BF16),) if short else ()),
+        [vmem] * 2,
+        "plan",
+        cost_estimate=pl.CostEstimate(flops=1 << 22, bytes_accessed=1 << 16, transcendentals=0),
+    )(near(near_route), near(near_weight))
+    got, chosen, share, pick = lax.optimization_barrier((paired(send), chosen, share, pick))
     chunks = call(pair_kernel, pltpu.VMEM((owners * chips, rows, span), BF16), [vmem] * 2, "pair")(
-        near(own), near(paired(send))
+        near(own), near(got)
     )
     same = [[e * heads + t for e in range(owners) for t in range(c, heads, 2)] for c in range(2)]
     chunks = lax.all_to_all(
@@ -349,12 +365,7 @@
     own = call(join_kernel, pltpu.VMEM((count, span), BF16), [vmem], "join")(
         near(chunks.reshape(owners, chips, rows, span))
     )
-    own, near_memory, keep, admitted, value = lax.optimization_barrier(
-        (own, near_memory, keep, admitted, value)
-    )
     got = paired(own)
-    state = keep[:, 0:1, None] * near_memory + admitted[:, :, None] * value[:, None, :]
-    got, state = lax.optimization_barrier((got, state))
     kept, send, *own_middle = call(
         expert_kernel,
         (pltpu.VMEM((part, width), BF16), pltpu.VMEM((part, width), BF16))
@@ -371,7 +382,11 @@
         near(w_up[0]),
         near(w_down[0]),
     )
+    send, state_parts = lax.optimization_barrier((send, state_parts))
     handed = paired(send)
+    keep, admitted, value, near_memory = state_parts
+    state = keep[:, None, :] * near_memory + admitted[:, :, None] * value[:, None, :]
+    handed, state = lax.optimization_barrier((handed, state))
     if aligned:
         pieces = call(
             spread_kernel, pltpu.VMEM((owners, heads, part, cols), BF16), [vmem, vmem], "spread"

time: 35.5 us -> 35.2 us (level)
    pallas_call x1 -> x2, Pallas kernels: 2.99 us -> 3.04 us  [the longest x1 2.72 us: shards(): call(cell_kernel, (pltpu.VMEM((rows, span), F32), pltpu.VMEM((rows, span)...]
  transfers between devices with their start and end apart: 3 -> 3, of which waited for: 3 -> 2; matrix products, arithmetic and copies ran while one was open for 3% -> 3% of each run, Pallas kernels for 0% -> 1%
where the time goes in v5:
time: 35.2 us; the launch traced here: 35 us
  blocking collectives  26.1 us (74%)
  Pallas kernels  4.43 us (13%)
  waiting for transfers between devices  1.75 us (5%)
  other arithmetic  1.18 us (3%)
  starting transfers between devices  0.85 us (2%)
  between operations  0.7 us (2%)
    all_to_all x1, blocking collectives, shards(): lax.all_to_all(chunks, ('ep', 'tp'), split_axis=0, concat_axis=0, tiled=T...  15.9 us
    all_to_all x1, blocking collectives, shards(): lax.all_to_all(pieces, ('ep', 'tp'), split_axis=0, concat_axis=0, tiled=T...  10.1 us
    pallas_call x1, Pallas kernels, shards(): call(cell_kernel, (pltpu.VMEM((rows, span), F32), pltpu.VMEM((rows, span)...  2.72 us
    ppermute x3, waiting for transfers between devices, paired(): return lax.ppermute(values, 'tp', [(i, i ^ 1) for i in range(heads)])  1.75 us
    add x1, other arithmetic, shards(): keep[:, None, :] * near_memory + admitted[:, :, None] * value[:, None, :]  1.18 us
    ppermute x3, starting transfers between devices, paired(): return lax.ppermute(values, 'tp', [(i, i ^ 1) for i in range(heads)])  0.85 us
    pallas_call x1, Pallas kernels, shards(): call(mix_kernel, spec((count, cols), BF16), [vmem] * 3, 'mix')  0.76 us
  transfers between devices with their start and end apart: 3, of which 2 were waited for; matrix products, arithmetic and copies ran while one was open for 3% of the time, Pallas kernels for 1%

profile of v5, /device:TPU:0, one launch (start us, length us, event | category | flops | bytes accessed | tf_op | source)
XLA Modules:
  0.0 35.0 jit_solution(4559906995907037807)
XLA Ops:
  0.6 0.0 copy-start.2
  0.6 2.7 %cell.1 = (f32[8,512]{1,0:T(8,128)S(1)}, bf16[8,512]{1,0:T(8,128)(2,1)S(1)}, f32[8,128]{1,0:T(8,128)}, f32[1,8]{1,0:T(1,128)}, f32[8,256]{1,0:T(8,128)S(1)}, /*i...) custom-call(bf16[8,1024]{1,0:T(8,128)(2,1)} %refs_0_.1, ...), custom_call_target="tpu_custom_call" | custom-call | tf_op jit(solution)/shard_map/cell/pallas_call | solution.py:319
  3.4 0.6 %collective-permute-start = (bf16[8,512]{1,0:T(8,128)(2,1)S(1)}, bf16[8,512]{1,0:T(8,128)(2,1)S(1)}, u32[]{:S(2)}, u32[]{:S(2)}) collective-permute-start(bf16[8,512]{1,0:T(8,128)(2,1)S(1)} %get-tuple-element.33), channel_id=1, source_target_pairs={{0,1},{1,0},{2,3},{3,2},{4,5},{5,4},{6,7},{7,6},{8,9},{9,8},{10,11... | collective-permute-start | bytes 24584 | tf_op jit(solution)/shard_map/ppermute | solution.py:250
  3.9 0.3 plan.1
  4.3 0.5 %collective-permute-done.got_ref = bf16[8,512]{1,0:T(8,128)(2,1)S(1)} collective-permute-done((bf16[8,512]{1,0:T(8,128)(2,1)S(1)}, bf16[8,512]{1,0:T(8,128)(2,1)S(1)}, u32[]{:S(2)}, u32[]{:S(2)}) %collective-permute-start) | collective-permute-done | bytes 8224 | tf_op jit(solution)/shard_map/ppermute | solution.py:250
  4.8 0.0 copy-start.1
  4.8 0.0 copy-start
  4.8 15.9 %all_to_all.10 = bf16[16,8,512]{2,1,0:T(8,128)(2,1)S(1)} all-to-all(bf16[16,8,512]{2,1,0:T(8,128)(2,1)S(1)} %pair.1), channel_id=1, replica_groups={{0,2,4,6,8,10,12,14,16,18,20,22,24,26,28,30},{1,3,5,7,9,11,13,15,17,19,..., dimensions={0} | all-to-all | bytes 262144 | tf_op jit(solution)/shard_map/all_to_all | solution.py:362
  20.7 0.1 collective-permute-start.1
  20.8 1.2 %collective-permute-done.1.got_ref = bf16[64,512]{1,0:T(8,128)(2,1)S(1)} collective-permute-done((bf16[64,512]{1,0:T(8,128)(2,1)S(1)}, bf16[64,512]{1,0:T(8,128)(2,1)S(1)}, u32[]{:S(2)}, u32[]{:S(2)}) %collective-permute-start.1) | collective-permute-done | bytes 65568 | tf_op jit(solution)/shard_map/ppermute | solution.py:250
  22.1 0.0 copy-done.2
  22.1 0.0 copy-done.1
  22.1 0.0 copy-done
  22.1 0.6 %expert.1 = (bf16[16,1024]{1,0:T(8,128)(2,1)S(1)}, bf16[16,1024]{1,0:T(8,128)(2,1)S(1)}, bf16[64,128]{1,0:T(8,128)(2,1)S(1)}) custom-call(bf16[64,512]{1,0:T(8,128)(2,1)S(1)} %join.1.own_ref, bf16[64,512]{1,0:T(8,128)(2,1)S(1)} %collective-permute-done.1.got_ref, f32[1,1024]{1,0:T(1,128)S(1)} %get-tuple-element.40.gain_ref, ...), custom_call_target="tpu_custom_call" | custom-call | tf_op jit(solution)/shard_map/expert/pallas_call | solution.py:369
  22.7 0.2 collective-permute-start.2
  22.9 1.2 %multiply_add_fusion = f32[8,128,256]{2,1,0:T(8,128)} fusion(f32[8,128,256]{2,1,0:T(8,128)S(1)} %get-tuple-element.53, f32[8,256]{1,0:T(8,128)S(1)} %get-tuple-element.55, f32[8,128]{1,0:T(8,128)S(1)} %get-tuple-element.54, f32[8,256]{1,0:T(8,128)S(1)} %get-tuple-element.52), kind=kLoop, calls=%fused_computation | loop fusion | flops 786432 | bytes 2117632 | tf_op jit(solution)/shard_map/add | solution.py:388
  24.1 0.0 collective-permute-done.2.got_ref
  24.1 10.1 %all_to_all.11 = bf16[32,16,128]{2,1,0:T(8,128)(2,1)S(1)} all-to-all(bf16[32,16,128]{2,1,0:T(8,128)(2,1)S(1)} %bitcast.25), channel_id=1, replica_groups=mesh['ep'=8,'tp'=4] {'ep','tp'}, dimensions={0} | all-to-all | bytes 262144 | tf_op jit(solution)/shard_map/all_to_all | solution.py:403
  34.2 0.8 %mix.1 = bf16[64,128]{1,0:T(8,128)(2,1)} custom-call(bf16[64,128]{1,0:T(8,128)(2,1)S(1)} %get-tuple-element.43.middle_ref, bf16[64,512]{1,0:T(8,128)(2,1)S(1)} %get-tuple-element.44.pick_ref, bf16[512,128]{1,0:T(8,128)(2,1)S(1)} %bitcast.24), custom_call_target="tpu_custom_call" | custom-call | tf_op jit(solution)/shard_map/mix/pallas_call | solution.py:406
  (3 shorter events, 0.0 us)
Async XLA Ops:
  0.6 21.4 %copy-start.2 = (bf16[1,128,1024]{2,1,0:T(8,128)(2,1)S(1)}, bf16[1,128,1024]{2,1,0:T(8,128)(2,1)}, u32[]{:S(2)}) copy-start(bf16[1,128,1024]{2,1,0:T(8,128)(2,1)} %param.39) | copy-start | bytes 786436
  3.4 1.4 %collective-permute-start = (bf16[8,512]{1,0:T(8,128)(2,1)S(1)}, bf16[8,512]{1,0:T(8,128)(2,1)S(1)}, u32[]{:S(2)}, u32[]{:S(2)}) collective-permute-start(bf16[8,512]{1,0:T(8,128)(2,1)S(1)} %get-tuple-element.33), channel_id=1, source_target_pairs={{0,1},{1,0},{2,3},{3,2},{4,5},{5,4},{6,7},{7,6},{8,9},{9,8},{10,11... | collective-permute-start | bytes 24584 | tf_op jit(solution)/shard_map/ppermute | solution.py:250
  4.8 17.3 %copy-start.1 = (bf16[1,1024,128]{2,1,0:T(8,128)(2,1)S(1)}, bf16[1,1024,128]{2,1,0:T(8,128)(2,1)}, u32[]{:S(2)}) copy-start(bf16[1,1024,128]{2,1,0:T(8,128)(2,1)} %param.38) | copy-start | bytes 786436
  4.8 17.3 %copy-start = (bf16[1,1024,128]{2,1,0:T(8,128)(2,1)S(1)}, bf16[1,1024,128]{2,1,0:T(8,128)(2,1)}, u32[]{:S(2)}) copy-start(bf16[1,1024,128]{2,1,0:T(8,128)(2,1)} %param.37) | copy-start | bytes 786436
  20.7 1.3 %collective-permute-start.1 = (bf16[64,512]{1,0:T(8,128)(2,1)S(1)}, bf16[64,512]{1,0:T(8,128)(2,1)S(1)}, u32[]{:S(2)}, u32[]{:S(2)}) collective-permute-start(bf16[64,512]{1,0:T(8,128)(2,1)S(1)} %join.1.own_ref), channel_id=1, source_target_pairs={{0,1},{1,0},{2,3},{3,2},{4,5},{5,4},{6,7},{7,6},{8,9},{9,8},{10,11... | collective-permute-start | bytes 196616 | tf_op jit(solution)/shard_map/ppermute | solution.py:250
  22.7 1.4 %collective-permute-start.2 = (bf16[16,1024]{1,0:T(8,128)(2,1)S(1)}, bf16[16,1024]{1,0:T(8,128)(2,1)S(1)}, u32[]{:S(2)}, u32[]{:S(2)}) collective-permute-start(bf16[16,1024]{1,0:T(8,128)(2,1)S(1)} %get-tuple-element.51), channel_id=1, source_target_pairs={{0,1},{1,0},{2,3},{3,2},{4,5},{5,4},{6,7},{7,6},{8,9},{9,8},{10,11... | collective-permute-start | bytes 98312 | tf_op jit(solution)/shard_map/ppermute | solution.py:250

commit v6 on v5

--- a/solution.py
+++ b/solution.py
@@ -13,8 +13,8 @@
 CHUNK_ROWS = 512
 VMEM_LIMIT = 32 << 20
 CELL_INPUTS = (
-    "tokens", "mix", "wi", "wf", "bias", "max", "wq", "wk", "norm", "mem", "wv", "wo", "hgain",
-    "wout", "fgain", "route", "share",
+    "tokens", "mix", "wq", "wi", "wf", "bias", "max", "wk", "norm", "mem", "hgain", "fgain", "route",
+    "share", "wv", "wo", "wout",
 )
 CELL_PASSED = ("mem", "fgain", "route", "share")
 
@@ -62,9 +62,10 @@
         copies[name] = pltpu.make_async_copy(far_refs[i], local[name], sems.at[i])
         copies[name].start()
 
-    def ready(name):
-        copies[name].wait()
-        return local[name]
+    def ready(*names):
+        for name in names:
+            copies[name].wait()
+        return local[names[-1]]
 
     head = lax.axis_index("tp")
     tokens = ready("tokens")[...].astype(F32)
@@ -88,10 +89,11 @@
     nmax_near[...] = row_of(new_max, eye)
     nmax_copy = pltpu.make_async_copy(nmax_near, nmax_ref, out_sems.at[0])
     nmax_copy.start()
-    query = rounded(normed, ready("wq")[...])
-    scaled_key = rounded(normed, ready("wk")[...]) * query.shape[1] ** (-0.5)
+    ready("norm", "hgain", "fgain", "route", "share", "wq", "wk")
+    query = rounded(normed, local["wq"][...])
+    scaled_key = rounded(normed, local["wk"][...]) * query.shape[1] ** (-0.5)
     admitted = admit * scaled_key
-    norm_state = keep * ready("norm")[...] + admitted
+    norm_state = keep * local["norm"][...] + admitted
     nstate_near[...] = norm_state
     nstate_copy = pltpu.make_async_copy(nstate_near, nstate_ref, out_sems.at[1])
     nstate_copy.start()
@@ -104,13 +106,14 @@
     reads = [
         jnp.sum(query_cols[:, t : t + 1] * mem[t], axis=0, keepdims=True) for t in range(rows)
     ]
-    value = rounded(normed, ready("wv")[...])
+    ready("wv", "wo")
+    value = rounded(normed, local["wv"][...])
+    ogate = rounded(normed, local["wo"][...])
     value_ref[...] = value
     numer = keep * jnp.concatenate(reads, axis=0) + overlap * value
     read = numer / jnp.maximum(jnp.abs(denom), jnp.exp(-new_max))
     scale = lax.rsqrt(jnp.mean(read * read, axis=-1, keepdims=True) + EPS)
-    ogate = rounded(normed, ready("wo")[...])
-    gated = (jax.nn.sigmoid(ogate) * read * scale * ready("hgain")[...]).astype(BF16)
+    gated = (jax.nn.sigmoid(ogate) * read * scale * local["hgain"][...]).astype(BF16)
     partial = dot(gated, ready("wout")[...])
     span = own_ref.shape[1]
     low, high = partial[:, :span], partial[:, span:]
@@ -118,24 +121,39 @@
     residual = jnp.where(first, tokens[:, :span], tokens[:, span:]) * 0.5
     own_ref[...] = jnp.where(first, low, high) + residual
     send_ref[...] = jnp.where(first, high, low).astype(BF16)
-    for name in ("fgain", "route", "share"):
-        ready(name)
     nmax_copy.wait()
     nstate_copy.wait()
 
 
+def state_kernel(keep_ref, adk_ref, value_ref, mem_ref, out_ref, made, sems):
+    adk_cols = jnp.transpose(adk_ref[...])
+    copies = []
+    for t in range(mem_ref.shape[0]):
+        old = keep_ref[t : t + 1, :] * mem_ref[t]
+        made[t] = old + adk_cols[:, t : t + 1] * value_ref[t : t + 1, :]
+        copies.append(pltpu.make_async_copy(made.at[t], out_ref.at[t], sems.at[t]))
+        copies[-1].start()
+    for copy in copies:
+        copy.wait()
+
+
 def pair_kernel(own_ref, got_ref, out_ref):
     total = (own_ref[...] + got_ref[...].astype(F32)).astype(BF16)
-    for copy in range(out_ref.shape[0]):
-        out_ref[copy] = total
+    places, cores, _, span = out_ref.shape
+    for core in range(cores):
+        piece = total[:, core * span : (core + 1) * span]
+        for place in range(places):
+            out_ref[place, core] = piece
 
 
 def join_kernel(got_ref, out_ref):
-    owners, chips, rows, span = got_ref.shape
-    total = got_ref[:, 0].astype(F32)
-    for chip in range(1, chips):
-        total = total + got_ref[:, chip].astype(F32)
-    out_ref[...] = total.astype(BF16).reshape(owners * rows, span)
+    owners, chips, cores, rows, span = got_ref.shape
+    for core in range(cores):
+        total = got_ref[:, 0, core].astype(F32)
+        for chip in range(1, chips):
+            total = total + got_ref[:, chip, core].astype(F32)
+        total = total.astype(BF16).reshape(owners * rows, span)
+        out_ref[:, core * span : (core + 1) * span] = total
 
 
 def earlier_matrix(count):
@@ -192,24 +210,27 @@
     expert, half = lax.axis_index("ep"), lax.axis_index("tp") % 2
     span = own_ref.shape[1]
     width = 2 * span
+    quarter = span // 2
     for block_ref in block_refs:
         cols = block_ref.shape[1]
         start = expert * cols
-        inner = pl.ds(pl.multiple_of(start % span, cols), cols)
-        mine = start // span == half
+        inner = pl.ds(pl.multiple_of(start // span * quarter + start % quarter, cols), cols)
+        mine = start % span // quarter == half
         block_ref[...] = jnp.where(mine, own_ref[:, inner], got_ref[:, inner])
     gate = up = 0.0
     chosen = chosen_ref[...]
-    sides = []
+    pieces = []
     for side, ref in ((half, own_ref), (1 - half, got_ref)):
         rows = dot(chosen, ref[...])
-        sides.append((rows, pl.multiple_of(side * span, span)))
-    square = sum(jnp.sum(rows * rows, axis=-1, keepdims=True) for rows, _ in sides)
+        for core in range(2):
+            piece = rows[:, core * quarter : (core + 1) * quarter]
+            pieces.append((piece, pl.multiple_of(core * span + side * quarter, quarter)))
+    square = sum(jnp.sum(piece * piece, axis=-1, keepdims=True) for piece, _ in pieces)
     scale = lax.rsqrt(square / width + EPS)
-    for rows, start in sides:
-        normed = (rows * scale * gain_ref[:, pl.ds(start, span)]).astype(BF16)
-        gate = gate + dot(normed, wg_ref[pl.ds(start, span), :])
-        up = up + dot(normed, wu_ref[pl.ds(start, span), :])
+    for piece, start in pieces:
+        normed = (piece * scale * gain_ref[:, pl.ds(start, quarter)]).astype(BF16)
+        gate = gate + dot(normed, wg_ref[pl.ds(start, quarter), :])
+        up = up + dot(normed, wu_ref[pl.ds(start, quarter), :])
     act = (jax.nn.silu(gate) * up).astype(BF16)
     result = (dot(act, wd_ref[...]) * share_ref[:, 0:1]).astype(BF16)
     part = keep_ref.shape[0]
@@ -355,15 +376,13 @@
         cost_estimate=pl.CostEstimate(flops=1 << 22, bytes_accessed=1 << 16, transcendentals=0),
     )(near(near_route), near(near_weight))
     got, chosen, share, pick = lax.optimization_barrier((paired(send), chosen, share, pick))
-    chunks = call(pair_kernel, pltpu.VMEM((owners * chips, rows, span), BF16), [vmem] * 2, "pair")(
-        near(own), near(got)
-    )
-    same = [[e * heads + t for e in range(owners) for t in range(c, heads, 2)] for c in range(2)]
-    chunks = lax.all_to_all(
-        chunks, ("ep", "tp"), split_axis=0, concat_axis=0, tiled=True, axis_index_groups=same
-    )
+    chunks = call(
+        pair_kernel, pltpu.VMEM((owners * chips, 2, rows, span // 2), BF16), [vmem] * 2, "pair"
+    )(near(own), near(got))
+    chunks = chunks.reshape(owners * heads, rows, span // 2)
+    chunks = lax.all_to_all(chunks, ("ep", "tp"), split_axis=0, concat_axis=0, tiled=True)
     own = call(join_kernel, pltpu.VMEM((count, span), BF16), [vmem], "join")(
-        near(chunks.reshape(owners, chips, rows, span))
+        near(chunks.reshape(owners, chips, 2, rows, span // 2))
     )
     got = paired(own)
     kept, send, *own_middle = call(
@@ -384,8 +403,15 @@
     )
     send, state_parts = lax.optimization_barrier((send, state_parts))
     handed = paired(send)
-    keep, admitted, value, near_memory = state_parts
-    state = keep[:, None, :] * near_memory + admitted[:, :, None] * value[:, None, :]
+    state = call(
+        state_kernel,
+        pltpu.HBM((rows, qk_dim, dv), F32),
+        [vmem] * 4,
+        "state",
+        out_specs=hbm,
+        scratch_shapes=[pltpu.VMEM((rows, qk_dim, dv), F32), pltpu.SemaphoreType.DMA((rows,))],
+        cost_estimate=pl.CostEstimate(flops=1 << 20, bytes_accessed=1 << 21, transcendentals=0),
+    )(*map(near, state_parts))
     handed, state = lax.optimization_barrier((handed, state))
     if aligned:
         pieces = call(
@@ -393,7 +419,8 @@
         )(near(kept), near(handed))
     else:
         first = lax.axis_index("tp") % 2 == 0
-        middle = jnp.concatenate([jnp.where(first, own, got), jnp.where(first, got, own)], axis=1)
+        sides = jnp.stack([jnp.where(first, own, got), jnp.where(first, got, own)], axis=1)
+        middle = sides.reshape(count, 2, 2, span // 2).swapaxes(1, 2).reshape(count, width)
         start = lax.axis_index("ep") * cols
         own_middle = [lax.dynamic_slice_in_dim(middle, start, cols, axis=1)]
         total = (kept.astype(F32) + handed.astype(F32)).astype(BF16)

time: 35.2 us -> 34.2 us (0.972)
  other arithmetic: 1.18 us -> 0 us
  Pallas kernels: 4.43 us -> 5.49 us
  blocking collectives: 26.1 us -> 25.1 us
    pallas_call x1 -> x2, Pallas kernels: 0.01 us -> 1.26 us  [the longest x1 1.25 us: shards(): call(state_kernel, pltpu.HBM((rows, qk_dim, dv), F32), [vmem] * 4, 'state...]
    add x1 -> x0, other arithmetic: 1.18 us -> none  [shards(): keep[:, None, :] * near_memory + admitted[:, :, None] * value[:, None, :]]
    all_to_all x1, blocking collectives: 15.9 us -> 15.2 us  [shards(): lax.all_to_all(chunks, ('ep', 'tp'), split_axis=0, concat_axis=0, tiled=T...]
  transfers between devices with their start and end apart: 3 -> 3, of which waited for: 2 -> 2; matrix products, arithmetic and copies ran while one was open for 3% -> 0% of each run, Pallas kernels for 1% -> 5%
where the time goes in v6:
time: 34.2 us; the launch traced here: 34 us
  blocking collectives  25.1 us (73%)
  Pallas kernels  5.49 us (16%)
  waiting for transfers between devices  1.55 us (5%)
  starting transfers between devices  1.13 us (3%)
  between operations  0.71 us (2%)
    all_to_all x1, blocking collectives, shards(): lax.all_to_all(chunks, ('ep', 'tp'), split_axis=0, concat_axis=0, tiled=T...  15.2 us
    all_to_all x1, blocking collectives, shards(): lax.all_to_all(pieces, ('ep', 'tp'), split_axis=0, concat_axis=0, tiled=T...  9.91 us
    pallas_call x1, Pallas kernels, shards(): call(cell_kernel, (pltpu.VMEM((rows, span), F32), pltpu.VMEM((rows, span)...  2.54 us
    ppermute x3, waiting for transfers between devices, paired(): return lax.ppermute(values, 'tp', [(i, i ^ 1) for i in range(heads)])  1.55 us
    pallas_call x1, Pallas kernels, shards(): call(state_kernel, pltpu.HBM((rows, qk_dim, dv), F32), [vmem] * 4, 'state...  1.25 us
    ppermute x3, starting transfers between devices, paired(): return lax.ppermute(values, 'tp', [(i, i ^ 1) for i in range(heads)])  1.13 us
    pallas_call x1, Pallas kernels, shards(): call(mix_kernel, spec((count, cols), BF16), [vmem] * 3, 'mix')  0.77 us
  transfers between devices with their start and end apart: 3, of which 2 were waited for; matrix products, arithmetic and copies ran while one was open for 0% of the time, Pallas kernels for 5%

profile of v6, /device:TPU:0, one launch (start us, length us, event | category | flops | bytes accessed | tf_op | source)
XLA Modules:
  0.0 34.0 jit_solution(13530574289344209224)
XLA Ops:
  0.6 0.0 copy-start.2
  0.6 2.5 %cell.1 = (f32[8,512]{1,0:T(8,128)S(1)}, bf16[8,512]{1,0:T(8,128)(2,1)S(1)}, f32[8,128]{1,0:T(8,128)}, f32[1,8]{1,0:T(1,128)}, f32[8,256]{1,0:T(8,128)S(1)}, /*i...) custom-call(bf16[8,1024]{1,0:T(8,128)(2,1)} %refs_0_.1, ...), custom_call_target="tpu_custom_call" | custom-call | tf_op jit(solution)/shard_map/cell/pallas_call | solution.py:340
  3.2 0.6 %collective-permute-start = (bf16[8,512]{1,0:T(8,128)(2,1)S(1)}, bf16[8,512]{1,0:T(8,128)(2,1)S(1)}, u32[]{:S(2)}, u32[]{:S(2)}) collective-permute-start(bf16[8,512]{1,0:T(8,128)(2,1)S(1)} %get-tuple-element.33), channel_id=1, source_target_pairs={{0,1},{1,0},{2,3},{3,2},{4,5},{5,4},{6,7},{7,6},{8,9},{9,8},{10,11... | collective-permute-start | bytes 24584 | tf_op jit(solution)/shard_map/ppermute | solution.py:271
  3.8 0.3 plan.1
  4.1 0.5 %collective-permute-done.got_ref = bf16[8,512]{1,0:T(8,128)(2,1)S(1)} collective-permute-done((bf16[8,512]{1,0:T(8,128)(2,1)S(1)}, bf16[8,512]{1,0:T(8,128)(2,1)S(1)}, u32[]{:S(2)}, u32[]{:S(2)}) %collective-permute-start) | collective-permute-done | bytes 8224 | tf_op jit(solution)/shard_map/ppermute | solution.py:271
  4.6 0.0 copy-start.1
  4.6 0.0 copy-start
  4.6 15.2 %all_to_all.10 = bf16[32,8,256]{2,1,0:T(8,128)(2,1)S(1)} all-to-all(bf16[32,8,256]{2,1,0:T(8,128)(2,1)S(1)} %bitcast.26), channel_id=1, replica_groups=mesh['ep'=8,'tp'=4] {'ep','tp'}, dimensions={0} | all-to-all | bytes 262144 | tf_op jit(solution)/shard_map/all_to_all | solution.py:383
  19.8 0.3 collective-permute-start.1
  20.1 1.0 %collective-permute-done.1.got_ref = bf16[64,512]{1,0:T(8,128)(2,1)S(1)} collective-permute-done((bf16[64,512]{1,0:T(8,128)(2,1)S(1)}, bf16[64,512]{1,0:T(8,128)(2,1)S(1)}, u32[]{:S(2)}, u32[]{:S(2)}) %collective-permute-start.1) | collective-permute-done | bytes 65568 | tf_op jit(solution)/shard_map/ppermute | solution.py:271
  21.1 0.0 copy-done.2
  21.1 0.0 copy-done.1
  21.1 0.0 copy-done
  21.2 0.6 %expert.1 = (bf16[16,1024]{1,0:T(8,128)(2,1)S(1)}, bf16[16,1024]{1,0:T(8,128)(2,1)S(1)}, bf16[64,128]{1,0:T(8,128)(2,1)S(1)}) custom-call(bf16[64,512]{1,0:T(8,128)(2,1)S(1)} %join.1.own_ref, bf16[64,512]{1,0:T(8,128)(2,1)S(1)} %collective-permute-done.1.got_ref, f32[1,1024]{1,0:T(1,128)S(1)} %get-tuple-element.40.gain_ref, ...), custom_call_target="tpu_custom_call" | custom-call | tf_op jit(solution)/shard_map/expert/pallas_call | solution.py:388
  21.7 0.3 collective-permute-start.2
  22.0 1.2 %state.1 = f32[8,128,256]{2,1,0:T(8,128)} custom-call(f32[8,256]{1,0:T(8,128)S(1)} %get-tuple-element.52.keep_ref, f32[8,128]{1,0:T(8,128)S(1)} %get-tuple-element.53.adk_ref, f32[8,256]{1,0:T(8,128)S(1)} %get-tuple-element.54.value_ref, f32[8,128,256]{2,1,0:T(8,128)S(1)} %get-tuple-element.55.mem_ref), custom_call_target="tpu_custom_call" | custom-call | flops 1048576 | bytes 2097152 | tf_op jit(solution)/shard_map/state/pallas_call | solution.py:406
  23.3 0.0 collective-permute-done.2.got_ref
  23.3 9.9 %all_to_all.11 = bf16[32,16,128]{2,1,0:T(8,128)(2,1)S(1)} all-to-all(bf16[32,16,128]{2,1,0:T(8,128)(2,1)S(1)} %bitcast.27), channel_id=1, replica_groups=mesh['ep'=8,'tp'=4] {'ep','tp'}, dimensions={0} | all-to-all | bytes 262144 | tf_op jit(solution)/shard_map/all_to_all | solution.py:430
  33.2 0.8 %mix.1 = bf16[64,128]{1,0:T(8,128)(2,1)} custom-call(bf16[64,128]{1,0:T(8,128)(2,1)S(1)} %get-tuple-element.43.middle_ref, bf16[64,512]{1,0:T(8,128)(2,1)S(1)} %get-tuple-element.44.pick_ref, bf16[512,128]{1,0:T(8,128)(2,1)S(1)} %bitcast.25), custom_call_target="tpu_custom_call" | custom-call | tf_op jit(solution)/shard_map/mix/pallas_call | solution.py:433
  (3 shorter events, 0.0 us)
Async XLA Ops:
  0.6 20.5 %copy-start.2 = (bf16[1,128,1024]{2,1,0:T(8,128)(2,1)S(1)}, bf16[1,128,1024]{2,1,0:T(8,128)(2,1)}, u32[]{:S(2)}) copy-start(bf16[1,128,1024]{2,1,0:T(8,128)(2,1)} %param.39) | copy-start | bytes 786436
  3.2 1.4 %collective-permute-start = (bf16[8,512]{1,0:T(8,128)(2,1)S(1)}, bf16[8,512]{1,0:T(8,128)(2,1)S(1)}, u32[]{:S(2)}, u32[]{:S(2)}) collective-permute-start(bf16[8,512]{1,0:T(8,128)(2,1)S(1)} %get-tuple-element.33), channel_id=1, source_target_pairs={{0,1},{1,0},{2,3},{3,2},{4,5},{5,4},{6,7},{7,6},{8,9},{9,8},{10,11... | collective-permute-start | bytes 24584 | tf_op jit(solution)/shard_map/ppermute | solution.py:271
  4.6 16.6 %copy-start.1 = (bf16[1,1024,128]{2,1,0:T(8,128)(2,1)S(1)}, bf16[1,1024,128]{2,1,0:T(8,128)(2,1)}, u32[]{:S(2)}) copy-start(bf16[1,1024,128]{2,1,0:T(8,128)(2,1)} %param.38) | copy-start | bytes 786436
  4.6 16.5 %copy-start = (bf16[1,1024,128]{2,1,0:T(8,128)(2,1)S(1)}, bf16[1,1024,128]{2,1,0:T(8,128)(2,1)}, u32[]{:S(2)}) copy-start(bf16[1,1024,128]{2,1,0:T(8,128)(2,1)} %param.37) | copy-start | bytes 786436
  19.8 1.3 %collective-permute-start.1 = (bf16[64,512]{1,0:T(8,128)(2,1)S(1)}, bf16[64,512]{1,0:T(8,128)(2,1)S(1)}, u32[]{:S(2)}, u32[]{:S(2)}) collective-permute-start(bf16[64,512]{1,0:T(8,128)(2,1)S(1)} %join.1.own_ref), channel_id=1, source_target_pairs={{0,1},{1,0},{2,3},{3,2},{4,5},{5,4},{6,7},{7,6},{8,9},{9,8},{10,11... | collective-permute-start | bytes 196616 | tf_op jit(solution)/shard_map/ppermute | solution.py:271
  21.7 1.5 %collective-permute-start.2 = (bf16[16,1024]{1,0:T(8,128)(2,1)S(1)}, bf16[16,1024]{1,0:T(8,128)(2,1)S(1)}, u32[]{:S(2)}, u32[]{:S(2)}) collective-permute-start(bf16[16,1024]{1,0:T(8,128)(2,1)S(1)} %get-tuple-element.51), channel_id=1, source_target_pairs={{0,1},{1,0},{2,3},{3,2},{4,5},{5,4},{6,7},{7,6},{8,9},{9,8},{10,11... | collective-permute-start | bytes 98312 | tf_op jit(solution)/shard_map/ppermute | solution.py:271

commit v7 on v6

--- a/solution.py
+++ b/solution.py
@@ -20,6 +20,14 @@
 
 F32 = jnp.float32
 BF16 = jnp.bfloat16
+
+
+def ranked(count):
+    return [i // 2 if i % 2 == 0 else count - 1 - i // 2 for i in range(count)]
+
+
+def ranked_at(index, count):
+    return jnp.where(index % 2 == 0, index // 2, count - 1 - index // 2)
 
 
 def iota(shape, dim):
@@ -125,13 +133,15 @@
     nstate_copy.wait()
 
 
-def state_kernel(keep_ref, adk_ref, value_ref, mem_ref, out_ref, made, sems):
+def state_kernel(keep_ref, adk_ref, value_ref, mem_ref, _, *refs, first, last):
+    *_, out_ref, made, sems = refs
     adk_cols = jnp.transpose(adk_ref[...])
     copies = []
-    for t in range(mem_ref.shape[0]):
+    for t in range(first, last):
         old = keep_ref[t : t + 1, :] * mem_ref[t]
-        made[t] = old + adk_cols[:, t : t + 1] * value_ref[t : t + 1, :]
-        copies.append(pltpu.make_async_copy(made.at[t], out_ref.at[t], sems.at[t]))
+        i = t - first
+        made[i] = old + adk_cols[:, t : t + 1] * value_ref[t : t + 1, :]
+        copies.append(pltpu.make_async_copy(made.at[i], out_ref.at[t], sems.at[i]))
         copies[-1].start()
     for copy in copies:
         copy.wait()
@@ -139,21 +149,23 @@
 
 def pair_kernel(own_ref, got_ref, out_ref):
     total = (own_ref[...] + got_ref[...].astype(F32)).astype(BF16)
-    places, cores, _, span = out_ref.shape
-    for core in range(cores):
-        piece = total[:, core * span : (core + 1) * span]
-        for place in range(places):
-            out_ref[place, core] = piece
-
-
-def join_kernel(got_ref, out_ref):
-    owners, chips, cores, rows, span = got_ref.shape
-    for core in range(cores):
-        total = got_ref[:, 0, core].astype(F32)
-        for chip in range(1, chips):
-            total = total + got_ref[:, chip, core].astype(F32)
-        total = total.astype(BF16).reshape(owners * rows, span)
-        out_ref[:, core * span : (core + 1) * span] = total
+    devices, _, span = out_ref.shape
+    for rank, device in enumerate(ranked(devices)):
+        core = device % 2
+        out_ref[rank] = total[:, core * span : (core + 1) * span]
+
+
+def join_kernel(got_ref, *refs, heads):
+    out_ref = refs[-1]
+    devices, rows, span = got_ref.shape
+    rank_of = {device: rank for rank, device in enumerate(ranked(devices))}
+    for owner in range(devices // heads):
+        for core in range(2):
+            total = 0.0
+            for chip in range(heads // 2):
+                total = total + got_ref[rank_of[owner * heads + 2 * chip + core]].astype(F32)
+            place = slice(owner * rows, (owner + 1) * rows), slice(core * span, (core + 1) * span)
+            out_ref[place] = total.astype(BF16)
 
 
 def earlier_matrix(count):
@@ -192,19 +204,23 @@
 
 def pick_matrix(slots, start, size, sources, part):
     experts = slots.shape[0]
-    column = iota((experts, size), 1) + start
-    expand = (column // (sources * part) == iota((experts, size), 0)).astype(BF16)
+
+    def device(shape):
+        return ranked_at((iota(shape, len(shape) - 1) + start) // part, experts * sources)
+
+    shape = (experts, size)
+    expand = (device(shape) // sources == iota(shape, 0)).astype(BF16)
     expanded = lax.dot_general(
         slots, expand, (((0,), (0,)), ((), ())), preferred_element_type=F32
     )
     column = iota((1, size), 1) + start
-    source = (column // part) % sources
-    slot = (source % (EXPERT_CAPACITY // part)) * part + column % part
+    groups = EXPERT_CAPACITY // part
+    slot = (device((1, size)) % sources % groups) * part + column % part
     return (expanded == slot.astype(F32)).astype(BF16)
 
 
 def expert_kernel(
-    own_ref, got_ref, gain_ref, chosen_ref, share_ref, wg_ref, wu_ref, wd_ref,
+    own_ref, got_ref, gain_ref, chosen_ref, share_ref, wg_ref, wu_ref, wd_ref, _,
     keep_ref, send_ref, *block_refs,
 ):
     expert, half = lax.axis_index("ep"), lax.axis_index("tp") % 2
@@ -239,13 +255,12 @@
     send_ref[...] = jnp.where(half == 0, high, low)
 
 
-def spread_kernel(own_ref, got_ref, out_ref):
+def spread_kernel(own_ref, got_ref, _, out_ref, *, heads):
     total = (own_ref[...].astype(F32) + got_ref[...].astype(F32)).astype(BF16)
-    owners, copies, _, cols = out_ref.shape
-    for owner in range(owners):
-        piece = total[:, owner * cols : (owner + 1) * cols]
-        for copy in range(copies):
-            out_ref[owner, copy] = piece
+    devices, _, cols = out_ref.shape
+    for rank, device in enumerate(ranked(devices)):
+        owner = device // heads
+        out_ref[rank] = total[:, owner * cols : (owner + 1) * cols]
 
 
 def mix_kernel(middle_ref, pick_ref, got_ref, out_ref):
@@ -269,6 +284,25 @@
 def paired(values):
     heads = lax.axis_size("tp")
     return lax.ppermute(values, "tp", [(i, i ^ 1) for i in range(heads)])
+
+
+def update(parts, first, last, after, *begun):
+    hbm = pl.BlockSpec(memory_space=pl.ANY)
+    shape = parts[-1].shape
+    begun = [far(part) for part in begun]
+    return call(
+        functools.partial(state_kernel, first=first, last=last),
+        pltpu.HBM(shape, F32),
+        [pl.BlockSpec(memory_space=pltpu.VMEM)] * 5 + [hbm] * len(begun),
+        "state",
+        out_specs=hbm,
+        scratch_shapes=[
+            pltpu.VMEM((last - first,) + shape[1:], F32),
+            pltpu.SemaphoreType.DMA((last - first,)),
+        ],
+        input_output_aliases={5: 0} if begun else {},
+        cost_estimate=pl.CostEstimate(flops=1 << 20, bytes_accessed=1 << 20, transcendentals=0),
+    )(*map(near, parts), near(after), *begun)
 
 
 def near(values):
@@ -376,20 +410,28 @@
         cost_estimate=pl.CostEstimate(flops=1 << 22, bytes_accessed=1 << 16, transcendentals=0),
     )(near(near_route), near(near_weight))
     got, chosen, share, pick = lax.optimization_barrier((paired(send), chosen, share, pick))
+    devices = owners * heads
+    order = [ranked(devices)]
+    weights = [near(w_gate[0]), near(w_up[0]), near(w_down[0])]
     chunks = call(
-        pair_kernel, pltpu.VMEM((owners * chips, 2, rows, span // 2), BF16), [vmem] * 2, "pair"
+        pair_kernel, pltpu.VMEM((devices, rows, span // 2), BF16), [vmem] * 2, "pair"
     )(near(own), near(got))
-    chunks = chunks.reshape(owners * heads, rows, span // 2)
-    chunks = lax.all_to_all(chunks, ("ep", "tp"), split_axis=0, concat_axis=0, tiled=True)
-    own = call(join_kernel, pltpu.VMEM((count, span), BF16), [vmem], "join")(
-        near(chunks.reshape(owners, chips, 2, rows, span // 2))
-    )
+    chunks = lax.all_to_all(
+        chunks, ("ep", "tp"), split_axis=0, concat_axis=0, tiled=True, axis_index_groups=order
+    )
+    own = call(
+        functools.partial(join_kernel, heads=heads),
+        pltpu.VMEM((count, span), BF16),
+        [vmem] * 4,
+        "join",
+    )(near(chunks), *weights)
     got = paired(own)
+    state = update(state_parts, 0, rows // 2, own)
     kept, send, *own_middle = call(
         expert_kernel,
         (pltpu.VMEM((part, width), BF16), pltpu.VMEM((part, width), BF16))
         + ((pltpu.VMEM((count, cols), BF16),) if aligned else ()),
-        [vmem] * 8,
+        [vmem] * 8 + [hbm],
         "expert",
     )(
         near(own),
@@ -397,26 +439,18 @@
         near(gain),
         near(chosen),
         near(share),
-        near(w_gate[0]),
-        near(w_up[0]),
-        near(w_down[0]),
-    )
-    send, state_parts = lax.optimization_barrier((send, state_parts))
+        *weights,
+        far(state),
+    )
     handed = paired(send)
-    state = call(
-        state_kernel,
-        pltpu.HBM((rows, qk_dim, dv), F32),
-        [vmem] * 4,
-        "state",
-        out_specs=hbm,
-        scratch_shapes=[pltpu.VMEM((rows, qk_dim, dv), F32), pltpu.SemaphoreType.DMA((rows,))],
-        cost_estimate=pl.CostEstimate(flops=1 << 20, bytes_accessed=1 << 21, transcendentals=0),
-    )(*map(near, state_parts))
-    handed, state = lax.optimization_barrier((handed, state))
+    state = update(state_parts, rows // 2, rows, send, state)
     if aligned:
         pieces = call(
-            spread_kernel, pltpu.VMEM((owners, heads, part, cols), BF16), [vmem, vmem], "spread"
-        )(near(kept), near(handed))
+            functools.partial(spread_kernel, heads=heads),
+            pltpu.VMEM((devices, part, cols), BF16),
+            [vmem, vmem, hbm],
+            "spread",
+        )(near(kept), near(handed), far(state))
     else:
         first = lax.axis_index("tp") % 2 == 0
         sides = jnp.stack([jnp.where(first, own, got), jnp.where(first, got, own)], axis=1)
@@ -425,9 +459,10 @@
         own_middle = [lax.dynamic_slice_in_dim(middle, start, cols, axis=1)]
         total = (kept.astype(F32) + handed.astype(F32)).astype(BF16)
         total = total.reshape(part, owners, cols).transpose(1, 0, 2)
-        pieces = jnp.broadcast_to(total[:, None], (owners, heads, part, cols))
-    pieces = pieces.reshape(owners * heads, part, cols)
-    results = lax.all_to_all(pieces, ("ep", "tp"), split_axis=0, concat_axis=0, tiled=True)
+        pieces = total[jnp.asarray(order[0]) // heads]
+    results = lax.all_to_all(
+        pieces, ("ep", "tp"), split_axis=0, concat_axis=0, tiled=True, axis_index_groups=order
+    )
     results = near(results.reshape(got_rows, cols))
     if short:
         mixed = call(mix_kernel, spec((count, cols), BF16), [vmem] * 3, "mix")(

time: 34.2 us -> 33.3 us (0.974)
  blocking collectives: 25.1 us -> 24 us
  waiting for transfers between devices: 1.55 us -> 0.51 us
  Pallas kernels: 5.49 us -> 6.33 us
  starting transfers between devices: 1.13 us -> 1.48 us
    ppermute x3, waiting for transfers between devices: 1.55 us -> 0.51 us  [paired(): return lax.ppermute(values, 'tp', [(i, i ^ 1) for i in range(heads)])]
    pallas_call x4 -> x5, Pallas kernels: 1.3 us -> 2.13 us  [the longest x2 2.08 us: update(): call(functools.partial(state_kernel, first=first, last=last), pltpu.HBM(s...]
    all_to_all x1, blocking collectives: 9.91 us -> 9.35 us  [shards(): lax.all_to_all(pieces, ('ep', 'tp'), split_axis=0, concat_axis=0, tiled=T...]
    all_to_all x1, blocking collectives: 15.2 us -> 14.6 us  [shards(): lax.all_to_all(chunks, ('ep', 'tp'), split_axis=0, concat_axis=0, tiled=T...]
    ppermute x3, starting transfers between devices: 1.13 us -> 1.48 us  [paired(): return lax.ppermute(values, 'tp', [(i, i ^ 1) for i in range(heads)])]
  transfers between devices with their start and end apart: 3 -> 3, of which waited for: 2 -> 1; matrix products, arithmetic and copies ran while one was open for 0% -> 0% of each run, Pallas kernels for 5% -> 7%
where the time goes in v7:
time: 33.3 us; the launch traced here: 33 us
  blocking collectives  24 us (72%)
  Pallas kernels  6.33 us (19%)
  starting transfers between devices  1.48 us (4%)
  between operations  0.73 us (2%)
  waiting for transfers between devices  0.51 us (2%)
    all_to_all x1, blocking collectives, shards(): lax.all_to_all(chunks, ('ep', 'tp'), split_axis=0, concat_axis=0, tiled=T...  14.6 us
    all_to_all x1, blocking collectives, shards(): lax.all_to_all(pieces, ('ep', 'tp'), split_axis=0, concat_axis=0, tiled=T...  9.35 us
    pallas_call x1, Pallas kernels, shards(): call(cell_kernel, (pltpu.VMEM((rows, span), F32), pltpu.VMEM((rows, span)...  2.54 us
    pallas_call x2, Pallas kernels, update(): call(functools.partial(state_kernel, first=first, last=last), pltpu.HBM(s...  2.08 us
    ppermute x3, starting transfers between devices, paired(): return lax.ppermute(values, 'tp', [(i, i ^ 1) for i in range(heads)])  1.48 us
    pallas_call x1, Pallas kernels, shards(): call(mix_kernel, spec((count, cols), BF16), [vmem] * 3, 'mix')  0.77 us
  transfers between devices with their start and end apart: 3, of which 1 were waited for; matrix products, arithmetic and copies ran while one was open for 0% of the time, Pallas kernels for 7%

profile of v7, /device:TPU:0, one launch (start us, length us, event | category | flops | bytes accessed | tf_op | source)
XLA Modules:
  0.0 33.0 jit_solution(8509312123182450076)
XLA Ops:
  0.6 0.0 copy-start.1
  0.6 0.0 copy-start.2
  0.7 2.5 %cell.1 = (f32[8,512]{1,0:T(8,128)S(1)}, bf16[8,512]{1,0:T(8,128)(2,1)S(1)}, f32[8,128]{1,0:T(8,128)}, f32[1,8]{1,0:T(1,128)}, f32[8,256]{1,0:T(8,128)S(1)}, /*i...) custom-call(bf16[8,1024]{1,0:T(8,128)(2,1)} %refs_0_.1, ...), custom_call_target="tpu_custom_call" | custom-call | tf_op jit(solution)/shard_map/cell/pallas_call | solution.py:374
  3.2 0.0 copy-start
  3.2 0.6 %collective-permute-start = (bf16[8,512]{1,0:T(8,128)(2,1)S(1)}, bf16[8,512]{1,0:T(8,128)(2,1)S(1)}, u32[]{:S(2)}, u32[]{:S(2)}) collective-permute-start(bf16[8,512]{1,0:T(8,128)(2,1)S(1)} %get-tuple-element.26), channel_id=1, source_target_pairs={{0,1},{1,0},{2,3},{3,2},{4,5},{5,4},{6,7},{7,6},{8,9},{9,8},{10,11... | collective-permute-start | bytes 24584 | tf_op jit(solution)/shard_map/ppermute | solution.py:286
  3.8 0.3 plan.1
  4.1 0.5 %collective-permute-done.got_ref = bf16[8,512]{1,0:T(8,128)(2,1)S(1)} collective-permute-done((bf16[8,512]{1,0:T(8,128)(2,1)S(1)}, bf16[8,512]{1,0:T(8,128)(2,1)S(1)}, u32[]{:S(2)}, u32[]{:S(2)}) %collective-permute-start) | collective-permute-done | bytes 8224 | tf_op jit(solution)/shard_map/ppermute | solution.py:286
  4.6 14.6 %all_to_all.10.got_ref = bf16[32,8,256]{2,1,0:T(8,128)(2,1)S(1)} all-to-all(bf16[32,8,256]{2,1,0:T(8,128)(2,1)S(1)} %pair.1), channel_id=1, replica_groups={{0,31,1,30,2,29,3,28,4,27,5,26,6,25,7,24,8,23,9,22,10,21,11,20,12,19,13..., dimensions={0} | all-to-all | bytes 262144 | tf_op jit(solution)/shard_map/all_to_all | solution.py:419
  19.2 0.0 copy-done.1
  19.2 0.0 copy-done.2
  19.2 0.0 copy-done
  19.3 0.7 %collective-permute-start.1 = (bf16[64,512]{1,0:T(8,128)(2,1)S(1)}, bf16[64,512]{1,0:T(8,128)(2,1)S(1)}, u32[]{:S(2)}, u32[]{:S(2)}) collective-permute-start(bf16[64,512]{1,0:T(8,128)(2,1)S(1)} %join.1._.own_ref), channel_id=1, source_target_pairs={{0,1},{1,0},{2,3},{3,2},{4,5},{5,4},{6,7},{7,6},{8,9},{9,8},{10,11... | collective-permute-start | bytes 196616 | tf_op jit(solution)/shard_map/ppermute | solution.py:286
  20.0 1.0 %state.2._.refs_0_ = f32[8,128,256]{2,1,0:T(8,128)} custom-call(f32[8,256]{1,0:T(8,128)S(1)} %get-tuple-element.36.keep_ref, f32[8,128]{1,0:T(8,128)S(1)} %get-tuple-element.37.adk_ref, f32[8,256]{1,0:T(8,128)S(1)} %get-tuple-element.38.value_ref, f32[8,128,256]{2,1,0:T(8,128)S(1)} %get-tuple-element.39.mem_ref, bf16[64,512]{1,0:T(8,128)(2,1)S(1)} %join.1._.own_ref), custom_call_target="tpu_custom_call" | custom-call | flops 1048576 | bytes 1048576 | tf_op jit(solution)/shard_map/state/pallas_call | solution.py:293
  21.0 0.0 collective-permute-done.1.got_ref
  21.0 0.6 %expert.1 = (bf16[16,1024]{1,0:T(8,128)(2,1)S(1)}, bf16[16,1024]{1,0:T(8,128)(2,1)S(1)}, bf16[64,128]{1,0:T(8,128)(2,1)S(1)}) custom-call(bf16[64,512]{1,0:T(8,128)(2,1)S(1)} %join.1._.own_ref, bf16[64,512]{1,0:T(8,128)(2,1)S(1)} %collective-permute-done.1.got_ref, f32[1,1024]{1,0:T(1,128)S(1)} %get-tuple-element.33.gain_ref, ...), custom_call_target="tpu_custom_call" | custom-call | tf_op jit(solution)/shard_map/expert/pallas_call | solution.py:430
  21.6 0.3 collective-permute-start.2
  21.8 1.0 %state.3._ = f32[8,128,256]{2,1,0:T(8,128)} custom-call(f32[8,256]{1,0:T(8,128)S(1)} %get-tuple-element.36.keep_ref, f32[8,128]{1,0:T(8,128)S(1)} %get-tuple-element.37.adk_ref, f32[8,256]{1,0:T(8,128)S(1)} %get-tuple-element.38.value_ref, f32[8,128,256]{2,1,0:T(8,128)S(1)} %get-tuple-element.39.mem_ref, ...), custom_call_target="tpu_custom_call", output_to_operand_aliasing={{}: (5, {})} | custom-call | flops 1048576 | bytes 1048576 | tf_op jit(solution)/shard_map/state/pallas_call | solution.py:293
  22.9 0.0 collective-permute-done.2.got_ref
  22.9 9.3 %all_to_all.11 = bf16[32,16,128]{2,1,0:T(8,128)(2,1)S(1)} all-to-all(bf16[32,16,128]{2,1,0:T(8,128)(2,1)S(1)} %spread.1), channel_id=1, replica_groups={{0,31,1,30,2,29,3,28,4,27,5,26,6,25,7,24,8,23,9,22,10,21,11,20,12,19,13..., dimensions={0} | all-to-all | bytes 262144 | tf_op jit(solution)/shard_map/all_to_all | solution.py:463
  32.3 0.8 %mix.1 = bf16[64,128]{1,0:T(8,128)(2,1)} custom-call(bf16[64,128]{1,0:T(8,128)(2,1)S(1)} %get-tuple-element.40.middle_ref, bf16[64,512]{1,0:T(8,128)(2,1)S(1)} %get-tuple-element.41.pick_ref, bf16[512,128]{1,0:T(8,128)(2,1)S(1)} %bitcast.28), custom_call_target="tpu_custom_call" | custom-call | tf_op jit(solution)/shard_map/mix/pallas_call | solution.py:468
  (3 shorter events, 0.0 us)
Async XLA Ops:
  0.6 18.6 %copy-start.1 = (bf16[1,1024,128]{2,1,0:T(8,128)(2,1)S(1)}, bf16[1,1024,128]{2,1,0:T(8,128)(2,1)}, u32[]{:S(2)}) copy-start(bf16[1,1024,128]{2,1,0:T(8,128)(2,1)} %param.38) | copy-start | bytes 786436
  0.6 18.6 %copy-start.2 = (bf16[1,128,1024]{2,1,0:T(8,128)(2,1)S(1)}, bf16[1,128,1024]{2,1,0:T(8,128)(2,1)}, u32[]{:S(2)}) copy-start(bf16[1,128,1024]{2,1,0:T(8,128)(2,1)} %param.39) | copy-start | bytes 786436
  3.2 16.0 %copy-start = (bf16[1,1024,128]{2,1,0:T(8,128)(2,1)S(1)}, bf16[1,1024,128]{2,1,0:T(8,128)(2,1)}, u32[]{:S(2)}) copy-start(bf16[1,1024,128]{2,1,0:T(8,128)(2,1)} %param.37) | copy-start | bytes 786436
  3.2 1.4 %collective-permute-start = (bf16[8,512]{1,0:T(8,128)(2,1)S(1)}, bf16[8,512]{1,0:T(8,128)(2,1)S(1)}, u32[]{:S(2)}, u32[]{:S(2)}) collective-permute-start(bf16[8,512]{1,0:T(8,128)(2,1)S(1)} %get-tuple-element.26), channel_id=1, source_target_pairs={{0,1},{1,0},{2,3},{3,2},{4,5},{5,4},{6,7},{7,6},{8,9},{9,8},{10,11... | collective-permute-start | bytes 24584 | tf_op jit(solution)/shard_map/ppermute | solution.py:286
  19.3 1.7 %collective-permute-start.1 = (bf16[64,512]{1,0:T(8,128)(2,1)S(1)}, bf16[64,512]{1,0:T(8,128)(2,1)S(1)}, u32[]{:S(2)}, u32[]{:S(2)}) collective-permute-start(bf16[64,512]{1,0:T(8,128)(2,1)S(1)} %join.1._.own_ref), channel_id=1, source_target_pairs={{0,1},{1,0},{2,3},{3,2},{4,5},{5,4},{6,7},{7,6},{8,9},{9,8},{10,11... | collective-permute-start | bytes 196616 | tf_op jit(solution)/shard_map/ppermute | solution.py:286
  21.6 1.3 %collective-permute-start.2 = (bf16[16,1024]{1,0:T(8,128)(2,1)S(1)}, bf16[16,1024]{1,0:T(8,128)(2,1)S(1)}, u32[]{:S(2)}, u32[]{:S(2)}) collective-permute-start(bf16[16,1024]{1,0:T(8,128)(2,1)S(1)} %get-tuple-element.43._), channel_id=1, source_target_pairs={{0,1},{1,0},{2,3},{3,2},{4,5},{5,4},{6,7},{7,6},{8,9},{9,8},{10,11... | collective-permute-start | bytes 98312 | tf_op jit(solution)/shard_map/ppermute | solution.py:286

commit v8 on v7

--- a/solution.py
+++ b/solution.py
@@ -2,6 +2,7 @@
 
 import jax
 import jax.numpy as jnp
+import numpy as np
 from jax import lax
 from jax.experimental import pallas as pl
 from jax.experimental.pallas import tpu as pltpu
@@ -14,9 +15,9 @@
 VMEM_LIMIT = 32 << 20
 CELL_INPUTS = (
     "tokens", "mix", "wq", "wi", "wf", "bias", "max", "wk", "norm", "mem", "hgain", "fgain", "route",
-    "share", "wv", "wo", "wout",
+    "share", "source", "wv", "wo", "wout",
 )
-CELL_PASSED = ("mem", "fgain", "route", "share")
+CELL_PASSED = ("mem", "fgain", "route", "share", "source")
 
 F32 = jnp.float32
 BF16 = jnp.bfloat16
@@ -26,8 +27,8 @@
     return [i // 2 if i % 2 == 0 else count - 1 - i // 2 for i in range(count)]
 
 
-def ranked_at(index, count):
-    return jnp.where(index % 2 == 0, index // 2, count - 1 - index // 2)
+def led_by(leader, ranks):
+    return [leader] + [rank for rank in ranks if rank != leader]
 
 
 def iota(shape, dim):
@@ -61,9 +62,9 @@
     near_refs, (nstate_near, nmax_near), (sems, out_sems) = scratch[:count], scratch[count:-2], scratch[-2:]
     (
         own_ref, send_ref, nstate_ref, nmax_ref, keep_ref, adk_ref, value_ref, mem_ref, gain_ref,
-        route_ref, share_ref,
+        route_ref, share_ref, source_ref,
     ) = outs
-    direct = dict(zip(CELL_PASSED, (mem_ref, gain_ref, route_ref, share_ref)))
+    direct = dict(zip(CELL_PASSED, (mem_ref, gain_ref, route_ref, share_ref, source_ref)))
     copies, local = {}, {}
     for i, name in enumerate(CELL_INPUTS):
         local[name] = direct.get(name, near_refs[i])
@@ -97,7 +98,7 @@
     nmax_near[...] = row_of(new_max, eye)
     nmax_copy = pltpu.make_async_copy(nmax_near, nmax_ref, out_sems.at[0])
     nmax_copy.start()
-    ready("norm", "hgain", "fgain", "route", "share", "wq", "wk")
+    ready("norm", "hgain", "fgain", "route", "share", "source", "wq", "wk")
     query = rounded(normed, local["wq"][...])
     scaled_key = rounded(normed, local["wk"][...]) * query.shape[1] ** (-0.5)
     admitted = admit * scaled_key
@@ -133,48 +134,44 @@
     nstate_copy.wait()
 
 
-def state_kernel(keep_ref, adk_ref, value_ref, mem_ref, _, *refs, first, last):
+def state_kernel(keep_ref, adk_ref, value_ref, mem_ref, _, *refs, early):
     *_, out_ref, made, sems = refs
-    adk_cols = jnp.transpose(adk_ref[...])
-    copies = []
-    for t in range(first, last):
-        old = keep_ref[t : t + 1, :] * mem_ref[t]
-        i = t - first
-        made[i] = old + adk_cols[:, t : t + 1] * value_ref[t : t + 1, :]
-        copies.append(pltpu.make_async_copy(made.at[i], out_ref.at[t], sems.at[i]))
-        copies[-1].start()
-    for copy in copies:
-        copy.wait()
-
-
-def pair_kernel(own_ref, got_ref, out_ref):
+
+    @pl.when((lax.axis_index("ep") < lax.axis_size("ep") * 3 // 4) == early)
+    def write():
+        adk_cols = jnp.transpose(adk_ref[...])
+        copies = []
+        for t in range(mem_ref.shape[0]):
+            old = keep_ref[t : t + 1, :] * mem_ref[t]
+            made[t] = old + adk_cols[:, t : t + 1] * value_ref[t : t + 1, :]
+            copies.append(pltpu.make_async_copy(made.at[t], out_ref.at[t], sems.at[t]))
+            copies[-1].start()
+        for copy in copies:
+            copy.wait()
+
+
+def pair_kernel(own_ref, got_ref, _, out_ref):
     total = (own_ref[...] + got_ref[...].astype(F32)).astype(BF16)
-    devices, _, span = out_ref.shape
-    for rank, device in enumerate(ranked(devices)):
-        core = device % 2
-        out_ref[rank] = total[:, core * span : (core + 1) * span]
-
-
-def join_kernel(got_ref, *refs, heads):
+    for rank in range(out_ref.shape[0]):
+        out_ref[rank] = total
+
+
+def join_kernel(got_ref, *refs, order, chips):
     out_ref = refs[-1]
-    devices, rows, span = got_ref.shape
-    rank_of = {device: rank for rank, device in enumerate(ranked(devices))}
-    for owner in range(devices // heads):
-        for core in range(2):
-            total = 0.0
-            for chip in range(heads // 2):
-                total = total + got_ref[rank_of[owner * heads + 2 * chip + core]].astype(F32)
-            place = slice(owner * rows, (owner + 1) * rows), slice(core * span, (core + 1) * span)
-            out_ref[place] = total.astype(BF16)
+    rows = got_ref.shape[1]
+    rank_of = {place: rank for rank, place in enumerate(order)}
+    for owner in range(len(order) // chips):
+        total = 0.0
+        for chip in range(chips):
+            total = total + got_ref[rank_of[owner * chips + chip]].astype(F32)
+        out_ref[owner * rows : (owner + 1) * rows] = total.astype(BF16)
 
 
 def earlier_matrix(count):
     return (iota((count, count), 0) < iota((count, count), 1)).astype(BF16)
 
 
-def plan_kernel(
-    route_ref, weight_ref, chosen_ref, share_ref, *pick_refs, experts, sources, part
-):
+def plan_kernel(route_ref, weight_ref, source_ref, chosen_ref, share_ref, *pick_refs, experts):
     route, weight = route_ref[...], weight_ref[...]
     count = route.shape[1]
     named = route == lax.axis_index("ep")
@@ -189,7 +186,7 @@
     share_ref[...] = jnp.broadcast_to(slot_share, share_ref.shape)
     for pick_ref in pick_refs:
         slots = slot_table(route, experts)
-        pick_ref[...] = pick_matrix(slots, 0, pick_ref.shape[1], sources, part)
+        pick_ref[...] = pick_matrix(slots, source_ref[...])
 
 
 def slot_table(route, experts):
@@ -202,82 +199,72 @@
     return jnp.where(member, slots, -1.0).astype(BF16)
 
 
-def pick_matrix(slots, start, size, sources, part):
-    experts = slots.shape[0]
-
-    def device(shape):
-        return ranked_at((iota(shape, len(shape) - 1) + start) // part, experts * sources)
-
-    shape = (experts, size)
-    expand = (device(shape) // sources == iota(shape, 0)).astype(BF16)
+def pick_matrix(slots, source):
+    shape = (slots.shape[0], source.shape[1])
+    expand = (source == iota(shape, 0)).astype(BF16)
     expanded = lax.dot_general(
         slots, expand, (((0,), (0,)), ((), ())), preferred_element_type=F32
     )
-    column = iota((1, size), 1) + start
-    groups = EXPERT_CAPACITY // part
-    slot = (device((1, size)) % sources % groups) * part + column % part
+    slot = iota((1, shape[1]), 1) % EXPERT_CAPACITY
     return (expanded == slot.astype(F32)).astype(BF16)
 
 
 def expert_kernel(
     own_ref, got_ref, gain_ref, chosen_ref, share_ref, wg_ref, wu_ref, wd_ref, _,
-    keep_ref, send_ref, *block_refs,
+    out_ref, *block_refs, order, chips,
 ):
     expert, half = lax.axis_index("ep"), lax.axis_index("tp") % 2
     span = own_ref.shape[1]
     width = 2 * span
-    quarter = span // 2
     for block_ref in block_refs:
         cols = block_ref.shape[1]
         start = expert * cols
-        inner = pl.ds(pl.multiple_of(start // span * quarter + start % quarter, cols), cols)
-        mine = start % span // quarter == half
+        inner = pl.ds(pl.multiple_of(start % span, cols), cols)
+        mine = start // span == half
         block_ref[...] = jnp.where(mine, own_ref[:, inner], got_ref[:, inner])
     gate = up = 0.0
     chosen = chosen_ref[...]
-    pieces = []
+    sides = []
     for side, ref in ((half, own_ref), (1 - half, got_ref)):
         rows = dot(chosen, ref[...])
-        for core in range(2):
-            piece = rows[:, core * quarter : (core + 1) * quarter]
-            pieces.append((piece, pl.multiple_of(core * span + side * quarter, quarter)))
-    square = sum(jnp.sum(piece * piece, axis=-1, keepdims=True) for piece, _ in pieces)
+        sides.append((rows, pl.multiple_of(side * span, span)))
+    square = sum(jnp.sum(rows * rows, axis=-1, keepdims=True) for rows, _ in sides)
     scale = lax.rsqrt(square / width + EPS)
-    for piece, start in pieces:
-        normed = (piece * scale * gain_ref[:, pl.ds(start, quarter)]).astype(BF16)
-        gate = gate + dot(normed, wg_ref[pl.ds(start, quarter), :])
-        up = up + dot(normed, wu_ref[pl.ds(start, quarter), :])
+    for rows, start in sides:
+        normed = (rows * scale * gain_ref[:, pl.ds(start, span)]).astype(BF16)
+        gate = gate + dot(normed, wg_ref[pl.ds(start, span), :])
+        up = up + dot(normed, wu_ref[pl.ds(start, span), :])
     act = (jax.nn.silu(gate) * up).astype(BF16)
     result = (dot(act, wd_ref[...]) * share_ref[:, 0:1]).astype(BF16)
-    part = keep_ref.shape[0]
-    low, high = result[:part], result[part:]
-    keep_ref[...] = jnp.where(half == 0, low, high)
-    send_ref[...] = jnp.where(half == 0, high, low)
-
-
-def spread_kernel(own_ref, got_ref, _, out_ref, *, heads):
-    total = (own_ref[...].astype(F32) + got_ref[...].astype(F32)).astype(BF16)
-    devices, _, cols = out_ref.shape
-    for rank, device in enumerate(ranked(devices)):
-        owner = device // heads
-        out_ref[rank] = total[:, owner * cols : (owner + 1) * cols]
-
-
-def mix_kernel(middle_ref, pick_ref, got_ref, out_ref):
-    total = middle_ref[...].astype(F32) + dot(pick_ref[...], got_ref[...])
-    out_ref[...] = total.astype(BF16)
-
-
-def long_mix_kernel(middle_ref, route_ref, got_ref, out_ref, *, experts, sources, part):
+    if not block_refs:
+        out_ref[...] = result
+        return
+    for rank, place in enumerate(order):
+        owner = place // chips
+        out_ref[rank] = result[:, owner * cols : (owner + 1) * cols]
+
+
+def mix_kernel(pick_ref, got_ref, own_ref, send_ref):
+    total = dot(pick_ref[...], got_ref[...])
+    own_ref[...] = total
+    send_ref[...] = total.astype(BF16)
+
+
+def long_mix_kernel(route_ref, source_ref, got_ref, own_ref, send_ref, *, experts):
     slots = slot_table(route_ref[...], experts)
 
     def add(step, total):
-        start = step * CHUNK_ROWS
-        pick = pick_matrix(slots, start, CHUNK_ROWS, sources, part)
-        return total + dot(pick, got_ref[pl.ds(start, CHUNK_ROWS), :])
+        rows = pl.ds(pl.multiple_of(step * CHUNK_ROWS, CHUNK_ROWS), CHUNK_ROWS)
+        return total + dot(pick_matrix(slots, source_ref[:, rows]), got_ref[rows, :])
 
     steps = got_ref.shape[0] // CHUNK_ROWS
-    total = lax.fori_loop(0, steps, add, middle_ref[...].astype(F32))
+    total = lax.fori_loop(0, steps, add, jnp.zeros(own_ref.shape, F32))
+    own_ref[...] = total
+    send_ref[...] = total.astype(BF16)
+
+
+def final_kernel(middle_ref, own_ref, got_ref, out_ref):
+    total = middle_ref[...].astype(F32) + (own_ref[...] + got_ref[...].astype(F32))
     out_ref[...] = total.astype(BF16)
 
 
@@ -286,20 +273,17 @@
     return lax.ppermute(values, "tp", [(i, i ^ 1) for i in range(heads)])
 
 
-def update(parts, first, last, after, *begun):
+def update(parts, early, after, *begun):
     hbm = pl.BlockSpec(memory_space=pl.ANY)
     shape = parts[-1].shape
     begun = [far(part) for part in begun]
     return call(
-        functools.partial(state_kernel, first=first, last=last),
+        functools.partial(state_kernel, early=early),
         pltpu.HBM(shape, F32),
         [pl.BlockSpec(memory_space=pltpu.VMEM)] * 5 + [hbm] * len(begun),
         "state",
         out_specs=hbm,
-        scratch_shapes=[
-            pltpu.VMEM((last - first,) + shape[1:], F32),
-            pltpu.SemaphoreType.DMA((last - first,)),
-        ],
+        scratch_shapes=[pltpu.VMEM(shape, F32), pltpu.SemaphoreType.DMA(shape[:1])],
         input_output_aliases={5: 0} if begun else {},
         cost_estimate=pl.CostEstimate(flops=1 << 20, bytes_accessed=1 << 20, transcendentals=0),
     )(*map(near, parts), near(after), *begun)
@@ -341,11 +325,17 @@
     cols = width // owners
     count = route.shape[0]
     qk_dim, dv = w_query.shape[1], w_value.shape[1]
-    part = EXPERT_CAPACITY // 2
-    got_rows = owners * heads * part
+    places = owners * chips
+    got_rows = places * EXPERT_CAPACITY
     short = got_rows <= CHUNK_ROWS
     aligned = cols % LANES == 0
-    sizes = dict(experts=owners, sources=heads, part=part)
+    first_order = led_by(places // 2 - 1, range(places))
+    second_order = led_by(3 * places // 4 - 1, ranked(places)[::-1])
+    groups = [
+        [[2 * place + core for place in order] for core in range(2)]
+        for order in (first_order, second_order)
+    ]
+    source = np.repeat(np.array(second_order, np.int32) // chips, EXPERT_CAPACITY)
     spec = jax.ShapeDtypeStruct
     memory_rows = memory.reshape(rows, qk_dim, dv)
     cell_inputs = dict(
@@ -357,6 +347,7 @@
         max=running_max.T,
         route=route.T,
         share=route_weight.T,
+        source=jnp.asarray(source).reshape(1, -1),
         fgain=ffn_gain.reshape(1, -1),
         wq=w_query,
         wk=w_key,
@@ -371,7 +362,7 @@
     scratch = [
         (8, LANES) if name in CELL_PASSED else x.shape for name, x in zip(CELL_INPUTS, cell_inputs)
     ]
-    own, send, norm_state, new_max, *state_parts, gain, near_route, near_weight = call(
+    own, send, norm_state, new_max, *state_parts, gain, near_route, near_weight, near_source = call(
         cell_kernel,
         (
             pltpu.VMEM((rows, span), F32),
@@ -385,10 +376,11 @@
             pltpu.VMEM((1, width), F32),
             pltpu.VMEM((route.shape[1], count), jnp.int32),
             pltpu.VMEM((route.shape[1], count), F32),
+            pltpu.VMEM((1, got_rows), jnp.int32),
         ),
         [hbm] * len(cell_inputs),
         "cell",
-        out_specs=[vmem, vmem, hbm, hbm] + [vmem] * 7,
+        out_specs=[vmem, vmem, hbm, hbm] + [vmem] * 8,
         scratch_shapes=[pltpu.VMEM(shape, x.dtype) for shape, x in zip(scratch, cell_inputs)]
         + [
             pltpu.VMEM((rows, qk_dim), F32),
@@ -399,38 +391,37 @@
     )(*map(far, cell_inputs))
 
     chosen, share, *pick = call(
-        functools.partial(plan_kernel, **sizes),
+        functools.partial(plan_kernel, experts=owners),
         (
             pltpu.VMEM((EXPERT_CAPACITY, count), BF16),
             pltpu.VMEM((EXPERT_CAPACITY, LANES), F32),
         )
         + ((pltpu.VMEM((count, got_rows), BF16),) if short else ()),
-        [vmem] * 2,
+        [vmem] * 3,
         "plan",
         cost_estimate=pl.CostEstimate(flops=1 << 22, bytes_accessed=1 << 16, transcendentals=0),
-    )(near(near_route), near(near_weight))
+    )(near(near_route), near(near_weight), near(near_source))
     got, chosen, share, pick = lax.optimization_barrier((paired(send), chosen, share, pick))
-    devices = owners * heads
-    order = [ranked(devices)]
+    state = update(state_parts, True, send)
     weights = [near(w_gate[0]), near(w_up[0]), near(w_down[0])]
     chunks = call(
-        pair_kernel, pltpu.VMEM((devices, rows, span // 2), BF16), [vmem] * 2, "pair"
-    )(near(own), near(got))
+        pair_kernel, pltpu.VMEM((places, rows, span), BF16), [vmem] * 2 + [hbm], "pair"
+    )(near(own), near(got), far(state))
     chunks = lax.all_to_all(
-        chunks, ("ep", "tp"), split_axis=0, concat_axis=0, tiled=True, axis_index_groups=order
+        chunks, ("ep", "tp"), split_axis=0, concat_axis=0, tiled=True, axis_index_groups=groups[0]
     )
     own = call(
-        functools.partial(join_kernel, heads=heads),
+        functools.partial(join_kernel, order=first_order, chips=chips),
         pltpu.VMEM((count, span), BF16),
         [vmem] * 4,
         "join",
     )(near(chunks), *weights)
     got = paired(own)
-    state = update(state_parts, 0, rows // 2, own)
-    kept, send, *own_middle = call(
-        expert_kernel,
-        (pltpu.VMEM((part, width), BF16), pltpu.VMEM((part, width), BF16))
-        + ((pltpu.VMEM((count, cols), BF16),) if aligned else ()),
+    state = update(state_parts, False, own, state)
+    shape = (places, EXPERT_CAPACITY, cols) if aligned else (EXPERT_CAPACITY, width)
+    pieces, *own_middle = call(
+        functools.partial(expert_kernel, order=second_order, chips=chips),
+        (pltpu.VMEM(shape, BF16),) + ((pltpu.VMEM((count, cols), BF16),) if aligned else ()),
         [vmem] * 8 + [hbm],
         "expert",
     )(
@@ -442,39 +433,27 @@
         *weights,
         far(state),
     )
-    handed = paired(send)
-    state = update(state_parts, rows // 2, rows, send, state)
-    if aligned:
-        pieces = call(
-            functools.partial(spread_kernel, heads=heads),
-            pltpu.VMEM((devices, part, cols), BF16),
-            [vmem, vmem, hbm],
-            "spread",
-        )(near(kept), near(handed), far(state))
-    else:
+    if not aligned:
         first = lax.axis_index("tp") % 2 == 0
-        sides = jnp.stack([jnp.where(first, own, got), jnp.where(first, got, own)], axis=1)
-        middle = sides.reshape(count, 2, 2, span // 2).swapaxes(1, 2).reshape(count, width)
+        middle = jnp.concatenate([jnp.where(first, own, got), jnp.where(first, got, own)], axis=1)
         start = lax.axis_index("ep") * cols
         own_middle = [lax.dynamic_slice_in_dim(middle, start, cols, axis=1)]
-        total = (kept.astype(F32) + handed.astype(F32)).astype(BF16)
-        total = total.reshape(part, owners, cols).transpose(1, 0, 2)
-        pieces = total[jnp.asarray(order[0]) // heads]
+        pieces = pieces.reshape(EXPERT_CAPACITY, owners, cols).transpose(1, 0, 2)
+        pieces = pieces[np.array(second_order) // chips]
     results = lax.all_to_all(
-        pieces, ("ep", "tp"), split_axis=0, concat_axis=0, tiled=True, axis_index_groups=order
+        pieces, ("ep", "tp"), split_axis=0, concat_axis=0, tiled=True, axis_index_groups=groups[1]
     )
     results = near(results.reshape(got_rows, cols))
+    shapes = (pltpu.VMEM((count, cols), F32), pltpu.VMEM((count, cols), BF16))
     if short:
-        mixed = call(mix_kernel, spec((count, cols), BF16), [vmem] * 3, "mix")(
-            near(own_middle[0]), near(pick[0]), results
-        )
+        own, send = call(mix_kernel, shapes, [vmem] * 2, "mix")(near(pick[0]), results)
     else:
-        mixed = call(
-            functools.partial(long_mix_kernel, **sizes),
-            spec((count, cols), BF16),
-            [vmem] * 3,
-            "mix",
-        )(own_middle[0], route.T, results)
+        own, send = call(
+            functools.partial(long_mix_kernel, experts=owners), shapes, [vmem] * 3, "mix"
+        )(near(near_route), near(near_source), results)
+    mixed = call(final_kernel, spec((count, cols), BF16), [vmem] * 3, "final")(
+        near(own_middle[0]), near(own), near(paired(send))
+    )
     return (
         mixed,
         state.reshape(memory.shape),

time: 33.3 us -> 32.4 us (0.973)
  waiting for transfers between devices: 0.51 us -> 2.32 us
  blocking collectives: 24 us -> 22.7 us
  Pallas kernels: 6.33 us -> 5.55 us
  starting transfers between devices: 1.48 us -> 0.7 us
    ppermute x3, waiting for transfers between devices: 0.51 us -> 2.32 us  [paired(): return lax.ppermute(values, 'tp', [(i, i ^ 1) for i in range(heads)])]
    all_to_all x1, blocking collectives: 14.6 us -> 13 us  [shards(): lax.all_to_all(chunks, ('ep', 'tp'), split_axis=0, concat_axis=0, tiled=T...]
    ppermute x3, starting transfers between devices: 1.48 us -> 0.7 us  [paired(): return lax.ppermute(values, 'tp', [(i, i ^ 1) for i in range(heads)])]
    pallas_call x8, Pallas kernels: 3.78 us -> 3.03 us  [the longest x2 1.34 us: update(): call(functools.partial(state_kernel, early=early), pltpu.HBM(shape, F32),...]
    all_to_all x1, blocking collectives: 9.35 us -> 9.76 us  [shards(): lax.all_to_all(pieces, ('ep', 'tp'), split_axis=0, concat_axis=0, tiled=T...]
  transfers between devices with their start and end apart: 3 -> 3, of which waited for: 1 -> 2; matrix products, arithmetic and copies ran while one was open for 0% -> 0% of each run, Pallas kernels for 7% -> 5%
where the time goes in v8:
time: 32.4 us; the launch traced here: 32.1 us
  blocking collectives  22.7 us (70%)
  Pallas kernels  5.55 us (17%)
  waiting for transfers between devices  2.32 us (7%)
  between operations  0.74 us (2%)
  starting transfers between devices  0.7 us (2%)
    all_to_all x1, blocking collectives, shards(): lax.all_to_all(chunks, ('ep', 'tp'), split_axis=0, concat_axis=0, tiled=T...  13 us
    all_to_all x1, blocking collectives, shards(): lax.all_to_all(pieces, ('ep', 'tp'), split_axis=0, concat_axis=0, tiled=T...  9.76 us
    pallas_call x1, Pallas kernels, shards(): call(cell_kernel, (pltpu.VMEM((rows, span), F32), pltpu.VMEM((rows, span)...  2.52 us
    ppermute x3, waiting for transfers between devices, paired(): return lax.ppermute(values, 'tp', [(i, i ^ 1) for i in range(heads)])  2.32 us
    pallas_call x2, Pallas kernels, update(): call(functools.partial(state_kernel, early=early), pltpu.HBM(shape, F32),...  1.34 us
    ppermute x3, starting transfers between devices, paired(): return lax.ppermute(values, 'tp', [(i, i ^ 1) for i in range(heads)])  0.7 us
  transfers between devices with their start and end apart: 3, of which 2 were waited for; matrix products, arithmetic and copies ran while one was open for 0% of the time, Pallas kernels for 5%

profile of v8, /device:TPU:0, one launch (start us, length us, event | category | flops | bytes accessed | tf_op | source)
XLA Modules:
  0.0 32.1 jit_solution(18339354612798098785)
XLA Ops:
  0.6 2.5 %cell.1 = (f32[8,512]{1,0:T(8,128)S(1)}, bf16[8,512]{1,0:T(8,128)(2,1)S(1)}, f32[8,128]{1,0:T(8,128)}, f32[1,8]{1,0:T(1,128)}, f32[8,256]{1,0:T(8,128)S(1)}, /*i...) custom-call(bf16[8,1024]{1,0:T(8,128)(2,1)} %refs_0_.1, ...), custom_call_target="tpu_custom_call" | custom-call | tf_op jit(solution)/shard_map/cell/pallas_call | solution.py:365
  3.2 0.6 %collective-permute-start = (bf16[8,512]{1,0:T(8,128)(2,1)S(1)}, bf16[8,512]{1,0:T(8,128)(2,1)S(1)}, u32[]{:S(2)}, u32[]{:S(2)}) collective-permute-start(bf16[8,512]{1,0:T(8,128)(2,1)S(1)} %get-tuple-element.28._), channel_id=1, source_target_pairs={{0,1},{1,0},{2,3},{3,2},{4,5},{5,4},{6,7},{7,6},{8,9},{9,8},{10,11... | collective-permute-start | bytes 24584 | tf_op jit(solution)/shard_map/ppermute | solution.py:273
  3.7 1.2 %state.2._.refs_0_ = f32[8,128,256]{2,1,0:T(8,128)} custom-call(f32[8,256]{1,0:T(8,128)S(1)} %get-tuple-element.36.keep_ref, f32[8,128]{1,0:T(8,128)S(1)} %get-tuple-element.37.adk_ref, f32[8,256]{1,0:T(8,128)S(1)} %get-tuple-element.38.value_ref, f32[8,128,256]{2,1,0:T(8,128)S(1)} %get-tuple-element.39.mem_ref, bf16[8,512]{1,0:T(8,128)(2,1)S(1)} %get-tuple-element.28._), custom_call_target="tpu_custom_call" | custom-call | flops 1048576 | bytes 1048576 | tf_op jit(solution)/shard_map/state/pallas_call | solution.py:280
  5.0 0.3 plan.1
  5.3 0.0 collective-permute-done.got_ref
  5.3 0.0 copy-start.1
  5.3 0.0 copy-start.2
  5.4 0.0 copy-start
  5.4 13.0 %all_to_all.10.got_ref = bf16[16,8,512]{2,1,0:T(8,128)(2,1)S(1)} all-to-all(bf16[16,8,512]{2,1,0:T(8,128)(2,1)S(1)} %pair.1), channel_id=1, replica_groups={{14,0,2,4,6,8,10,12,16,18,20,22,24,26,28,30},{15,1,3,5,7,9,11,13,17,19,..., dimensions={0} | all-to-all | bytes 262144 | tf_op jit(solution)/shard_map/all_to_all | solution.py:410
  18.3 0.0 copy-done.1
  18.3 0.0 copy-done.2
  18.3 0.0 copy-done
  18.4 0.1 collective-permute-start.1
  18.5 0.1 state.3._
  18.6 1.1 %collective-permute-done.1.got_ref = bf16[64,512]{1,0:T(8,128)(2,1)S(1)} collective-permute-done((bf16[64,512]{1,0:T(8,128)(2,1)S(1)}, bf16[64,512]{1,0:T(8,128)(2,1)S(1)}, u32[]{:S(2)}, u32[]{:S(2)}) %collective-permute-start.1) | collective-permute-done | bytes 65568 | tf_op jit(solution)/shard_map/ppermute | solution.py:273
  19.7 0.6 %expert.1 = (bf16[16,32,128]{2,1,0:T(8,128)(2,1)S(1)}, bf16[64,128]{1,0:T(8,128)(2,1)S(1)}) custom-call(bf16[64,512]{1,0:T(8,128)(2,1)S(1)} %join.1._.own_ref, bf16[64,512]{1,0:T(8,128)(2,1)S(1)} %collective-permute-done.1.got_ref, f32[1,1024]{1,0:T(1,128)S(1)} %get-tuple-element.40.gain_ref, bf16[32,64]{1,0:T(8,128)(2,1)S(1)} %get-tuple-element.41.chosen_ref, ...), custom_call_target="tpu_custom_call" | custom-call | tf_op jit(solution)/shard_map/expert/pallas_call | solution.py:422
  20.3 9.8 %all_to_all.11 = bf16[16,32,128]{2,1,0:T(8,128)(2,1)S(1)} all-to-all(bf16[16,32,128]{2,1,0:T(8,128)(2,1)S(1)} %get-tuple-element.45), channel_id=1, replica_groups={{22,16,14,18,12,20,10,8,24,6,26,4,28,2,30,0},{23,17,15,19,13,21,11,9,25..., dimensions={0} | all-to-all | bytes 262144 | tf_op jit(solution)/shard_map/all_to_all | solution.py:443
  30.0 0.2 mix.1
  30.2 0.1 collective-permute-start.2
  30.3 1.2 %collective-permute-done.2.got_ref = bf16[64,128]{1,0:T(8,128)(2,1)S(1)} collective-permute-done((bf16[64,128]{1,0:T(8,128)(2,1)S(1)}, bf16[64,128]{1,0:T(8,128)(2,1)S(1)}, u32[]{:S(2)}, u32[]{:S(2)}) %collective-permute-start.2) | collective-permute-done | bytes 16416 | tf_op jit(solution)/shard_map/ppermute | solution.py:273
  31.4 0.6 %final.1 = bf16[64,128]{1,0:T(8,128)(2,1)} custom-call(bf16[64,128]{1,0:T(8,128)(2,1)S(1)} %get-tuple-element.43.middle_ref, f32[64,128]{1,0:T(8,128)S(1)} %get-tuple-element.46.own_ref, bf16[64,128]{1,0:T(8,128)(2,1)S(1)} %collective-permute-done.2.got_ref), custom_call_target="tpu_custom_call" | custom-call | tf_op jit(solution)/shard_map/final/pallas_call | solution.py:454
  (2 shorter events, 0.0 us)
Async XLA Ops:
  3.2 2.1 %collective-permute-start = (bf16[8,512]{1,0:T(8,128)(2,1)S(1)}, bf16[8,512]{1,0:T(8,128)(2,1)S(1)}, u32[]{:S(2)}, u32[]{:S(2)}) collective-permute-start(bf16[8,512]{1,0:T(8,128)(2,1)S(1)} %get-tuple-element.28._), channel_id=1, source_target_pairs={{0,1},{1,0},{2,3},{3,2},{4,5},{5,4},{6,7},{7,6},{8,9},{9,8},{10,11... | collective-permute-start | bytes 24584 | tf_op jit(solution)/shard_map/ppermute | solution.py:273
  5.3 13.0 %copy-start.1 = (bf16[1,1024,128]{2,1,0:T(8,128)(2,1)S(1)}, bf16[1,1024,128]{2,1,0:T(8,128)(2,1)}, u32[]{:S(2)}) copy-start(bf16[1,1024,128]{2,1,0:T(8,128)(2,1)} %param.39) | copy-start | bytes 786436
  5.3 13.0 %copy-start.2 = (bf16[1,128,1024]{2,1,0:T(8,128)(2,1)S(1)}, bf16[1,128,1024]{2,1,0:T(8,128)(2,1)}, u32[]{:S(2)}) copy-start(bf16[1,128,1024]{2,1,0:T(8,128)(2,1)} %param.40) | copy-start | bytes 786436
  5.4 13.0 %copy-start = (bf16[1,1024,128]{2,1,0:T(8,128)(2,1)S(1)}, bf16[1,1024,128]{2,1,0:T(8,128)(2,1)}, u32[]{:S(2)}) copy-start(bf16[1,1024,128]{2,1,0:T(8,128)(2,1)} %param.38) | copy-start | bytes 786436
  18.4 1.3 %collective-permute-start.1 = (bf16[64,512]{1,0:T(8,128)(2,1)S(1)}, bf16[64,512]{1,0:T(8,128)(2,1)S(1)}, u32[]{:S(2)}, u32[]{:S(2)}) collective-permute-start(bf16[64,512]{1,0:T(8,128)(2,1)S(1)} %join.1._.own_ref), channel_id=1, source_target_pairs={{0,1},{1,0},{2,3},{3,2},{4,5},{5,4},{6,7},{7,6},{8,9},{9,8},{10,11... | collective-permute-start | bytes 196616 | tf_op jit(solution)/shard_map/ppermute | solution.py:273
  30.2 1.2 %collective-permute-start.2 = (bf16[64,128]{1,0:T(8,128)(2,1)S(1)}, bf16[64,128]{1,0:T(8,128)(2,1)S(1)}, u32[]{:S(2)}, u32[]{:S(2)}) collective-permute-start(bf16[64,128]{1,0:T(8,128)(2,1)S(1)} %get-tuple-element.47), channel_id=1, source_target_pairs={{0,1},{1,0},{2,3},{3,2},{4,5},{5,4},{6,7},{7,6},{8,9},{9,8},{10,11... | collective-permute-start | bytes 49160 | tf_op jit(solution)/shard_map/ppermute | solution.py:273

commit v9 on v8

--- a/solution.py
+++ b/solution.py
@@ -137,7 +137,7 @@
 def state_kernel(keep_ref, adk_ref, value_ref, mem_ref, _, *refs, early):
     *_, out_ref, made, sems = refs
 
-    @pl.when((lax.axis_index("ep") < lax.axis_size("ep") * 3 // 4) == early)
+    @pl.when((lax.axis_index("ep") < lax.axis_size("ep") // 2) == early)
     def write():
         adk_cols = jnp.transpose(adk_ref[...])
         copies = []
@@ -210,7 +210,7 @@
 
 
 def expert_kernel(
-    own_ref, got_ref, gain_ref, chosen_ref, share_ref, wg_ref, wu_ref, wd_ref, _,
+    own_ref, got_ref, gain_ref, chosen_ref, share_ref, wg_ref, wu_ref, wd_ref,
     out_ref, *block_refs, order, chips,
 ):
     expert, half = lax.axis_index("ep"), lax.axis_index("tp") % 2
@@ -263,7 +263,7 @@
     send_ref[...] = total.astype(BF16)
 
 
-def final_kernel(middle_ref, own_ref, got_ref, out_ref):
+def final_kernel(middle_ref, own_ref, got_ref, _, out_ref):
     total = middle_ref[...].astype(F32) + (own_ref[...] + got_ref[...].astype(F32))
     out_ref[...] = total.astype(BF16)
 
@@ -329,11 +329,14 @@
     got_rows = places * EXPERT_CAPACITY
     short = got_rows <= CHUNK_ROWS
     aligned = cols % LANES == 0
-    first_order = led_by(places // 2 - 1, range(places))
+    first_order = led_by(3 * places // 4 - 1, range(places))
     second_order = led_by(3 * places // 4 - 1, ranked(places)[::-1])
     groups = [
-        [[2 * place + core for place in order] for core in range(2)]
-        for order in (first_order, second_order)
+        [[2 * place + core for place in first_order] for core in range(2)],
+        [
+            [2 * place + (core + (place >= places // 2)) % 2 for place in second_order]
+            for core in range(2)
+        ],
     ]
     source = np.repeat(np.array(second_order, np.int32) // chips, EXPERT_CAPACITY)
     spec = jax.ShapeDtypeStruct
@@ -417,12 +420,11 @@
         "join",
     )(near(chunks), *weights)
     got = paired(own)
-    state = update(state_parts, False, own, state)
     shape = (places, EXPERT_CAPACITY, cols) if aligned else (EXPERT_CAPACITY, width)
     pieces, *own_middle = call(
         functools.partial(expert_kernel, order=second_order, chips=chips),
         (pltpu.VMEM(shape, BF16),) + ((pltpu.VMEM((count, cols), BF16),) if aligned else ()),
-        [vmem] * 8 + [hbm],
+        [vmem] * 8,
         "expert",
     )(
         near(own),
@@ -431,7 +433,6 @@
         near(chosen),
         near(share),
         *weights,
-        far(state),
     )
     if not aligned:
         first = lax.axis_index("tp") % 2 == 0
@@ -451,8 +452,10 @@
         own, send = call(
             functools.partial(long_mix_kernel, experts=owners), shapes, [vmem] * 3, "mix"
         )(near(near_route), near(near_source), results)
-    mixed = call(final_kernel, spec((count, cols), BF16), [vmem] * 3, "final")(
-        near(own_middle[0]), near(own), near(paired(send))
+    got = paired(send)
+    state = update(state_parts, False, send, state)
+    mixed = call(final_kernel, spec((count, cols), BF16), [vmem] * 3 + [hbm], "final")(
+        near(own_middle[0]), near(own), near(got), far(state)
     )
     return (
         mixed,

time: 32.4 us -> 31.2 us (0.963)
  blocking collectives: 22.7 us -> 21.1 us
  starting transfers between devices: 0.7 us -> 1.47 us
    all_to_all x1, blocking collectives: 13 us -> 12.2 us  [shards(): lax.all_to_all(chunks, ('ep', 'tp'), split_axis=0, concat_axis=0, tiled=T...]
    all_to_all x1, blocking collectives: 9.76 us -> 8.97 us  [shards(): lax.all_to_all(pieces, ('ep', 'tp'), split_axis=0, concat_axis=0, tiled=T...]
    ppermute x3, starting transfers between devices: 0.7 us -> 1.47 us  [paired(): return lax.ppermute(values, 'tp', [(i, i ^ 1) for i in range(heads)])]
where the time goes in v9:
time: 31.2 us; the launch traced here: 30.9 us
  blocking collectives  21.1 us (68%)
  Pallas kernels  5.54 us (18%)
  waiting for transfers between devices  2 us (6%)
  starting transfers between devices  1.47 us (5%)
  between operations  0.73 us (2%)
    all_to_all x1, blocking collectives, shards(): lax.all_to_all(chunks, ('ep', 'tp'), split_axis=0, concat_axis=0, tiled=T...  12.2 us
    all_to_all x1, blocking collectives, shards(): lax.all_to_all(pieces, ('ep', 'tp'), split_axis=0, concat_axis=0, tiled=T...  8.97 us
    pallas_call x1, Pallas kernels, shards(): call(cell_kernel, (pltpu.VMEM((rows, span), F32), pltpu.VMEM((rows, span)...  2.52 us
    ppermute x3, waiting for transfers between devices, paired(): return lax.ppermute(values, 'tp', [(i, i ^ 1) for i in range(heads)])  2 us
    ppermute x3, starting transfers between devices, paired(): return lax.ppermute(values, 'tp', [(i, i ^ 1) for i in range(heads)])  1.47 us
    pallas_call x2, Pallas kernels, update(): call(functools.partial(state_kernel, early=early), pltpu.HBM(shape, F32),...  1.32 us
  transfers between devices with their start and end apart: 3, of which 2 were waited for; matrix products, arithmetic and copies ran while one was open for 0% of the time, Pallas kernels for 5%

profile of v9, /device:TPU:0, one launch (start us, length us, event | category | flops | bytes accessed | tf_op | source)
XLA Modules:
  0.0 30.9 jit_solution(14192868873618999539)
XLA Ops:
  0.6 2.5 %cell.1 = (f32[8,512]{1,0:T(8,128)S(1)}, bf16[8,512]{1,0:T(8,128)(2,1)S(1)}, f32[8,128]{1,0:T(8,128)}, f32[1,8]{1,0:T(1,128)}, f32[8,256]{1,0:T(8,128)S(1)}, /*i...) custom-call(bf16[8,1024]{1,0:T(8,128)(2,1)} %refs_0_.1, ...), custom_call_target="tpu_custom_call" | custom-call | tf_op jit(solution)/shard_map/cell/pallas_call | solution.py:368
  3.2 0.6 %collective-permute-start = (bf16[8,512]{1,0:T(8,128)(2,1)S(1)}, bf16[8,512]{1,0:T(8,128)(2,1)S(1)}, u32[]{:S(2)}, u32[]{:S(2)}) collective-permute-start(bf16[8,512]{1,0:T(8,128)(2,1)S(1)} %get-tuple-element.28._), channel_id=1, source_target_pairs={{0,1},{1,0},{2,3},{3,2},{4,5},{5,4},{6,7},{7,6},{8,9},{9,8},{10,11... | collective-permute-start | bytes 24584 | tf_op jit(solution)/shard_map/ppermute | solution.py:273
  3.7 1.2 %state.2._.refs_0_ = f32[8,128,256]{2,1,0:T(8,128)} custom-call(f32[8,256]{1,0:T(8,128)S(1)} %get-tuple-element.36.keep_ref, f32[8,128]{1,0:T(8,128)S(1)} %get-tuple-element.37.adk_ref, f32[8,256]{1,0:T(8,128)S(1)} %get-tuple-element.38.value_ref, f32[8,128,256]{2,1,0:T(8,128)S(1)} %get-tuple-element.39.mem_ref, bf16[8,512]{1,0:T(8,128)(2,1)S(1)} %get-tuple-element.28._), custom_call_target="tpu_custom_call" | custom-call | flops 1048576 | bytes 1048576 | tf_op jit(solution)/shard_map/state/pallas_call | solution.py:280
  5.0 0.3 %plan.1 = (bf16[32,64]{1,0:T(8,128)(2,1)S(1)}, f32[32,128]{1,0:T(8,128)S(1)}, bf16[64,512]{1,0:T(8,128)(2,1)S(1)}) custom-call(s32[2,64]{1,0:T(2,128)S(1)} %get-tuple-element.29.route_ref, f32[2,64]{1,0:T(2,128)S(1)} %get-tuple-element.30.weight_ref, s32[1,512]{1,0:T(1,128)S(1)} %get-tuple-element.31.source_ref), custom_call_target="tpu_custom_call" | custom-call | flops 4194304 | bytes 65536 | tf_op jit(solution)/shard_map/plan/pallas_call | solution.py:396
  5.3 0.0 collective-permute-done.got_ref
  5.3 0.0 copy-start.1
  5.3 0.0 copy-start.2
  5.4 0.0 copy-start
  5.4 12.2 %all_to_all.10.got_ref = bf16[16,8,512]{2,1,0:T(8,128)(2,1)S(1)} all-to-all(bf16[16,8,512]{2,1,0:T(8,128)(2,1)S(1)} %pair.1), channel_id=1, replica_groups={{22,0,2,4,6,8,10,12,14,16,18,20,24,26,28,30},{23,1,3,5,7,9,11,13,15,17,..., dimensions={0} | all-to-all | bytes 262144 | tf_op jit(solution)/shard_map/all_to_all | solution.py:413
  17.5 0.0 copy-done.1
  17.5 0.0 copy-done.2
  17.5 0.0 copy-done
  17.6 0.1 collective-permute-start.1
  17.6 1.2 %collective-permute-done.1.got_ref = bf16[64,512]{1,0:T(8,128)(2,1)S(1)} collective-permute-done((bf16[64,512]{1,0:T(8,128)(2,1)S(1)}, bf16[64,512]{1,0:T(8,128)(2,1)S(1)}, u32[]{:S(2)}, u32[]{:S(2)}) %collective-permute-start.1) | collective-permute-done | bytes 65568 | tf_op jit(solution)/shard_map/ppermute | solution.py:273
  18.9 0.6 %expert.1 = (bf16[16,32,128]{2,1,0:T(8,128)(2,1)S(1)}, bf16[64,128]{1,0:T(8,128)(2,1)S(1)}) custom-call(bf16[64,512]{1,0:T(8,128)(2,1)S(1)} %join.1.own_ref, bf16[64,512]{1,0:T(8,128)(2,1)S(1)} %collective-permute-done.1.got_ref, f32[1,1024]{1,0:T(1,128)S(1)} %get-tuple-element.40.gain_ref, bf16[32,64]{1,0:T(8,128)(2,1)S(1)} %get-tuple-element.41.chosen_ref, ...), custom_call_target="tpu_custom_call" | custom-call | tf_op jit(solution)/shard_map/expert/pallas_call | solution.py:424
  19.5 9.0 %all_to_all.11 = bf16[16,32,128]{2,1,0:T(8,128)(2,1)S(1)} all-to-all(bf16[16,32,128]{2,1,0:T(8,128)(2,1)S(1)} %get-tuple-element.45), channel_id=1, replica_groups={{23,17,14,19,12,21,10,8,25,6,27,4,29,2,31,0},{22,16,15,18,13,20,11,9,24..., dimensions={0} | all-to-all | bytes 262144 | tf_op jit(solution)/shard_map/all_to_all | solution.py:444
  28.4 0.2 mix.1
  28.6 0.8 %collective-permute-start.2 = (bf16[64,128]{1,0:T(8,128)(2,1)S(1)}, bf16[64,128]{1,0:T(8,128)(2,1)S(1)}, u32[]{:S(2)}, u32[]{:S(2)}) collective-permute-start(bf16[64,128]{1,0:T(8,128)(2,1)S(1)} %get-tuple-element.47._), channel_id=1, source_target_pairs={{0,1},{1,0},{2,3},{3,2},{4,5},{5,4},{6,7},{7,6},{8,9},{9,8},{10,11... | collective-permute-start | bytes 49160 | tf_op jit(solution)/shard_map/ppermute | solution.py:273
  29.4 0.1 state.3._
  29.5 0.8 %collective-permute-done.2.got_ref = bf16[64,128]{1,0:T(8,128)(2,1)S(1)} collective-permute-done((bf16[64,128]{1,0:T(8,128)(2,1)S(1)}, bf16[64,128]{1,0:T(8,128)(2,1)S(1)}, u32[]{:S(2)}, u32[]{:S(2)}) %collective-permute-start.2) | collective-permute-done | bytes 16416 | tf_op jit(solution)/shard_map/ppermute | solution.py:273
  30.3 0.6 %final.1 = bf16[64,128]{1,0:T(8,128)(2,1)} custom-call(bf16[64,128]{1,0:T(8,128)(2,1)S(1)} %get-tuple-element.43.middle_ref, f32[64,128]{1,0:T(8,128)S(1)} %get-tuple-element.46.own_ref, bf16[64,128]{1,0:T(8,128)(2,1)S(1)} %collective-permute-done.2.got_ref, f32[8,128,256]{2,1,0:T(8,128)} %state.3._), custom_call_target="tpu_custom_call" | custom-call | tf_op jit(solution)/shard_map/final/pallas_call | solution.py:457
  (2 shorter events, 0.0 us)
Async XLA Ops:
  3.2 2.1 %collective-permute-start = (bf16[8,512]{1,0:T(8,128)(2,1)S(1)}, bf16[8,512]{1,0:T(8,128)(2,1)S(1)}, u32[]{:S(2)}, u32[]{:S(2)}) collective-permute-start(bf16[8,512]{1,0:T(8,128)(2,1)S(1)} %get-tuple-element.28._), channel_id=1, source_target_pairs={{0,1},{1,0},{2,3},{3,2},{4,5},{5,4},{6,7},{7,6},{8,9},{9,8},{10,11... | collective-permute-start | bytes 24584 | tf_op jit(solution)/shard_map/ppermute | solution.py:273
  5.3 12.2 %copy-start.1 = (bf16[1,1024,128]{2,1,0:T(8,128)(2,1)S(1)}, bf16[1,1024,128]{2,1,0:T(8,128)(2,1)}, u32[]{:S(2)}) copy-start(bf16[1,1024,128]{2,1,0:T(8,128)(2,1)} %param.39) | copy-start | bytes 786436
  5.3 12.2 %copy-start.2 = (bf16[1,128,1024]{2,1,0:T(8,128)(2,1)S(1)}, bf16[1,128,1024]{2,1,0:T(8,128)(2,1)}, u32[]{:S(2)}) copy-start(bf16[1,128,1024]{2,1,0:T(8,128)(2,1)} %param.40) | copy-start | bytes 786436
  5.4 12.2 %copy-start = (bf16[1,1024,128]{2,1,0:T(8,128)(2,1)S(1)}, bf16[1,1024,128]{2,1,0:T(8,128)(2,1)}, u32[]{:S(2)}) copy-start(bf16[1,1024,128]{2,1,0:T(8,128)(2,1)} %param.38) | copy-start | bytes 786436
  17.6 1.3 %collective-permute-start.1 = (bf16[64,512]{1,0:T(8,128)(2,1)S(1)}, bf16[64,512]{1,0:T(8,128)(2,1)S(1)}, u32[]{:S(2)}, u32[]{:S(2)}) collective-permute-start(bf16[64,512]{1,0:T(8,128)(2,1)S(1)} %join.1.own_ref), channel_id=1, source_target_pairs={{0,1},{1,0},{2,3},{3,2},{4,5},{5,4},{6,7},{7,6},{8,9},{9,8},{10,11... | collective-permute-start | bytes 196616 | tf_op jit(solution)/shard_map/ppermute | solution.py:273
  28.6 1.7 %collective-permute-start.2 = (bf16[64,128]{1,0:T(8,128)(2,1)S(1)}, bf16[64,128]{1,0:T(8,128)(2,1)S(1)}, u32[]{:S(2)}, u32[]{:S(2)}) collective-permute-start(bf16[64,128]{1,0:T(8,128)(2,1)S(1)} %get-tuple-element.47._), channel_id=1, source_target_pairs={{0,1},{1,0},{2,3},{3,2},{4,5},{5,4},{6,7},{7,6},{8,9},{9,8},{10,11... | collective-permute-start | bytes 49160 | tf_op jit(solution)/shard_map/ppermute | solution.py:273

commit v10 on v9

--- a/solution.py
+++ b/solution.py
@@ -329,7 +329,7 @@
     got_rows = places * EXPERT_CAPACITY
     short = got_rows <= CHUNK_ROWS
     aligned = cols % LANES == 0
-    first_order = led_by(3 * places // 4 - 1, range(places))
+    first_order = led_by(3 * places // 4 - 1, ranked(places)[::-1])
     second_order = led_by(3 * places // 4 - 1, ranked(places)[::-1])
     groups = [
         [[2 * place + core for place in first_order] for core in range(2)],

time: 31.2 us -> 31 us (level)
  no operation moved by 1% of the time
where the time goes in v10:
time: 31 us; the launch traced here: 30.7 us
  blocking collectives  21.1 us (68%)
  Pallas kernels  5.54 us (18%)
  waiting for transfers between devices  2 us (6%)
  starting transfers between devices  1.33 us (4%)
  between operations  0.73 us (2%)
    all_to_all x1, blocking collectives, shards(): lax.all_to_all(chunks, ('ep', 'tp'), split_axis=0, concat_axis=0, tiled=T...  11.8 us
    all_to_all x1, blocking collectives, shards(): lax.all_to_all(pieces, ('ep', 'tp'), split_axis=0, concat_axis=0, tiled=T...  9.24 us
    pallas_call x1, Pallas kernels, shards(): call(cell_kernel, (pltpu.VMEM((rows, span), F32), pltpu.VMEM((rows, span)...  2.52 us
    ppermute x3, waiting for transfers between devices, paired(): return lax.ppermute(values, 'tp', [(i, i ^ 1) for i in range(heads)])  2 us
    ppermute x3, starting transfers between devices, paired(): return lax.ppermute(values, 'tp', [(i, i ^ 1) for i in range(heads)])  1.33 us
    pallas_call x2, Pallas kernels, update(): call(functools.partial(state_kernel, early=early), pltpu.HBM(shape, F32),...  1.32 us
  transfers between devices with their start and end apart: 3, of which 2 were waited for; matrix products, arithmetic and copies ran while one was open for 0% of the time, Pallas kernels for 5%

profile of v10, /device:TPU:0, one launch (start us, length us, event | category | flops | bytes accessed | tf_op | source)
XLA Modules:
  0.0 30.7 jit_solution(11714149358636127284)
XLA Ops:
  0.6 2.5 %cell.1 = (f32[8,512]{1,0:T(8,128)S(1)}, bf16[8,512]{1,0:T(8,128)(2,1)S(1)}, f32[8,128]{1,0:T(8,128)}, f32[1,8]{1,0:T(1,128)}, f32[8,256]{1,0:T(8,128)S(1)}, /*i...) custom-call(bf16[8,1024]{1,0:T(8,128)(2,1)} %refs_0_.1, ...), custom_call_target="tpu_custom_call" | custom-call | tf_op jit(solution)/shard_map/cell/pallas_call | solution.py:368
  3.2 0.6 %collective-permute-start = (bf16[8,512]{1,0:T(8,128)(2,1)S(1)}, bf16[8,512]{1,0:T(8,128)(2,1)S(1)}, u32[]{:S(2)}, u32[]{:S(2)}) collective-permute-start(bf16[8,512]{1,0:T(8,128)(2,1)S(1)} %get-tuple-element.28._), channel_id=1, source_target_pairs={{0,1},{1,0},{2,3},{3,2},{4,5},{5,4},{6,7},{7,6},{8,9},{9,8},{10,11... | collective-permute-start | bytes 24584 | tf_op jit(solution)/shard_map/ppermute | solution.py:273
  3.7 1.2 %state.2._.refs_0_ = f32[8,128,256]{2,1,0:T(8,128)} custom-call(f32[8,256]{1,0:T(8,128)S(1)} %get-tuple-element.36.keep_ref, f32[8,128]{1,0:T(8,128)S(1)} %get-tuple-element.37.adk_ref, f32[8,256]{1,0:T(8,128)S(1)} %get-tuple-element.38.value_ref, f32[8,128,256]{2,1,0:T(8,128)S(1)} %get-tuple-element.39.mem_ref, bf16[8,512]{1,0:T(8,128)(2,1)S(1)} %get-tuple-element.28._), custom_call_target="tpu_custom_call" | custom-call | flops 1048576 | bytes 1048576 | tf_op jit(solution)/shard_map/state/pallas_call | solution.py:280
  5.0 0.3 %plan.1 = (bf16[32,64]{1,0:T(8,128)(2,1)S(1)}, f32[32,128]{1,0:T(8,128)S(1)}, bf16[64,512]{1,0:T(8,128)(2,1)S(1)}) custom-call(s32[2,64]{1,0:T(2,128)S(1)} %get-tuple-element.29.route_ref, f32[2,64]{1,0:T(2,128)S(1)} %get-tuple-element.30.weight_ref, s32[1,512]{1,0:T(1,128)S(1)} %get-tuple-element.31.source_ref), custom_call_target="tpu_custom_call" | custom-call | flops 4194304 | bytes 65536 | tf_op jit(solution)/shard_map/plan/pallas_call | solution.py:396
  5.3 0.0 collective-permute-done.got_ref
  5.3 0.0 copy-start.1
  5.3 0.0 copy-start.2
  5.4 0.0 copy-start
  5.4 11.8 %all_to_all.10.got_ref = bf16[16,8,512]{2,1,0:T(8,128)(2,1)S(1)} all-to-all(bf16[16,8,512]{2,1,0:T(8,128)(2,1)S(1)} %pair.1), channel_id=1, replica_groups={{22,16,14,18,12,20,10,8,24,6,26,4,28,2,30,0},{23,17,15,19,13,21,11,9,25..., dimensions={0} | all-to-all | bytes 262144 | tf_op jit(solution)/shard_map/all_to_all | solution.py:413
  17.2 0.0 copy-done.1
  17.2 0.0 copy-done.2
  17.2 0.0 copy-done
  17.3 0.1 collective-permute-start.1
  17.3 1.2 %collective-permute-done.1.got_ref = bf16[64,512]{1,0:T(8,128)(2,1)S(1)} collective-permute-done((bf16[64,512]{1,0:T(8,128)(2,1)S(1)}, bf16[64,512]{1,0:T(8,128)(2,1)S(1)}, u32[]{:S(2)}, u32[]{:S(2)}) %collective-permute-start.1) | collective-permute-done | bytes 65568 | tf_op jit(solution)/shard_map/ppermute | solution.py:273
  18.6 0.6 %expert.1 = (bf16[16,32,128]{2,1,0:T(8,128)(2,1)S(1)}, bf16[64,128]{1,0:T(8,128)(2,1)S(1)}) custom-call(bf16[64,512]{1,0:T(8,128)(2,1)S(1)} %join.1.own_ref, bf16[64,512]{1,0:T(8,128)(2,1)S(1)} %collective-permute-done.1.got_ref, f32[1,1024]{1,0:T(1,128)S(1)} %get-tuple-element.40.gain_ref, bf16[32,64]{1,0:T(8,128)(2,1)S(1)} %get-tuple-element.41.chosen_ref, ...), custom_call_target="tpu_custom_call" | custom-call | tf_op jit(solution)/shard_map/expert/pallas_call | solution.py:424
  19.2 9.2 %all_to_all.11 = bf16[16,32,128]{2,1,0:T(8,128)(2,1)S(1)} all-to-all(bf16[16,32,128]{2,1,0:T(8,128)(2,1)S(1)} %get-tuple-element.45), channel_id=1, replica_groups={{23,17,14,19,12,21,10,8,25,6,27,4,29,2,31,0},{22,16,15,18,13,20,11,9,24..., dimensions={0} | all-to-all | bytes 262144 | tf_op jit(solution)/shard_map/all_to_all | solution.py:444
  28.4 0.2 mix.1
  28.6 0.7 %collective-permute-start.2 = (bf16[64,128]{1,0:T(8,128)(2,1)S(1)}, bf16[64,128]{1,0:T(8,128)(2,1)S(1)}, u32[]{:S(2)}, u32[]{:S(2)}) collective-permute-start(bf16[64,128]{1,0:T(8,128)(2,1)S(1)} %get-tuple-element.47._), channel_id=1, source_target_pairs={{0,1},{1,0},{2,3},{3,2},{4,5},{5,4},{6,7},{7,6},{8,9},{9,8},{10,11... | collective-permute-start | bytes 49160 | tf_op jit(solution)/shard_map/ppermute | solution.py:273
  29.3 0.1 state.3._
  29.3 0.8 %collective-permute-done.2.got_ref = bf16[64,128]{1,0:T(8,128)(2,1)S(1)} collective-permute-done((bf16[64,128]{1,0:T(8,128)(2,1)S(1)}, bf16[64,128]{1,0:T(8,128)(2,1)S(1)}, u32[]{:S(2)}, u32[]{:S(2)}) %collective-permute-start.2) | collective-permute-done | bytes 16416 | tf_op jit(solution)/shard_map/ppermute | solution.py:273
  30.1 0.6 %final.1 = bf16[64,128]{1,0:T(8,128)(2,1)} custom-call(bf16[64,128]{1,0:T(8,128)(2,1)S(1)} %get-tuple-element.43.middle_ref, f32[64,128]{1,0:T(8,128)S(1)} %get-tuple-element.46.own_ref, bf16[64,128]{1,0:T(8,128)(2,1)S(1)} %collective-permute-done.2.got_ref, f32[8,128,256]{2,1,0:T(8,128)} %state.3._), custom_call_target="tpu_custom_call" | custom-call | tf_op jit(solution)/shard_map/final/pallas_call | solution.py:457
  (2 shorter events, 0.0 us)
Async XLA Ops:
  3.2 2.1 %collective-permute-start = (bf16[8,512]{1,0:T(8,128)(2,1)S(1)}, bf16[8,512]{1,0:T(8,128)(2,1)S(1)}, u32[]{:S(2)}, u32[]{:S(2)}) collective-permute-start(bf16[8,512]{1,0:T(8,128)(2,1)S(1)} %get-tuple-element.28._), channel_id=1, source_target_pairs={{0,1},{1,0},{2,3},{3,2},{4,5},{5,4},{6,7},{7,6},{8,9},{9,8},{10,11... | collective-permute-start | bytes 24584 | tf_op jit(solution)/shard_map/ppermute | solution.py:273
  5.3 11.9 %copy-start.1 = (bf16[1,1024,128]{2,1,0:T(8,128)(2,1)S(1)}, bf16[1,1024,128]{2,1,0:T(8,128)(2,1)}, u32[]{:S(2)}) copy-start(bf16[1,1024,128]{2,1,0:T(8,128)(2,1)} %param.39) | copy-start | bytes 786436
  5.3 11.9 %copy-start.2 = (bf16[1,128,1024]{2,1,0:T(8,128)(2,1)S(1)}, bf16[1,128,1024]{2,1,0:T(8,128)(2,1)}, u32[]{:S(2)}) copy-start(bf16[1,128,1024]{2,1,0:T(8,128)(2,1)} %param.40) | copy-start | bytes 786436
  5.4 11.9 %copy-start = (bf16[1,1024,128]{2,1,0:T(8,128)(2,1)S(1)}, bf16[1,1024,128]{2,1,0:T(8,128)(2,1)}, u32[]{:S(2)}) copy-start(bf16[1,1024,128]{2,1,0:T(8,128)(2,1)} %param.38) | copy-start | bytes 786436
  17.3 1.3 %collective-permute-start.1 = (bf16[64,512]{1,0:T(8,128)(2,1)S(1)}, bf16[64,512]{1,0:T(8,128)(2,1)S(1)}, u32[]{:S(2)}, u32[]{:S(2)}) collective-permute-start(bf16[64,512]{1,0:T(8,128)(2,1)S(1)} %join.1.own_ref), channel_id=1, source_target_pairs={{0,1},{1,0},{2,3},{3,2},{4,5},{5,4},{6,7},{7,6},{8,9},{9,8},{10,11... | collective-permute-start | bytes 196616 | tf_op jit(solution)/shard_map/ppermute | solution.py:273
  28.6 1.5 %collective-permute-start.2 = (bf16[64,128]{1,0:T(8,128)(2,1)S(1)}, bf16[64,128]{1,0:T(8,128)(2,1)S(1)}, u32[]{:S(2)}, u32[]{:S(2)}) collective-permute-start(bf16[64,128]{1,0:T(8,128)(2,1)S(1)} %get-tuple-element.47._), channel_id=1, source_target_pairs={{0,1},{1,0},{2,3},{3,2},{4,5},{5,4},{6,7},{7,6},{8,9},{9,8},{10,11... | collective-permute-start | bytes 49160 | tf_op jit(solution)/shard_map/ppermute | solution.py:273
